TPU v7x, 32 devices: a whole 2x2x4 slice. The times are simulated.
32 devices in a mesh: sp: 16 (over z, y, x), tp: 2 (over core).
Axes of the slice: x: 2, y: 2, z: 4, core: 2. Of those that a mesh axis runs over, the one named last changes fastest.
Arguments:
- resid: bfloat16 [4096, 2048], P(('sp', 'tp')), may hold values from -6 to 6
- value_in: bfloat16 [4096, 1536], P('sp', 'tp'), may hold values from -6 to 6
- gate_in: bfloat16 [4096, 1536], P('sp', 'tp'), may hold values from -8 to 8
- conv_weight: float32 [31, 1536], P(None, 'tp'), may hold values from -2.5 to 2.5
- norm_gain: float32 [1536], P('tp'), may hold values from 0.1 to 1.9
- out_weight: bfloat16 [1536, 2048], replicated, may hold values from -0.15625 to 0.15625
- ffn_gain: float32 [2048], replicated, may hold values from 0.1 to 1.9
- expert_ids: int32 [4096, 2], P(('sp', 'tp')), may hold values from 0 to 31, all different within a row; in each aligned block of 128 rows (0 to 127, 128 to 255, ...) at most 16 rows name the same one
- expert_mix: float32 [4096, 2], P(('sp', 'tp')), may hold values from 0.1 to 1
- w_gate: bfloat16 [32, 2048, 1024], P(('sp', 'tp')), may hold values from -0.125 to 0.125
- w_up: bfloat16 [32, 2048, 1024], P(('sp', 'tp')), may hold values from -0.125 to 0.125
- w_down: bfloat16 [32, 1024, 2048], P(('sp', 'tp')), may hold values from -0.1875 to 0.1875
Outputs:
- layer_out: bfloat16 [4096, 2048], P(('sp', 'tp'))
Inputs may be any that keep to these rules, and one draw needn't show every extreme that they name: `expert_ids`: each row names 2 different experts; within each aligned block of 128 rows no expert is named by more than 16 rows, a bound that some block reaches.
All inputs are finite; a program needn't handle non-finite values.
Results may differ from a plain program's by a relative error of at most 0.012.
Values may be sent and summed in bfloat16 or wider, within the bound.
No kernel may reach another device: no remote copies, remote signals or barrier semaphores. Data moves between devices by JAX's collectives and lax.ppermute only.
A program may use at most 128 MiB of HBM per device.

v0:
```python
import jax
import jax.numpy as jnp
from jax import lax
from jax.sharding import PartitionSpec as P


def padded_2(block, sides, width):
    for axis, dim in sides:
        count = lax.axis_size(axis)
        forward = [(i, i + 1) for i in range(count - 1)]
        backward = [(target, source) for source, target in forward]
        low = lax.ppermute(
            lax.slice_in_dim(block, block.shape[dim] - width, None, axis=dim), axis, forward
        )
        high = lax.ppermute(lax.slice_in_dim(block, 0, width, axis=dim), axis, backward)
        block = jnp.concatenate([low, block, high], axis=dim)
    return block


def expert_apply(rows, gate_w, up_w, down_w):
    gate = jnp.dot(rows, gate_w, preferred_element_type=jnp.float32)
    up = jnp.dot(rows, up_w, preferred_element_type=jnp.float32)
    hidden = (jax.nn.silu(gate) * up).astype(jnp.bfloat16)
    return jnp.dot(hidden, down_w, preferred_element_type=jnp.float32).astype(jnp.bfloat16)


def per_device(
    resid,
    value_in,
    gate_in,
    conv_weight,
    norm_gain,
    out_weight,
    ffn_gain,
    expert_ids,
    expert_mix,
    w_gate,
    w_up,
    w_down,
):
    glu = (value_in.astype(jnp.float32) * jax.nn.sigmoid(gate_in.astype(jnp.float32))).astype(
        jnp.bfloat16
    )
    taps = conv_weight.shape[0]
    reach = taps // 2
    length = glu.shape[0]
    local_width = glu.shape[1]
    padded = padded_2(glu, (("sp", 0),), reach).astype(jnp.float32)
    conv = jnp.zeros((length, local_width), jnp.float32)
    for tap in range(taps):
        conv = conv + padded[tap : tap + length] * conv_weight[tap]
    sums = lax.psum((jnp.sum(conv, axis=1), jnp.sum(conv * conv, axis=1)), "tp")
    width = local_width * lax.axis_size("tp")
    mean = sums[0] / width
    var = sums[1] / width - mean * mean
    normed_conv = (conv - mean[:, None]) * lax.rsqrt(var + 1e-05)[:, None] * norm_gain
    mixed = jax.nn.silu(normed_conv).astype(jnp.bfloat16)
    regrouped = lax.all_to_all(mixed, "tp", split_axis=0, concat_axis=1, tiled=True)
    proj = jnp.dot(regrouped, out_weight, preferred_element_type=jnp.float32)
    stream = (resid.astype(jnp.float32) + proj).astype(jnp.bfloat16)
    wide = stream.astype(jnp.float32)
    normed = (
        wide * lax.rsqrt(jnp.mean(wide * wide, axis=1, keepdims=True) + 1e-06) * ffn_gain
    ).astype(jnp.bfloat16)
    sp_count = lax.axis_size("sp")
    tp_count = lax.axis_size("tp")
    experts_all = sp_count * tp_count
    rows_here = stream.shape[0]
    topk = expert_ids.shape[1]
    model_width = stream.shape[1]
    cap = max(2, (2 * topk * rows_here + experts_all - 1) // experts_all)
    flat = expert_ids.reshape(-1)
    onehot = (flat[:, None] == jnp.arange(experts_all, dtype=jnp.int32)[None, :]).astype(jnp.int32)
    rank = jnp.sum(jnp.cumsum(onehot, axis=0) * onehot, axis=1) - 1
    dest = flat * cap + rank
    owner = jnp.arange(rows_here * topk, dtype=jnp.int32) // topk
    table = jnp.full((experts_all * cap,), rows_here, jnp.int32).at[dest].set(owner)
    source = jnp.concatenate([normed, jnp.zeros((1, model_width), jnp.bfloat16)], axis=0)
    outgoing = jnp.take(source, table, axis=0).reshape(experts_all, cap, model_width)
    gate_w, up_w, down_w = (w_gate[0], w_up[0], w_down[0])
    arrived = lax.all_to_all(outgoing, ("sp", "tp"), split_axis=0, concat_axis=0, tiled=True)
    shape = arrived.shape
    done = expert_apply(arrived.reshape(-1, model_width), gate_w, up_w, down_w).reshape(shape)
    returned = lax.all_to_all(done, ("sp", "tp"), split_axis=0, concat_axis=0, tiled=True)
    picked = jnp.take(returned.reshape(experts_all * cap, model_width), dest, axis=0)
    picked = picked.astype(jnp.float32).reshape(rows_here, topk, model_width)
    total = wide + jnp.sum(picked * expert_mix[:, :, None], axis=1)
    return total.astype(jnp.bfloat16)


def solution(mesh):
    return jax.shard_map(
        per_device,
        mesh=mesh,
        in_specs=(
            P(("sp", "tp"), None),
            P("sp", "tp"),
            P("sp", "tp"),
            P(None, "tp"),
            P("tp"),
            P(),
            P(),
            P(("sp", "tp"), None),
            P(("sp", "tp"), None),
            P(("sp", "tp"), None, None),
            P(("sp", "tp"), None, None),
            P(("sp", "tp"), None, None),
        ),
        out_specs=P(("sp", "tp"), None),
        check_vma=False,
    )
```

profile of v0, /device:TPU:0, one launch (start us, length us, event | category | flops | bytes accessed | tf_op | source)
XLA Modules:
  0.0 166.2 jit_solution(5589472671035958623)
XLA Ops:
  0.0 1.3 multiply_convert_fusion.3
  1.4 4.9 %collective-permute-start = (bf16[15,768]{1,0:T(8,128)(2,1)S(1)}, bf16[15,768]{1,0:T(8,128)(2,1)S(1)}, u32[]{:S(2)}, u32[]{:S(2)}) collective-permute-start(bf16[15,768]{1,0:T(8,128)(2,1)S(1)} %get-tuple-element.41), channel_id=1, source_target_pairs={{0,2},{2,4},{4,6},{6,8},{8,10},{10,12},{12,14},{14,16},{16,18},{18... | collective-permute-start | bytes 69128 | tf_op jit(solution)/shard_map/ppermute | solution.py:12
  6.2 1.3 collective-permute-start.1
  7.5 1.5 slice_reduce_fusion.31
  9.0 1.2 slice_reduce_fusion.30
  10.2 0.8 copy.27
  11.0 0.1 eq.26
  11.1 0.1 reshape.106
  11.3 0.7 broadcast_multiply_fusion
  12.0 0.6 reduce-window.6
  12.6 0.2 slice_reduce_fusion
  12.8 0.1 fusion.46
  12.9 0.1 copy.32
  13.0 0.1 mul.499
  13.2 1.4 scatter_custom_fusion
  14.6 0.1 broadcast_in_dim.38
  14.7 0.0 collective-permute-done
  14.7 0.0 collective-permute-done.1
  14.7 0.1 maximum_convert_fusion
  14.8 0.0 copy-start.3
  14.8 4.2 %fusion.51 = (f32[256]{0:T(256)S(1)}, f32[256]{0:T(256)S(1)}, f32[256,768]{1,0:T(8,128)S(1)}) fusion(f32[768]{0:T(1024)S(1)} %get-tuple-element.36, f32[286,768]{1,0:T(8,128)S(1)} %maximum_convert_fusion, f32[768]{0:T(1024)S(1)} %get-tuple-element.37, f32[768]{0:T(1024)S(1)} %get-tuple-element.8, f32[768]{0:T(1024)S(1)} %get-tuple-element.9, ...), kind=kLoop, calls=%fused_computation.143 | loop fusion | flops 12582400 | bytes 25263104 | tf_op jit(solution)/shard_map/reduce_sum | solution.py:52
  19.0 0.0 copy-start
  19.0 2.6 %all-reduce.1 = (f32[256]{0:T(256)S(1)}, f32[256]{0:T(256)S(1)}) all-reduce(f32[256]{0:T(256)S(1)} %get-tuple-element.6, f32[256]{0:T(256)S(1)} %get-tuple-element.5), channel_id=1, replica_groups=mesh['sp'=16,'tp'=2] {'tp'}, use_global_device_ids=true, to_apply=%region_3.0 | all-reduce | flops 512 | bytes 4096 | tf_op jit(solution)/shard_map/psum | solution.py:52
  21.6 0.0 copy-done.3
  21.6 0.3 multiply_convert_fusion.2
  22.0 4.0 %all_to_all.29 = bf16[2,128,768]{2,1,0:T(8,128)(2,1)S(1)} all-to-all(bf16[2,128,768]{2,1,0:T(8,128)(2,1)S(1)} %bitcast.50), channel_id=1, replica_groups=mesh['sp'=16,'tp'=2] {'tp'}, dimensions={0} | all-to-all | bytes 786432 | tf_op jit(solution)/shard_map/all_to_all | solution.py:58
  26.0 0.2 copy.26
  26.2 0.0 copy-done
  26.3 0.0 copy-start.2
  26.3 3.9 %multiply_reduce_fusion.1 = (f32[128]{0:T(128)S(1)}, f32[128,2048]{1,0:T(8,128)S(1)}) fusion(bf16[128,1536]{0,1:T(8,128)(2,1)S(1)} %bitcast.45, bf16[1536,2048]{1,0:T(8,128)(2,1)} %param.17, bf16[128,2048]{1,0:T(8,128)(2,1)S(1)} %copy-done), kind=kOutput, calls=%fused_computation.19 | convolution fusion | flops 806879104 | bytes 8258048 | tf_op jit(solution)/shard_map/dot_general | solution.py:59
  30.2 0.0 copy-done.2
  30.2 0.2 multiply_convert_fusion.1
  30.4 3.3 %gather_fusion = bf16[512,2048]{1,0:T(8,128)(2,1)} fusion(bf16[129,2048]{1,0:T(8,128)(2,1)S(1)} %concatenate.7, s32[1024]{0:T(1024)S(1)} %pad_clamp_fusion.1), kind=kCustom, calls=%fused_computation | custom fusion | bytes 4196352 | tf_op jit(solution)/shard_map/jit(_take)/gather | solution.py:79
  33.7 1.8 %broadcast_select_fusion = bf16[32,16,2048]{2,1,0:T(8,128)(2,1)S(1)} fusion(bf16[32,16,2048]{2,1,0:T(8,128)(2,1)} %bitcast.44, pred[32,16]{1,0:T(8,128)(4,1)S(1)} %broadcast_in_dim.38), kind=kLoop, calls=%fused_computation.15 | loop fusion | flops 1048576 | bytes 4194816 | tf_op jit(solution)/shard_map/jit(_take)/select_n | solution.py:79
  35.6 0.0 copy-start.5
  35.6 55.5 %all_to_all.30 = bf16[32,16,2048]{2,1,0:T(8,128)(2,1)S(1)} all-to-all(bf16[32,16,2048]{2,1,0:T(8,128)(2,1)S(1)} %broadcast_select_fusion), channel_id=1, replica_groups=mesh['sp'=16,'tp'=2] {'sp','tp'}, dimensions={0} | all-to-all | bytes 4194304 | tf_op jit(solution)/shard_map/all_to_all | solution.py:81
  91.1 3.7 %fusion.4 = f32[512,1024]{1,0:T(8,128)} fusion(bf16[512,2048]{1,0:T(8,128)(2,1)S(1)} %bitcast.47, bf16[1,2048,1024]{2,1,0:T(8,128)(2,1)S(1)} %copy-done.5), kind=kOutput, calls=%fused_computation.7 | convolution fusion | flops 2147483648 | bytes 8388608 | tf_op jit(solution)/shard_map/dot_general | solution.py:21
  94.8 9.9 %fusion.6 = bf16[512,2048]{1,0:T(8,128)(2,1)} fusion(bf16[1,1024,2048]{2,1,0:T(8,128)(2,1)} %param.23, f32[512,1024]{1,0:T(8,128)} %fusion.4, bf16[512,2048]{1,0:T(8,128)(2,1)S(1)} %bitcast.48, bf16[1,2048,1024]{2,1,0:T(8,128)(2,1)} %param.22), kind=kOutput, calls=%fused_computation.9 | convolution fusion | flops 4299161600 | bytes 14680064 | tf_op jit(solution)/shard_map/dot_general | solution.py:24
  104.7 3.7 %all-to-all-start.2 = ((bf16[32,16,2048]{2,1,0:T(8,128)(2,1)}), bf16[32,16,2048]{2,1,0:T(8,128)(2,1)S(1)}, u32[]{:S(2)}, u32[]{:S(2)}) async-start(bf16[32,16,2048]{2,1,0:T(8,128)(2,1)} %bitcast.46), calls=%async_computation.2 | async-start | bytes 4194304 | tf_op jit(solution)/shard_map/all_to_all | solution.py:84
  108.4 0.1 sub.29
  108.5 0.1 copy.30
  108.6 0.1 copy.31
  108.8 0.1 copy.33
  108.9 48.2 %all-to-all-done.2 = bf16[32,16,2048]{2,1,0:T(8,128)(2,1)S(1)} async-done(((bf16[32,16,2048]{2,1,0:T(8,128)(2,1)}), bf16[32,16,2048]{2,1,0:T(8,128)(2,1)S(1)}, u32[]{:S(2)}, u32[]{:S(2)}) %all-to-all-start.2) | async-done | bytes 2097184 | tf_op jit(solution)/shard_map/all_to_all | solution.py:84
  157.1 2.3 %gather_fusion.1 = bf16[256,2048]{1,0:T(8,128)(2,1)} fusion(bf16[512,2048]{1,0:T(8,128)(2,1)S(1)} %bitcast.43, s32[1024]{0:T(1024)S(1)} %pad_clamp_fusion), kind=kCustom, calls=%fused_computation.1 | custom fusion | bytes 2098176 | tf_op jit(solution)/shard_map/jit(_take)/gather | solution.py:85
  159.5 1.7 %gather.15 = bf16[128,2,2048]{2,1,0:T(2,128)(2,1)S(1)} reshape(bf16[256,2048]{1,0:T(8,128)(2,1)} %gather_fusion.1) | data formatting | bytes 2097152 | tf_op jit(solution)/shard_map/jit(_take)/gather | solution.py:85
  161.2 4.1 %multiply_reduce_fusion = f32[128,2048]{1,0:T(8,128)S(1)} fusion(bf16[128,2,2048]{2,1,0:T(2,128)(2,1)S(1)} %gather.15, pred[128,2]{1,0:T(8,128)(4,1)S(1)} %copy.31, f32[128,2]{1,0:T(8,128)S(1)} %copy.33), kind=kLoop, calls=%fused_computation.13 | loop fusion | flops 1835008 | bytes 2098432 | tf_op jit(solution)/shard_map/reduce_sum | solution.py:87
  165.3 0.9 add_convert_fusion
  (20 shorter events, 0.2 us)
Async XLA Ops:
  1.4 13.4 %collective-permute-start = (bf16[15,768]{1,0:T(8,128)(2,1)S(1)}, bf16[15,768]{1,0:T(8,128)(2,1)S(1)}, u32[]{:S(2)}, u32[]{:S(2)}) collective-permute-start(bf16[15,768]{1,0:T(8,128)(2,1)S(1)} %get-tuple-element.41), channel_id=1, source_target_pairs={{0,2},{2,4},{4,6},{6,8},{8,10},{10,12},{12,14},{14,16},{16,18},{18... | collective-permute-start | bytes 69128 | tf_op jit(solution)/shard_map/ppermute | solution.py:12
  6.2 8.5 %collective-permute-start.1 = (bf16[15,768]{1,0:T(8,128)(2,1)S(1)}, bf16[15,768]{1,0:T(8,128)(2,1)S(1)}, u32[]{:S(2)}, u32[]{:S(2)}) collective-permute-start(bf16[15,768]{1,0:T(8,128)(2,1)S(1)} %get-tuple-element.42), channel_id=1, source_target_pairs={{2,0},{4,2},{6,4},{8,6},{10,8},{12,10},{14,12},{16,14},{18,16},{20... | collective-permute-start | bytes 69128 | tf_op jit(solution)/shard_map/ppermute | solution.py:15
  14.8 6.8 %copy-start.3 = (f32[768]{0:T(1024)S(1)}, f32[768]{0:T(1024)}, u32[]{:S(2)}) copy-start(f32[768]{0:T(1024)} %param.16) | copy-start | bytes 9220
  19.0 7.2 %copy-start = (bf16[128,2048]{1,0:T(8,128)(2,1)S(1)}, bf16[128,2048]{1,0:T(8,128)(2,1)}, u32[]{:S(2)}) copy-start(bf16[128,2048]{1,0:T(8,128)(2,1)} %param.12) | copy-start | bytes 1572868
  26.3 3.9 %copy-start.2 = (f32[2048]{0:T(1024)S(1)}, f32[2048]{0:T(1024)}, u32[]{:S(2)}) copy-start(f32[2048]{0:T(1024)} %param.18) | copy-start | bytes 24580
  35.6 55.5 %copy-start.5 = (bf16[1,2048,1024]{2,1,0:T(8,128)(2,1)S(1)}, bf16[1,2048,1024]{2,1,0:T(8,128)(2,1)}, u32[]{:S(2)}) copy-start(bf16[1,2048,1024]{2,1,0:T(8,128)(2,1)} %param.21) | copy-start | bytes 12582916
  104.7 3.9 %copy-start.1 = (s32[128,2]{0,1:T(2,128)S(1)}, s32[128,2]{0,1:T(2,128)}, u32[]{:S(2)}) copy-start(s32[128,2]{0,1:T(2,128)} %param.19) | copy-start | bytes 3076
  104.7 4.1 %copy-start.4 = (f32[128,2]{0,1:T(2,128)S(1)}, f32[128,2]{0,1:T(2,128)}, u32[]{:S(2)}) copy-start(f32[128,2]{0,1:T(2,128)} %param.20) | copy-start | bytes 3076
  104.7 52.4 %all-to-all-start.2 = ((bf16[32,16,2048]{2,1,0:T(8,128)(2,1)}), bf16[32,16,2048]{2,1,0:T(8,128)(2,1)S(1)}, u32[]{:S(2)}, u32[]{:S(2)}) async-start(bf16[32,16,2048]{2,1,0:T(8,128)(2,1)} %bitcast.46), calls=%async_computation.2 | async-start | bytes 4194304 | tf_op jit(solution)/shard_map/all_to_all | solution.py:84
where the time goes:
time: 167 us; the launch traced here: 166 us
  blocking collectives  62.1 us (37%)
  waiting for transfers between devices  48.2 us (29%)
  matrix products  17.5 us (10%)
  other arithmetic  14.4 us (9%)
  local copies, waits for them, and re-layouts  13.8 us (8%)
  starting transfers between devices  9.84 us (6%)
    all_to_all x1, blocking collectives, per_device(): lax.all_to_all(outgoing, ('sp', 'tp'), split_axis=0, concat_axis=0, tiled...  55.5 us
    all_to_all x1, waiting for transfers between devices, per_device(): lax.all_to_all(done, ('sp', 'tp'), split_axis=0, concat_axis=0, tiled=True)  48.2 us
    dot_general x1, matrix products, expert_apply(): jnp.dot(hidden, down_w, preferred_element_type=jnp.float32)  9.89 us
    ppermute x1, starting transfers between devices, padded_2(): lax.ppermute(lax.slice_in_dim(block, block.shape[dim] - width, None, axis...  4.87 us
    reduce_sum x1, other arithmetic, per_device(): sums = lax.psum((jnp.sum(conv, axis=1), jnp.sum(conv * conv, axis=1)), 'tp')  4.16 us
    gather x2, local copies, waits for them, and re-layouts, per_device(): jnp.take(returned.reshape(experts_all * cap, model_width), dest, axis=0)  4.09 us
    reduce_sum x1, other arithmetic, per_device(): total = wide + jnp.sum(picked * expert_mix[:, :, None], axis=1)  4.07 us
    all_to_all x1, blocking collectives, per_device(): lax.all_to_all(mixed, 'tp', split_axis=0, concat_axis=1, tiled=True)  4.05 us
  transfers between devices with their start and end apart: 3, of which 1 were waited for; matrix products, arithmetic and copies ran while one was open for 5% of the time, Pallas kernels for 0%

commit v1 on v0

v1 whole, which is shorter than its diff:
```python
import functools

import jax
import jax.numpy as jnp
from jax import lax
from jax.experimental import pallas as pl
from jax.experimental.pallas import tpu as pltpu
from jax.sharding import PartitionSpec as P

BOTH = ("sp", "tp")
LANES = 128
HALO = 16


def glu_kernel(core_ref, value_ref, gate_ref, mine_ref, give_ref, near_ref, far_ref, glu_ref):
    core = core_ref[0]
    value = value_ref[...].astype(jnp.float32)
    gate = gate_ref[...].astype(jnp.float32)
    glu_ref[...] = (value * jax.nn.sigmoid(gate)).astype(jnp.bfloat16)
    inner = mine_ref.shape[0]
    rows = glu_ref.shape[0]
    step = rows - inner
    last = rows - HALO
    mine_ref[...] = glu_ref[pl.ds(pl.multiple_of(core * step, HALO), inner), :]
    give_ref[...] = glu_ref[pl.ds(pl.multiple_of((1 - core) * step, HALO), inner), :]
    near_ref[...] = glu_ref[pl.ds(pl.multiple_of((1 - core) * last, HALO), HALO), :]
    far_ref[...] = glu_ref[pl.ds(pl.multiple_of(core * last, HALO), HALO), :]


def module_kernel(
    cap,
    experts,
    core_ref,
    mine_ref,
    other_ref,
    near_ref,
    far_ref,
    taps_ref,
    taps_other_ref,
    out_weight_ref,
    resid_ref,
    ffn_gain_ref,
    ids_ref,
    outgoing_ref,
    stream_ref,
    dest_ref,
    window_ref,
    conv_ref,
):
    core = core_ref[0]
    inner, half = mine_ref.shape
    rows = resid_ref.shape[0]
    taps = taps_ref.shape[0] - 1
    blocks = half // LANES
    inner_at = pl.multiple_of((1 - core) * HALO, HALO)
    outer_at = pl.multiple_of(core * inner, HALO)
    for source, outer, base in ((mine_ref, near_ref, 0), (other_ref, far_ref, blocks)):
        for b in range(blocks):
            lanes = slice(b * LANES, (b + 1) * LANES)
            window_ref[base + b, pl.ds(inner_at, inner), :] = source[:, lanes].astype(jnp.float32)
            window_ref[base + b, pl.ds(outer_at, HALO), :] = outer[:, lanes].astype(jnp.float32)
    first = HALO - taps // 2
    total = jnp.zeros((rows, LANES), jnp.float32)
    square = jnp.zeros((rows, LANES), jnp.float32)
    for b in range(2 * blocks):
        tap_ref = taps_ref if b < blocks else taps_other_ref
        lanes = slice((b % blocks) * LANES, (b % blocks + 1) * LANES)
        conv = jnp.zeros((rows, LANES), jnp.float32)
        for tap in range(taps):
            conv = conv + window_ref[b, first + tap : first + tap + rows, :] * tap_ref[tap : tap + 1, lanes]
        conv_ref[b] = conv
        total = total + conv
        square = square + conv * conv
    width = 2 * half
    mean = jnp.sum(total, axis=1, keepdims=True) / width
    var = jnp.sum(square, axis=1, keepdims=True) / width - mean * mean
    scale = lax.rsqrt(var + 1e-05)
    proj = None
    for side, tap_ref in ((0, taps_ref), (1, taps_other_ref)):
        parts = []
        for b in range(blocks):
            lanes = slice(b * LANES, (b + 1) * LANES)
            v = (conv_ref[side * blocks + b] - mean) * scale * tap_ref[taps : taps + 1, lanes]
            parts.append(jax.nn.silu(v).astype(jnp.bfloat16))
        mixed = jnp.concatenate(parts, axis=1)
        where = (core + side * (1 - 2 * core)) * half
        weight = out_weight_ref[pl.ds(pl.multiple_of(where, LANES), half), :]
        part = jnp.dot(mixed, weight, preferred_element_type=jnp.float32)
        proj = part if proj is None else proj + part
    stream = (resid_ref[...].astype(jnp.float32) + proj).astype(jnp.bfloat16)
    stream_ref[...] = stream
    wide = stream.astype(jnp.float32)
    power = jnp.mean(wide * wide, axis=1, keepdims=True)
    normed = (wide * lax.rsqrt(power + 1e-06) * ffn_gain_ref[...]).astype(jnp.bfloat16)
    ids = ids_ref[...]
    lane = lax.broadcasted_iota(jnp.int32, (rows, experts), 1)
    named = [ids[:, k : k + 1] == lane for k in range(ids.shape[1])]
    member = sum(n.astype(jnp.float32) for n in named).astype(jnp.bfloat16)
    down = lax.broadcasted_iota(jnp.int32, (rows, rows), 0)
    across = lax.broadcasted_iota(jnp.int32, (rows, rows), 1)
    before = (across < down).astype(jnp.float32).astype(jnp.bfloat16)
    rank = jnp.dot(before, member, preferred_element_type=jnp.float32)
    slot = lax.broadcasted_iota(jnp.int32, (rows, experts * cap), 1)
    place = jnp.zeros((rows, experts * cap), jnp.float32)
    dests = []
    for k, n in enumerate(named):
        own = jnp.sum(jnp.where(n, rank, 0.0), axis=1, keepdims=True).astype(jnp.int32)
        dest = ids[:, k : k + 1] * cap + own
        dests.append(dest)
        place = jnp.where(slot == dest, 1.0, place)
    dest_ref[...] = jnp.concatenate(dests, axis=1)
    outgoing_ref[...] = lax.dot_general(
        place.astype(jnp.bfloat16),
        normed,
        (((0,), (0,)), ((), ())),
        preferred_element_type=jnp.float32,
    ).astype(jnp.bfloat16)


def expert_kernel(rows_ref, gate_ref, up_ref, down_ref, out_ref, acc_ref):
    step = pl.program_id(0)
    rows = rows_ref[...]
    gate = jnp.dot(rows, gate_ref[...], preferred_element_type=jnp.float32)
    up = jnp.dot(rows, up_ref[...], preferred_element_type=jnp.float32)
    hidden = (jax.nn.silu(gate) * up).astype(jnp.bfloat16)
    part = jnp.dot(hidden, down_ref[...], preferred_element_type=jnp.float32)

    @pl.when(step == 0)
    def _():
        acc_ref[...] = part

    @pl.when(step > 0)
    def _():
        acc_ref[...] += part

    @pl.when(step == pl.num_programs(0) - 1)
    def _():
        out_ref[...] = acc_ref[...].astype(jnp.bfloat16)


def combine_kernel(returned_ref, dest_ref, mix_ref, stream_ref, out_ref):
    rows = stream_ref.shape[0]
    slots = returned_ref.shape[0]
    slot = lax.broadcasted_iota(jnp.int32, (rows, slots), 1)
    total = None
    for k in range(dest_ref.shape[1]):
        pick = (slot == dest_ref[:, k : k + 1]).astype(jnp.float32).astype(jnp.bfloat16)
        got = jnp.dot(pick, returned_ref[...], preferred_element_type=jnp.float32)
        part = got * mix_ref[:, k : k + 1]
        total = part if total is None else total + part
    out_ref[...] = (stream_ref[...].astype(jnp.float32) + total).astype(jnp.bfloat16)


def vmem(count):
    return [pl.BlockSpec(memory_space=pltpu.VMEM)] * count


def params(mib):
    return pltpu.CompilerParams(vmem_limit_bytes=mib << 20)


def per_device(
    resid,
    value_in,
    gate_in,
    conv_weight,
    norm_gain,
    out_weight,
    ffn_gain,
    expert_ids,
    expert_mix,
    w_gate,
    w_up,
    w_down,
):
    bf16 = jnp.bfloat16
    sp_count = lax.axis_size("sp")
    tp_count = lax.axis_size("tp")
    experts = sp_count * tp_count
    rows_here, model_width = resid.shape
    topk = expert_ids.shape[1]
    cap = max(2, (2 * topk * rows_here + experts - 1) // experts)
    slots = experts * cap
    core = lax.axis_index("tp").astype(jnp.int32).reshape(1)
    length, half = value_in.shape
    inner = rows_here + HALO

    swap = [(s * 2 + c, s * 2 + 1 - c) for s in range(sp_count) for c in range(2)]
    near = []
    far = []
    for s in range(sp_count):
        if s + 1 < sp_count:
            near.append((s * 2, (s + 1) * 2))
            far.append((s * 2 + 1, (s + 1) * 2))
        if s > 0:
            near.append((s * 2 + 1, (s - 1) * 2 + 1))
            far.append((s * 2, (s - 1) * 2 + 1))

    taps = jnp.concatenate([conv_weight, norm_gain[None, :]], axis=0)
    taps_other = lax.ppermute(taps, BOTH, swap)
    mine, give, near_rows, far_rows = pl.pallas_call(
        glu_kernel,
        out_shape=(
            jax.ShapeDtypeStruct((inner, half), bf16),
            jax.ShapeDtypeStruct((inner, half), bf16),
            jax.ShapeDtypeStruct((HALO, half), bf16),
            jax.ShapeDtypeStruct((HALO, half), bf16),
        ),
        in_specs=[pl.BlockSpec(memory_space=pltpu.SMEM)] + vmem(2),
        out_specs=vmem(4),
        scratch_shapes=[pltpu.VMEM((length, half), bf16)],
        compiler_params=params(8),
        name="glu",
    )(core, value_in, gate_in)
    near_rows = lax.ppermute(near_rows, BOTH, near)
    far_rows = lax.ppermute(far_rows, BOTH, far)
    other = lax.ppermute(give, BOTH, swap)

    outgoing, stream, dest = pl.pallas_call(
        functools.partial(module_kernel, cap, experts),
        out_shape=(
            jax.ShapeDtypeStruct((slots, model_width), bf16),
            jax.ShapeDtypeStruct((rows_here, model_width), bf16),
            jax.ShapeDtypeStruct((rows_here, topk), jnp.int32),
        ),
        in_specs=[pl.BlockSpec(memory_space=pltpu.SMEM)] + vmem(10),
        out_specs=vmem(3),
        scratch_shapes=[
            pltpu.VMEM((2 * half // LANES, inner + HALO, LANES), jnp.float32),
            pltpu.VMEM((2 * half // LANES, rows_here, LANES), jnp.float32),
        ],
        compiler_params=params(24),
        name="module",
    )(
        core,
        mine,
        other,
        near_rows,
        far_rows,
        taps,
        taps_other,
        out_weight,
        resid,
        ffn_gain.reshape(1, -1),
        expert_ids,
    )

    arrived = lax.all_to_all(
        outgoing.reshape(experts, cap, model_width), BOTH, split_axis=0, concat_axis=0, tiled=True
    ).reshape(slots, model_width)

    hidden_width = w_gate.shape[2]
    chunk = min(256, hidden_width)
    done = pl.pallas_call(
        expert_kernel,
        out_shape=jax.ShapeDtypeStruct((slots, model_width), bf16),
        grid=(hidden_width // chunk,),
        in_specs=[
            pl.BlockSpec((slots, model_width), lambda f: (0, 0)),
            pl.BlockSpec((None, model_width, chunk), lambda f: (0, 0, f)),
            pl.BlockSpec((None, model_width, chunk), lambda f: (0, 0, f)),
            pl.BlockSpec((None, chunk, model_width), lambda f: (0, f, 0)),
        ],
        out_specs=pl.BlockSpec((slots, model_width), lambda f: (0, 0)),
        scratch_shapes=[pltpu.VMEM((slots, model_width), jnp.float32)],
        compiler_params=params(32),
        name="experts",
    )(arrived, w_gate, w_up, w_down)

    returned = lax.all_to_all(
        done.reshape(experts, cap, model_width), BOTH, split_axis=0, concat_axis=0, tiled=True
    ).reshape(slots, model_width)

    return pl.pallas_call(
        combine_kernel,
        out_shape=jax.ShapeDtypeStruct((rows_here, model_width), bf16),
        in_specs=vmem(4),
        out_specs=pl.BlockSpec(memory_space=pltpu.VMEM),
        compiler_params=params(16),
        name="combine",
    )(returned, dest, expert_mix, stream)


def solution(mesh):
    return jax.shard_map(
        per_device,
        mesh=mesh,
        in_specs=(
            P(("sp", "tp"), None),
            P("sp", "tp"),
            P("sp", "tp"),
            P(None, "tp"),
            P("tp"),
            P(),
            P(),
            P(("sp", "tp"), None),
            P(("sp", "tp"), None),
            P(("sp", "tp"), None, None),
            P(("sp", "tp"), None, None),
            P(("sp", "tp"), None, None),
        ),
        out_specs=P(("sp", "tp"), None),
        check_vma=False,
    )
```

time: 167 us -> 146 us (0.87)
  matrix products: 17.5 us -> 0 us
  Pallas kernels: 0 us -> 16.5 us
  other arithmetic: 14.4 us -> 0.9 us
  blocking collectives: 62.1 us -> 58 us
  local copies, waits for them, and re-layouts: 13.8 us -> 11.6 us
    dot_general x3 -> x0, matrix products: 17.5 us -> none  [the longest x1 9.89 us: expert_apply(): jnp.dot(hidden, down_w, preferred_element_type=jnp.float32)]
    pallas_call x0 -> x4, Pallas kernels: none -> 16.5 us  [the longest x1 10 us: per_device(): pl.pallas_call(expert_kernel, out_shape=jax.ShapeDtypeStruct((slots, mode...]
    unnamed x14 -> x22, local copies, waits for them, and re-layouts: 0.93 us -> 10.9 us
    reduce_sum x3 -> x0, other arithmetic: 8.33 us -> none  [the longest x1 4.16 us: per_device(): sums = lax.psum((jnp.sum(conv, axis=1), jnp.sum(conv * conv, axis=1)), 'tp')]
    gather x3 -> x0, local copies, waits for them, and re-layouts: 7.44 us -> none  [the longest x2 4.09 us: per_device(): jnp.take(returned.reshape(experts_all * cap, model_width), dest, axis=0)]
    convert_element_type x6 -> x0, other arithmetic: 2.87 us -> none  [the longest x1 1.34 us: per_device(): (value_in.astype(jnp.float32) * jax.nn.sigmoid(gate_in.astype(jnp.float32...]
    slice x4 -> x0, local copies, waits for them, and re-layouts: 2.86 us -> none  [the longest x2 2.67 us: per_device(): conv = conv + padded[tap:tap + length] * conv_weight[tap]]
    psum x1 -> x0, blocking collectives: 2.6 us -> none  [per_device(): sums = lax.psum((jnp.sum(conv, axis=1), jnp.sum(conv * conv, axis=1)), 'tp')]
  transfers between devices with their start and end apart: 3 -> 5, of which waited for: 1 -> 1; matrix products, arithmetic and copies ran while one was open for 5% -> 2% of each run, Pallas kernels for 0% -> 0%
where the time goes in v1:
time: 146 us
  blocking collectives  58 us (40%)
  waiting for transfers between devices  48.7 us (33%)
  Pallas kernels  16.5 us (11%)
  local copies, waits for them, and re-layouts  11.6 us (8%)
  starting transfers between devices  9.82 us (7%)
    all_to_all x1, blocking collectives, per_device(): lax.all_to_all(outgoing.reshape(experts, cap, model_width), BOTH, split_a...  58 us
    all_to_all x1, waiting for transfers between devices, per_device(): lax.all_to_all(done.reshape(experts, cap, model_width), BOTH, split_axis=...  48.6 us
    unnamed x22, local copies, waits for them, and re-layouts  10.9 us
    pallas_call x1, Pallas kernels, per_device(): pl.pallas_call(expert_kernel, out_shape=jax.ShapeDtypeStruct((slots, mode...  10 us
    ppermute x1, starting transfers between devices, per_device(): near_rows = lax.ppermute(near_rows, BOTH, near)  4.86 us
    pallas_call x1, Pallas kernels, per_device(): pl.pallas_call(functools.partial(module_kernel, cap, experts), out_shape=...  4.61 us
    all_to_all x1, starting transfers between devices, per_device(): lax.all_to_all(done.reshape(experts, cap, model_width), BOTH, split_axis=...  3.66 us
  transfers between devices with their start and end apart: 5, of which 1 were waited for; matrix products, arithmetic and copies ran while one was open for 2% of the time, Pallas kernels for 0%

profile of v1, /device:TPU:0, one launch (start us, length us, event | category | flops | bytes accessed | tf_op | source)
XLA Modules:
  0.0 145.6 jit_solution(10353179792697452781)
XLA Ops:
  0.0 0.0 copy-start.6
  0.0 1.0 copy-done.6
  1.0 0.0 copy-start.7
  1.0 1.0 copy-done.7
  2.0 0.2 glu.1
  2.2 0.6 collective-permute-start
  2.8 0.7 broadcast_in_dim.3
  3.5 0.9 pad_maximum_fusion.taps_ref
  4.4 0.1 collective-permute-start.3
  4.5 4.9 %collective-permute-start.1 = (bf16[16,768]{1,0:T(8,128)(2,1)S(1)}, bf16[16,768]{1,0:T(8,128)(2,1)S(1)}, u32[]{:S(2)}, u32[]{:S(2)}) collective-permute-start(bf16[16,768]{1,0:T(8,128)(2,1)S(1)} %get-tuple-element.14), channel_id=1, source_target_pairs={{0,2},{2,4},{3,1},{4,6},{5,3},{6,8},{7,5},{8,10},{9,7},{10,12},{11... | collective-permute-start | bytes 73736 | tf_op jit(solution)/shard_map/ppermute | solution.py:215
  9.3 0.7 collective-permute-start.2
  10.0 0.8 copy.13.ids_ref
  10.8 0.0 collective-permute-done.1.near_ref
  10.8 0.0 collective-permute-done.2.far_ref
  10.8 0.0 collective-permute-done.3.taps_other_ref
  10.8 0.0 collective-permute-done.other_ref
  10.9 0.0 copy-start.1
  10.9 2.8 %copy-done.1 = bf16[1536,2048]{1,0:T(8,128)(2,1)S(1)} copy-done((bf16[1536,2048]{1,0:T(8,128)(2,1)S(1)}, bf16[1536,2048]{1,0:T(8,128)(2,1)}, u32[]{:S(2)}) %copy-start.1) | copy-done | bytes 6291480
  13.6 0.0 copy-start.5
  13.6 1.0 copy-done.5
  14.7 0.0 copy-start.8
  14.7 0.7 copy-done.8
  15.4 0.0 copy-start.2
  15.4 0.0 copy-start.3
  15.4 4.6 %module.1 = (bf16[512,2048]{1,0:T(8,128)(2,1)S(1)}, bf16[128,2048]{1,0:T(8,128)(2,1)S(1)}, s32[128,2]{1,0:T(8,128)S(1)}) custom-call(s32[1]{0:T(128)} %bitcast.core_ref, bf16[144,768]{1,0:T(8,128)(2,1)S(1)} %get-tuple-element.12.mine_ref, bf16[144,768]{1,0:T(8,128)(2,1)S(1)} %collective-permute-done.other_ref, ...), custom_call_target="tpu_custom_call" | custom-call | tf_op jit(solution)/shard_map/module/pallas_call | solution.py:219
  20.0 58.0 %all_to_all.10 = bf16[32,16,2048]{2,1,0:T(8,128)(2,1)S(1)} all-to-all(bf16[32,16,2048]{2,1,0:T(8,128)(2,1)S(1)} %bitcast.9), channel_id=1, replica_groups=mesh['sp'=16,'tp'=2] {'sp','tp'}, dimensions={0} | all-to-all | bytes 4194304 | tf_op jit(solution)/shard_map/all_to_all | solution.py:248
  78.0 0.0 copy-done.2
  78.0 0.0 copy-done.3
  78.0 0.0 copy-start.4
  78.0 2.2 %copy-done.4 = bf16[1,1024,2048]{2,1,0:T(8,128)(2,1)S(1)} copy-done((bf16[1,1024,2048]{2,1,0:T(8,128)(2,1)S(1)}, bf16[1,1024,2048]{2,1,0:T(8,128)(2,1)}, u32[]{:S(2)}) %copy-start.4) | copy-done | bytes 4194328
  80.2 10.0 %experts.1 = bf16[512,2048]{1,0:T(8,128)(2,1)S(1)} custom-call(bf16[512,2048]{1,0:T(8,128)(2,1)S(1)} %bitcast.8, bf16[1,2048,1024]{2,1,0:T(8,128)(2,1)S(1)} %copy-done.2, bf16[1,2048,1024]{2,1,0:T(8,128)(2,1)S(1)} %copy-done.3, bf16[1,1024,2048]{2,1,0:T(8,128)(2,1)S(1)} %copy-done.4), custom_call_target="tpu_custom_call" | custom-call | tf_op jit(solution)/shard_map/experts/pallas_call | solution.py:254
  90.2 0.0 copy-start
  90.3 1.3 copy-done
  91.6 0.0 copy-start.9
  91.6 3.7 %all-to-all-start.1 = ((bf16[32,16,2048]{2,1,0:T(8,128)(2,1)}), bf16[32,16,2048]{2,1,0:T(8,128)(2,1)S(1)}, u32[]{:S(2)}, u32[]{:S(2)}) async-start(bf16[32,16,2048]{2,1,0:T(8,128)(2,1)} %bitcast.7), calls=%async_computation.1 | async-start | bytes 4194304 | tf_op jit(solution)/shard_map/all_to_all | solution.py:270
  95.3 0.0 copy-done.9
  95.3 0.1 copy.14.mix_ref
  95.4 48.6 %all-to-all-done.1 = bf16[32,16,2048]{2,1,0:T(8,128)(2,1)S(1)} async-done(((bf16[32,16,2048]{2,1,0:T(8,128)(2,1)}), bf16[32,16,2048]{2,1,0:T(8,128)(2,1)S(1)}, u32[]{:S(2)}, u32[]{:S(2)}) %all-to-all-start.1) | async-done | bytes 2097184 | tf_op jit(solution)/shard_map/all_to_all | solution.py:270
  144.0 1.6 %combine.1 = bf16[128,2048]{1,0:T(8,128)(2,1)} custom-call(bf16[512,2048]{1,0:T(8,128)(2,1)S(1)} %bitcast.6, s32[128,2]{1,0:T(8,128)S(1)} %get-tuple-element.17.dest_ref, f32[128,2]{1,0:T(8,128)S(1)} %copy.14.mix_ref, bf16[128,2048]{1,0:T(8,128)(2,1)S(1)} %get-tuple-element.18.stream_ref), custom_call_target="tpu_custom_call" | custom-call | tf_op jit(solution)/shard_map/combine/pallas_call | solution.py:274
Async XLA Ops:
  0.0 1.0 copy-start.6
  1.0 1.0 copy-start.7
  2.2 8.6 %collective-permute-start = (bf16[144,768]{1,0:T(8,128)(2,1)S(1)}, bf16[144,768]{1,0:T(8,128)(2,1)S(1)}, u32[]{:S(2)}, u32[]{:S(2)}) collective-permute-start(bf16[144,768]{1,0:T(8,128)(2,1)S(1)} %get-tuple-element.13), channel_id=1, source_target_pairs={{0,1},{1,0},{2,3},{3,2},{4,5},{5,4},{6,7},{7,6},{8,9},{9,8},{10,11... | collective-permute-start | bytes 663560 | tf_op jit(solution)/shard_map/ppermute | solution.py:217
  4.4 6.5 %collective-permute-start.3 = (f32[32,768]{1,0:T(8,128)S(1)}, f32[32,768]{1,0:T(8,128)S(1)}, u32[]{:S(2)}, u32[]{:S(2)}) collective-permute-start(f32[32,768]{1,0:T(8,128)S(1)} %pad_maximum_fusion.taps_ref), channel_id=1, source_target_pairs={{0,1},{1,0},{2,3},{3,2},{4,5},{5,4},{6,7},{7,6},{8,9},{9,8},{10,11... | collective-permute-start | bytes 294920 | tf_op jit(solution)/shard_map/ppermute | solution.py:200
  4.5 6.4 %collective-permute-start.1 = (bf16[16,768]{1,0:T(8,128)(2,1)S(1)}, bf16[16,768]{1,0:T(8,128)(2,1)S(1)}, u32[]{:S(2)}, u32[]{:S(2)}) collective-permute-start(bf16[16,768]{1,0:T(8,128)(2,1)S(1)} %get-tuple-element.14), channel_id=1, source_target_pairs={{0,2},{2,4},{3,1},{4,6},{5,3},{6,8},{7,5},{8,10},{9,7},{10,12},{11... | collective-permute-start | bytes 73736 | tf_op jit(solution)/shard_map/ppermute | solution.py:215
  9.3 1.5 %collective-permute-start.2 = (bf16[16,768]{1,0:T(8,128)(2,1)S(1)}, bf16[16,768]{1,0:T(8,128)(2,1)S(1)}, u32[]{:S(2)}, u32[]{:S(2)}) collective-permute-start(bf16[16,768]{1,0:T(8,128)(2,1)S(1)} %get-tuple-element.15), channel_id=1, source_target_pairs={{1,2},{3,4},{2,1},{5,6},{4,3},{7,8},{6,5},{9,10},{8,7},{11,12},{10... | collective-permute-start | bytes 73736 | tf_op jit(solution)/shard_map/ppermute | solution.py:216
  10.9 2.8 %copy-start.1 = (bf16[1536,2048]{1,0:T(8,128)(2,1)S(1)}, bf16[1536,2048]{1,0:T(8,128)(2,1)}, u32[]{:S(2)}) copy-start(bf16[1536,2048]{1,0:T(8,128)(2,1)} %out_weight_ref.1) | copy-start | bytes 18874372
  13.6 1.0 copy-start.5
  14.7 0.7 copy-start.8
  15.4 62.6 %copy-start.2 = (bf16[1,2048,1024]{2,1,0:T(8,128)(2,1)S(1)}, bf16[1,2048,1024]{2,1,0:T(8,128)(2,1)}, u32[]{:S(2)}) copy-start(bf16[1,2048,1024]{2,1,0:T(8,128)(2,1)} %gate_ref.3) | copy-start | bytes 12582916
  15.4 62.6 %copy-start.3 = (bf16[1,2048,1024]{2,1,0:T(8,128)(2,1)S(1)}, bf16[1,2048,1024]{2,1,0:T(8,128)(2,1)}, u32[]{:S(2)}) copy-start(bf16[1,2048,1024]{2,1,0:T(8,128)(2,1)} %up_ref.1) | copy-start | bytes 12582916
  78.0 2.2 %copy-start.4 = (bf16[1,1024,2048]{2,1,0:T(8,128)(2,1)S(1)}, bf16[1,1024,2048]{2,1,0:T(8,128)(2,1)}, u32[]{:S(2)}) copy-start(bf16[1,1024,2048]{2,1,0:T(8,128)(2,1)} %down_ref.1) | copy-start | bytes 12582916
  90.2 1.3 copy-start
  91.6 3.7 %copy-start.9 = (f32[128,2]{0,1:T(2,128)S(1)}, f32[128,2]{0,1:T(2,128)}, u32[]{:S(2)}) copy-start(f32[128,2]{0,1:T(2,128)} %param.20) | copy-start | bytes 3076
  91.6 52.4 %all-to-all-start.1 = ((bf16[32,16,2048]{2,1,0:T(8,128)(2,1)}), bf16[32,16,2048]{2,1,0:T(8,128)(2,1)S(1)}, u32[]{:S(2)}, u32[]{:S(2)}) async-start(bf16[32,16,2048]{2,1,0:T(8,128)(2,1)} %bitcast.7), calls=%async_computation.1 | async-start | bytes 4194304 | tf_op jit(solution)/shard_map/all_to_all | solution.py:270

commit v2 on v1

v2 whole, which is shorter than its diff:
```python
import functools

import jax
import jax.numpy as jnp
from jax import lax
from jax.experimental import pallas as pl
from jax.experimental.pallas import tpu as pltpu
from jax.sharding import PartitionSpec as P

BOTH = ("sp", "tp")
LANES = 128
HALO = 16


def glu_kernel(
    core_ref,
    value_hbm,
    gate_hbm,
    weight_hbm,
    gain_hbm,
    mine_ref,
    give_ref,
    near_ref,
    far_ref,
    taps_ref,
    value_ref,
    gate_ref,
    glu_ref,
    weight_ref,
    gain_ref,
    sems,
):
    core = core_ref[0]
    copies = [
        pltpu.make_async_copy(source, target, sems.at[n])
        for n, (source, target) in enumerate(
            (
                (value_hbm, value_ref),
                (gate_hbm, gate_ref),
                (weight_hbm, weight_ref),
                (gain_hbm, gain_ref),
            )
        )
    ]
    for copy in copies:
        copy.start()
    copies[0].wait()
    copies[1].wait()
    value = value_ref[...].astype(jnp.float32)
    gate = gate_ref[...].astype(jnp.float32)
    glu_ref[...] = (value * jax.nn.sigmoid(gate)).astype(jnp.bfloat16)
    inner = mine_ref.shape[0]
    rows = glu_ref.shape[0]
    step = rows - inner
    last = rows - HALO
    mine_ref[...] = glu_ref[pl.ds(pl.multiple_of(core * step, HALO), inner), :]
    give_ref[...] = glu_ref[pl.ds(pl.multiple_of((1 - core) * step, HALO), inner), :]
    near_ref[...] = glu_ref[pl.ds(pl.multiple_of((1 - core) * last, HALO), HALO), :]
    far_ref[...] = glu_ref[pl.ds(pl.multiple_of(core * last, HALO), HALO), :]
    copies[2].wait()
    copies[3].wait()
    taps = weight_ref.shape[0]
    taps_ref[0:taps, :] = weight_ref[...]
    taps_ref[taps : taps + 1, :] = gain_ref[...].reshape(1, -1)


def places(ids, cap, experts):
    topk, rows = ids.shape
    lane = lax.broadcasted_iota(jnp.int32, (experts, rows), 0)
    named = [ids[k : k + 1, :] == lane for k in range(topk)]
    member = sum(n.astype(jnp.float32) for n in named).astype(jnp.bfloat16)
    down = lax.broadcasted_iota(jnp.int32, (rows, rows), 0)
    across = lax.broadcasted_iota(jnp.int32, (rows, rows), 1)
    before = (down < across).astype(jnp.float32).astype(jnp.bfloat16)
    rank = jnp.dot(member, before, preferred_element_type=jnp.float32)
    slot = lax.broadcasted_iota(jnp.int32, (experts * cap, rows), 0)
    found = []
    for k, n in enumerate(named):
        own = jnp.sum(jnp.where(n, rank, 0.0), axis=0, keepdims=True).astype(jnp.int32)
        found.append(slot == ids[k : k + 1, :] * cap + own)
    return found


def module_kernel(
    cap,
    experts,
    core_ref,
    mine_ref,
    other_ref,
    near_ref,
    far_ref,
    taps_ref,
    taps_other_ref,
    ids_ref,
    out_weight_hbm,
    resid_hbm,
    ffn_gain_hbm,
    outgoing_ref,
    stream_ref,
    window_ref,
    conv_ref,
    out_weight_ref,
    resid_ref,
    ffn_gain_ref,
    sems,
):
    core = core_ref[0]
    inner, half = mine_ref.shape
    copies = []
    for side in range(2):
        where = pl.multiple_of((core + side * (1 - 2 * core)) * half, LANES)
        copies.append(
            pltpu.make_async_copy(
                out_weight_hbm.at[pl.ds(where, half), :], out_weight_ref.at[side], sems.at[side]
            )
        )
    copies.append(pltpu.make_async_copy(resid_hbm, resid_ref, sems.at[2]))
    copies.append(pltpu.make_async_copy(ffn_gain_hbm, ffn_gain_ref, sems.at[3]))
    for copy in copies:
        copy.start()
    rows = resid_ref.shape[0]
    taps = taps_ref.shape[0] - 1
    blocks = half // LANES
    inner_at = pl.multiple_of((1 - core) * HALO, HALO)
    outer_at = pl.multiple_of(core * inner, HALO)
    for source, outer, base in ((mine_ref, near_ref, 0), (other_ref, far_ref, blocks)):
        for b in range(blocks):
            lanes = slice(b * LANES, (b + 1) * LANES)
            window_ref[base + b, pl.ds(inner_at, inner), :] = source[:, lanes].astype(jnp.float32)
            window_ref[base + b, pl.ds(outer_at, HALO), :] = outer[:, lanes].astype(jnp.float32)
    first = HALO - taps // 2
    total = jnp.zeros((rows, LANES), jnp.float32)
    square = jnp.zeros((rows, LANES), jnp.float32)
    for b in range(2 * blocks):
        tap_ref = taps_ref if b < blocks else taps_other_ref
        lanes = slice((b % blocks) * LANES, (b % blocks + 1) * LANES)
        conv = jnp.zeros((rows, LANES), jnp.float32)
        for tap in range(taps):
            conv = conv + window_ref[b, first + tap : first + tap + rows, :] * tap_ref[tap : tap + 1, lanes]
        conv_ref[b] = conv
        total = total + conv
        square = square + conv * conv
    width = 2 * half
    mean = jnp.sum(total, axis=1, keepdims=True) / width
    var = jnp.sum(square, axis=1, keepdims=True) / width - mean * mean
    scale = lax.rsqrt(var + 1e-05)
    proj = None
    for side, tap_ref in ((0, taps_ref), (1, taps_other_ref)):
        parts = []
        for b in range(blocks):
            lanes = slice(b * LANES, (b + 1) * LANES)
            v = (conv_ref[side * blocks + b] - mean) * scale * tap_ref[taps : taps + 1, lanes]
            parts.append(jax.nn.silu(v).astype(jnp.bfloat16))
        mixed = jnp.concatenate(parts, axis=1)
        copies[side].wait()
        part = jnp.dot(mixed, out_weight_ref[side], preferred_element_type=jnp.float32)
        proj = part if proj is None else proj + part
    copies[2].wait()
    copies[3].wait()
    stream = (resid_ref[...].astype(jnp.float32) + proj).astype(jnp.bfloat16)
    stream_ref[...] = stream
    wide = stream.astype(jnp.float32)
    power = jnp.mean(wide * wide, axis=1, keepdims=True)
    gain = ffn_gain_ref[...].reshape(1, -1)
    normed = (wide * lax.rsqrt(power + 1e-06) * gain).astype(jnp.bfloat16)
    place = sum(p.astype(jnp.float32) for p in places(ids_ref[...], cap, experts))
    outgoing_ref[...] = jnp.dot(
        place.astype(jnp.bfloat16), normed, preferred_element_type=jnp.float32
    ).astype(jnp.bfloat16)


def expert_kernel(rows_ref, gate_ref, up_ref, down_ref, out_hbm, hidden_ref, out_ref, sems):
    hidden_width = gate_ref.shape[2]
    model_width = rows_ref.shape[1]
    step = min(256, hidden_width)
    for at in range(0, hidden_width, step):
        gate = jnp.dot(
            rows_ref[...], gate_ref[0, :, at : at + step], preferred_element_type=jnp.float32
        )
        up = jnp.dot(
            rows_ref[...], up_ref[0, :, at : at + step], preferred_element_type=jnp.float32
        )
        hidden_ref[:, at : at + step] = (jax.nn.silu(gate) * up).astype(jnp.bfloat16)
    wide = model_width // out_ref.shape[0]
    copies = []
    for n in range(out_ref.shape[0]):
        out_ref[n] = jnp.dot(
            hidden_ref[...],
            down_ref[0, :, n * wide : (n + 1) * wide],
            preferred_element_type=jnp.float32,
        ).astype(jnp.bfloat16)
        copies.append(
            pltpu.make_async_copy(
                out_ref.at[n], out_hbm.at[:, n * wide : (n + 1) * wide], sems.at[n]
            )
        )
        copies[-1].start()
    for copy in copies:
        copy.wait()


def combine_kernel(cap, experts, returned_ref, ids_ref, mix_ref, stream_ref, out_ref):
    topk, rows = ids_ref.shape
    mix = jnp.concatenate([mix_ref[...], jnp.zeros((8 - topk, rows), jnp.float32)], axis=0).T
    total = None
    for k, place in enumerate(places(ids_ref[...], cap, experts)):
        got = lax.dot_general(
            place.astype(jnp.float32).astype(jnp.bfloat16),
            returned_ref[...],
            (((0,), (0,)), ((), ())),
            preferred_element_type=jnp.float32,
        )
        part = got * mix[:, k : k + 1]
        total = part if total is None else total + part
    out_ref[...] = (stream_ref[...].astype(jnp.float32) + total).astype(jnp.bfloat16)


def vmem(count):
    return [pl.BlockSpec(memory_space=pltpu.VMEM)] * count


def hbm(count):
    return [pl.BlockSpec(memory_space=pltpu.HBM)] * count


def params(mib):
    return pltpu.CompilerParams(vmem_limit_bytes=mib << 20)


def per_device(
    resid,
    value_in,
    gate_in,
    conv_weight,
    norm_gain,
    out_weight,
    ffn_gain,
    expert_ids,
    expert_mix,
    w_gate,
    w_up,
    w_down,
):
    bf16 = jnp.bfloat16
    f32 = jnp.float32
    sp_count = lax.axis_size("sp")
    tp_count = lax.axis_size("tp")
    experts = sp_count * tp_count
    rows_here, model_width = resid.shape
    topk = expert_ids.shape[1]
    cap = max(2, (2 * topk * rows_here + experts - 1) // experts)
    slots = experts * cap
    core = lax.axis_index("tp").astype(jnp.int32).reshape(1)
    length, half = value_in.shape
    taps_count = conv_weight.shape[0]
    inner = rows_here + HALO
    ids = expert_ids.T
    mix = expert_mix.T

    swap = [(s * 2 + c, s * 2 + 1 - c) for s in range(sp_count) for c in range(2)]
    near = []
    far = []
    for s in range(sp_count):
        if s + 1 < sp_count:
            near.append((s * 2, (s + 1) * 2))
            far.append((s * 2 + 1, (s + 1) * 2))
        if s > 0:
            near.append((s * 2 + 1, (s - 1) * 2 + 1))
            far.append((s * 2, (s - 1) * 2 + 1))

    mine, give, near_rows, far_rows, taps = pl.pallas_call(
        glu_kernel,
        out_shape=(
            jax.ShapeDtypeStruct((inner, half), bf16),
            jax.ShapeDtypeStruct((inner, half), bf16),
            jax.ShapeDtypeStruct((HALO, half), bf16),
            jax.ShapeDtypeStruct((HALO, half), bf16),
            jax.ShapeDtypeStruct((taps_count + 1, half), f32),
        ),
        in_specs=[pl.BlockSpec(memory_space=pltpu.SMEM)] + hbm(4),
        out_specs=vmem(5),
        scratch_shapes=[
            pltpu.VMEM((length, half), bf16),
            pltpu.VMEM((length, half), bf16),
            pltpu.VMEM((length, half), bf16),
            pltpu.VMEM((taps_count, half), f32),
            pltpu.VMEM((half,), f32),
            pltpu.SemaphoreType.DMA((4,)),
        ],
        compiler_params=params(8),
        name="glu",
    )(core, value_in, gate_in, conv_weight, norm_gain)
    near_rows = lax.ppermute(near_rows, BOTH, near)
    far_rows = lax.ppermute(far_rows, BOTH, far)
    other = lax.ppermute(give, BOTH, swap)
    taps_other = lax.ppermute(taps, BOTH, swap)

    outgoing, stream = pl.pallas_call(
        functools.partial(module_kernel, cap, experts),
        out_shape=(
            jax.ShapeDtypeStruct((slots, model_width), bf16),
            jax.ShapeDtypeStruct((rows_here, model_width), bf16),
        ),
        in_specs=[pl.BlockSpec(memory_space=pltpu.SMEM)] + vmem(7) + hbm(3),
        out_specs=vmem(2),
        scratch_shapes=[
            pltpu.VMEM((2 * half // LANES, inner + HALO, LANES), f32),
            pltpu.VMEM((2 * half // LANES, rows_here, LANES), f32),
            pltpu.VMEM((2, half, model_width), bf16),
            pltpu.VMEM((rows_here, model_width), bf16),
            pltpu.VMEM((model_width,), f32),
            pltpu.SemaphoreType.DMA((4,)),
        ],
        compiler_params=params(24),
        name="module",
    )(
        core,
        mine,
        other,
        near_rows,
        far_rows,
        taps,
        taps_other,
        ids,
        out_weight,
        resid,
        ffn_gain,
    )

    arrived = lax.all_to_all(
        outgoing.reshape(experts, cap, model_width), BOTH, split_axis=0, concat_axis=0, tiled=True
    ).reshape(slots, model_width)

    hidden_width = w_gate.shape[2]
    pieces = 4
    done = pl.pallas_call(
        expert_kernel,
        out_shape=jax.ShapeDtypeStruct((slots, model_width), bf16),
        in_specs=vmem(4),
        out_specs=hbm(1)[0],
        scratch_shapes=[
            pltpu.VMEM((slots, hidden_width), bf16),
            pltpu.VMEM((pieces, slots, model_width // pieces), bf16),
            pltpu.SemaphoreType.DMA((pieces,)),
        ],
        compiler_params=params(24),
        name="experts",
    )(arrived, w_gate, w_up, w_down)

    returned = lax.all_to_all(
        done.reshape(experts, cap, model_width), BOTH, split_axis=0, concat_axis=0, tiled=True
    ).reshape(slots, model_width)

    return pl.pallas_call(
        functools.partial(combine_kernel, cap, experts),
        out_shape=jax.ShapeDtypeStruct((rows_here, model_width), bf16),
        in_specs=vmem(4),
        out_specs=pl.BlockSpec(memory_space=pltpu.VMEM),
        compiler_params=params(16),
        name="combine",
    )(returned, ids, mix, stream)


def solution(mesh):
    return jax.shard_map(
        per_device,
        mesh=mesh,
        in_specs=(
            P(("sp", "tp"), None),
            P("sp", "tp"),
            P("sp", "tp"),
            P(None, "tp"),
            P("tp"),
            P(),
            P(),
            P(("sp", "tp"), None),
            P(("sp", "tp"), None),
            P(("sp", "tp"), None, None),
            P(("sp", "tp"), None, None),
            P(("sp", "tp"), None, None),
        ),
        out_specs=P(("sp", "tp"), None),
        check_vma=False,
    )
```

time: 146 us -> 145 us (level)
  blocking collectives: 58 us -> 110 us
  waiting for transfers between devices: 48.7 us -> 0.84 us
  starting transfers between devices: 9.82 us -> 6.1 us
    all_to_all x0 -> x1, blocking collectives: none -> 52.1 us  [per_device(): lax.all_to_all(done.reshape(experts, cap, model_width), BOTH, split_axis=...]
    all_to_all x1 -> x0, waiting for transfers between devices: 48.6 us -> none  [per_device(): lax.all_to_all(done.reshape(experts, cap, model_width), BOTH, split_axis=...]
    all_to_all x1 -> x0, starting transfers between devices: 3.66 us -> none  [per_device(): lax.all_to_all(done.reshape(experts, cap, model_width), BOTH, split_axis=...]
    pallas_call x1, Pallas kernels: 10 us -> 7.53 us  [per_device(): pl.pallas_call(expert_kernel, out_shape=jax.ShapeDtypeStruct((slots, mode...]
    pallas_call x1, Pallas kernels: 4.61 us -> 6.31 us  [per_device(): pl.pallas_call(functools.partial(module_kernel, cap, experts), out_shape=...]
    unnamed x22 -> x26, local copies, waits for them, and re-layouts: 10.9 us -> 11 us
  transfers between devices with their start and end apart: 5 -> 4, of which waited for: 1 -> 1; matrix products, arithmetic and copies ran while one was open for 2% -> 0% of each run, Pallas kernels for 0% -> 0%
where the time goes in v2:
time: 145 us
  blocking collectives  110 us (76%)
  Pallas kernels  16.4 us (11%)
  local copies, waits for them, and re-layouts  11 us (8%)
  starting transfers between devices  6.1 us (4%)
    all_to_all x1, blocking collectives, per_device(): lax.all_to_all(outgoing.reshape(experts, cap, model_width), BOTH, split_a...  58.1 us
    all_to_all x1, blocking collectives, per_device(): lax.all_to_all(done.reshape(experts, cap, model_width), BOTH, split_axis=...  52.1 us
    unnamed x26, local copies, waits for them, and re-layouts  11 us
    pallas_call x1, Pallas kernels, per_device(): pl.pallas_call(expert_kernel, out_shape=jax.ShapeDtypeStruct((slots, mode...  7.53 us
    pallas_call x1, Pallas kernels, per_device(): pl.pallas_call(functools.partial(module_kernel, cap, experts), out_shape=...  6.31 us
    ppermute x1, starting transfers between devices, per_device(): near_rows = lax.ppermute(near_rows, BOTH, near)  4.8 us
  transfers between devices with their start and end apart: 4, of which 1 were waited for; matrix products, arithmetic and copies ran while one was open for 0% of the time, Pallas kernels for 0%

profile of v2, /device:TPU:0, one launch (start us, length us, event | category | flops | bytes accessed | tf_op | source)
XLA Modules:
  0.0 144.6 jit_solution(16230698009628887430)
XLA Ops:
  0.0 0.0 copy-start.5
  0.0 1.0 copy-done.5
  1.0 0.0 copy-start.6
  1.0 1.0 copy-done.6
  2.0 0.0 copy-start.7
  2.0 0.9 copy-done.7
  2.9 0.0 copy-start.9
  2.9 0.7 copy-done.9
  3.6 0.8 glu.1
  4.4 0.6 collective-permute-start
  4.9 0.1 collective-permute-start.3
  5.0 4.8 %collective-permute-start.1 = (bf16[16,768]{1,0:T(8,128)(2,1)S(1)}, bf16[16,768]{1,0:T(8,128)(2,1)S(1)}, u32[]{:S(2)}, u32[]{:S(2)}) collective-permute-start(bf16[16,768]{1,0:T(8,128)(2,1)S(1)} %get-tuple-element.14), channel_id=1, source_target_pairs={{0,2},{2,4},{3,1},{4,6},{5,3},{6,8},{7,5},{8,10},{9,7},{10,12},{11... | collective-permute-start | bytes 73736 | tf_op jit(solution)/shard_map/ppermute | solution.py:293
  9.8 0.7 collective-permute-start.2
  10.5 0.8 collective-permute-done.1.near_ref
  11.3 0.0 collective-permute-done.2.far_ref
  11.3 0.0 collective-permute-done.3.taps_other_ref
  11.3 0.0 collective-permute-done.other_ref
  11.3 0.0 copy-start
  11.3 2.8 %copy-done = bf16[1536,2048]{1,0:T(8,128)(2,1)S(1)} copy-done((bf16[1536,2048]{1,0:T(8,128)(2,1)S(1)}, bf16[1536,2048]{1,0:T(8,128)(2,1)}, u32[]{:S(2)}) %copy-start) | copy-done | bytes 6291480
  14.1 0.0 copy-start.4
  14.1 1.0 copy-done.4
  15.1 0.0 copy-start.8
  15.2 0.7 copy-done.8
  15.8 0.0 copy-start.10
  15.8 0.7 copy-done.10
  16.5 0.0 copy-start.1
  16.5 0.0 copy-start.2
  16.5 6.3 %module.1 = (bf16[512,2048]{1,0:T(8,128)(2,1)S(1)}, bf16[128,2048]{1,0:T(8,128)(2,1)S(1)}) custom-call(s32[1]{0:T(128)} %bitcast.core_ref, bf16[144,768]{1,0:T(8,128)(2,1)S(1)} %get-tuple-element.12.mine_ref, bf16[144,768]{1,0:T(8,128)(2,1)S(1)} %collective-permute-done.other_ref, bf16[16,768]{1,0:T(8,128)(2,1)S(1)} %collective-permute-done.1.near_ref, ...), custom_call_target="tpu_custom_call" | custom-call | tf_op jit(solution)/shard_map/module/pallas_call | solution.py:298
  22.8 58.1 %all_to_all.10 = bf16[32,16,2048]{2,1,0:T(8,128)(2,1)S(1)} all-to-all(bf16[32,16,2048]{2,1,0:T(8,128)(2,1)S(1)} %bitcast.10), channel_id=1, replica_groups=mesh['sp'=16,'tp'=2] {'sp','tp'}, dimensions={0} | all-to-all | bytes 4194304 | tf_op jit(solution)/shard_map/all_to_all | solution.py:330
  80.9 0.0 copy-done.1
  80.9 0.0 copy-done.2
  80.9 0.0 copy-start.3
  80.9 2.2 %copy-done.3 = bf16[1,1024,2048]{2,1,0:T(8,128)(2,1)S(1)} copy-done((bf16[1,1024,2048]{2,1,0:T(8,128)(2,1)S(1)}, bf16[1,1024,2048]{2,1,0:T(8,128)(2,1)}, u32[]{:S(2)}) %copy-start.3) | copy-done | bytes 4194328
  83.1 7.5 %experts.1 = bf16[512,2048]{1,0:T(8,128)(2,1)S(1)} custom-call(bf16[512,2048]{1,0:T(8,128)(2,1)S(1)} %bitcast.8, bf16[1,2048,1024]{2,1,0:T(8,128)(2,1)S(1)} %copy-done.1, bf16[1,2048,1024]{2,1,0:T(8,128)(2,1)S(1)} %copy-done.2, bf16[1,1024,2048]{2,1,0:T(8,128)(2,1)S(1)} %copy-done.3), custom_call_target="tpu_custom_call" | custom-call | tf_op jit(solution)/shard_map/experts/pallas_call | solution.py:336
  90.6 0.0 copy-start.11
  90.7 0.0 copy-start.12
  90.7 52.1 %all_to_all.11 = bf16[32,16,2048]{2,1,0:T(8,128)(2,1)S(1)} all-to-all(bf16[32,16,2048]{2,1,0:T(8,128)(2,1)S(1)} %bitcast.9), channel_id=1, replica_groups=mesh['sp'=16,'tp'=2] {'sp','tp'}, dimensions={0} | all-to-all | bytes 4194304 | tf_op jit(solution)/shard_map/all_to_all | solution.py:350
  142.8 0.0 copy-done.11
  142.8 0.0 copy-done.12
  142.8 1.8 %combine.1 = bf16[128,2048]{1,0:T(8,128)(2,1)} custom-call(bf16[512,2048]{1,0:T(8,128)(2,1)S(1)} %bitcast.7, s32[2,128]{1,0:T(2,128)S(1)} %bitcast.12, f32[2,128]{1,0:T(2,128)S(1)} %bitcast.13, bf16[128,2048]{1,0:T(8,128)(2,1)S(1)} %get-tuple-element.18.stream_ref), custom_call_target="tpu_custom_call" | custom-call | tf_op jit(solution)/shard_map/combine/pallas_call | solution.py:354
Async XLA Ops:
  0.0 1.0 copy-start.5
  1.0 1.0 copy-start.6
  2.0 0.9 copy-start.7
  2.9 0.7 copy-start.9
  4.4 7.0 %collective-permute-start = (bf16[144,768]{1,0:T(8,128)(2,1)S(1)}, bf16[144,768]{1,0:T(8,128)(2,1)S(1)}, u32[]{:S(2)}, u32[]{:S(2)}) collective-permute-start(bf16[144,768]{1,0:T(8,128)(2,1)S(1)} %get-tuple-element.13), channel_id=1, source_target_pairs={{0,1},{1,0},{2,3},{3,2},{4,5},{5,4},{6,7},{7,6},{8,9},{9,8},{10,11... | collective-permute-start | bytes 663560 | tf_op jit(solution)/shard_map/ppermute | solution.py:295
  4.9 6.4 %collective-permute-start.3 = (f32[32,768]{1,0:T(8,128)S(1)}, f32[32,768]{1,0:T(8,128)S(1)}, u32[]{:S(2)}, u32[]{:S(2)}) collective-permute-start(f32[32,768]{1,0:T(8,128)S(1)} %get-tuple-element.16.taps_ref), channel_id=1, source_target_pairs={{0,1},{1,0},{2,3},{3,2},{4,5},{5,4},{6,7},{7,6},{8,9},{9,8},{10,11... | collective-permute-start | bytes 294920 | tf_op jit(solution)/shard_map/ppermute | solution.py:296
  5.0 6.3 %collective-permute-start.1 = (bf16[16,768]{1,0:T(8,128)(2,1)S(1)}, bf16[16,768]{1,0:T(8,128)(2,1)S(1)}, u32[]{:S(2)}, u32[]{:S(2)}) collective-permute-start(bf16[16,768]{1,0:T(8,128)(2,1)S(1)} %get-tuple-element.14), channel_id=1, source_target_pairs={{0,2},{2,4},{3,1},{4,6},{5,3},{6,8},{7,5},{8,10},{9,7},{10,12},{11... | collective-permute-start | bytes 73736 | tf_op jit(solution)/shard_map/ppermute | solution.py:293
  9.8 1.5 %collective-permute-start.2 = (bf16[16,768]{1,0:T(8,128)(2,1)S(1)}, bf16[16,768]{1,0:T(8,128)(2,1)S(1)}, u32[]{:S(2)}, u32[]{:S(2)}) collective-permute-start(bf16[16,768]{1,0:T(8,128)(2,1)S(1)} %get-tuple-element.15), channel_id=1, source_target_pairs={{1,2},{3,4},{2,1},{5,6},{4,3},{7,8},{6,5},{9,10},{8,7},{11,12},{10... | collective-permute-start | bytes 73736 | tf_op jit(solution)/shard_map/ppermute | solution.py:294
  11.3 2.8 %copy-start = (bf16[1536,2048]{1,0:T(8,128)(2,1)S(1)}, bf16[1536,2048]{1,0:T(8,128)(2,1)}, u32[]{:S(2)}) copy-start(bf16[1536,2048]{1,0:T(8,128)(2,1)} %out_weight_hbm.1) | copy-start | bytes 18874372
  14.1 1.0 copy-start.4
  15.1 0.7 copy-start.8
  15.8 0.7 copy-start.10
  16.5 64.4 %copy-start.1 = (bf16[1,2048,1024]{2,1,0:T(8,128)(2,1)S(1)}, bf16[1,2048,1024]{2,1,0:T(8,128)(2,1)}, u32[]{:S(2)}) copy-start(bf16[1,2048,1024]{2,1,0:T(8,128)(2,1)} %gate_ref.1) | copy-start | bytes 12582916
  16.5 64.4 %copy-start.2 = (bf16[1,2048,1024]{2,1,0:T(8,128)(2,1)S(1)}, bf16[1,2048,1024]{2,1,0:T(8,128)(2,1)}, u32[]{:S(2)}) copy-start(bf16[1,2048,1024]{2,1,0:T(8,128)(2,1)} %up_ref.1) | copy-start | bytes 12582916
  80.9 2.2 %copy-start.3 = (bf16[1,1024,2048]{2,1,0:T(8,128)(2,1)S(1)}, bf16[1,1024,2048]{2,1,0:T(8,128)(2,1)}, u32[]{:S(2)}) copy-start(bf16[1,1024,2048]{2,1,0:T(8,128)(2,1)} %down_ref.1) | copy-start | bytes 12582916
  90.6 52.2 %copy-start.11 = (s32[128,2]{0,1:T(2,128)S(1)}, s32[128,2]{0,1:T(2,128)}, u32[]{:S(2)}) copy-start(s32[128,2]{0,1:T(2,128)} %param.19) | copy-start | bytes 3076
  90.7 52.2 %copy-start.12 = (f32[128,2]{0,1:T(2,128)S(1)}, f32[128,2]{0,1:T(2,128)}, u32[]{:S(2)}) copy-start(f32[128,2]{0,1:T(2,128)} %param.20) | copy-start | bytes 3076

commit v3 on v2

--- a/solution.py
+++ b/solution.py
@@ -223,6 +223,10 @@
     return [pl.BlockSpec(memory_space=pltpu.HBM)] * count
 
 
+def far(*arrays):
+    return [pltpu.with_memory_space_constraint(a, pltpu.HBM) for a in arrays]
+
+
 def params(mib):
     return pltpu.CompilerParams(vmem_limit_bytes=mib << 20)
 
@@ -259,14 +263,14 @@
 
     swap = [(s * 2 + c, s * 2 + 1 - c) for s in range(sp_count) for c in range(2)]
     near = []
-    far = []
+    cross = []
     for s in range(sp_count):
         if s + 1 < sp_count:
             near.append((s * 2, (s + 1) * 2))
-            far.append((s * 2 + 1, (s + 1) * 2))
+            cross.append((s * 2 + 1, (s + 1) * 2))
         if s > 0:
             near.append((s * 2 + 1, (s - 1) * 2 + 1))
-            far.append((s * 2, (s - 1) * 2 + 1))
+            cross.append((s * 2, (s - 1) * 2 + 1))
 
     mine, give, near_rows, far_rows, taps = pl.pallas_call(
         glu_kernel,
@@ -289,9 +293,9 @@
         ],
         compiler_params=params(8),
         name="glu",
-    )(core, value_in, gate_in, conv_weight, norm_gain)
+    )(core, *far(value_in, gate_in, conv_weight, norm_gain))
     near_rows = lax.ppermute(near_rows, BOTH, near)
-    far_rows = lax.ppermute(far_rows, BOTH, far)
+    far_rows = lax.ppermute(far_rows, BOTH, cross)
     other = lax.ppermute(give, BOTH, swap)
     taps_other = lax.ppermute(taps, BOTH, swap)
 
@@ -322,9 +326,7 @@
         taps,
         taps_other,
         ids,
-        out_weight,
-        resid,
-        ffn_gain,
+        *far(out_weight, resid, ffn_gain),
     )
 
     arrived = lax.all_to_all(

time: 145 us -> 135 us (0.931)
  local copies, waits for them, and re-layouts: 11 us -> 0.7 us
    unnamed x26 -> x12, local copies, waits for them, and re-layouts: 11 us -> 0.7 us
where the time goes in v3:
time: 135 us
  blocking collectives  110 us (81%)
  Pallas kernels  16.8 us (12%)
  starting transfers between devices  6.1 us (5%)
    all_to_all x1, blocking collectives, per_device(): lax.all_to_all(outgoing.reshape(experts, cap, model_width), BOTH, split_a...  58.1 us
    all_to_all x1, blocking collectives, per_device(): lax.all_to_all(done.reshape(experts, cap, model_width), BOTH, split_axis=...  52.1 us
    pallas_call x1, Pallas kernels, per_device(): pl.pallas_call(expert_kernel, out_shape=jax.ShapeDtypeStruct((slots, mode...  7.62 us
    pallas_call x1, Pallas kernels, per_device(): pl.pallas_call(functools.partial(module_kernel, cap, experts), out_shape=...  5.85 us
    ppermute x1, starting transfers between devices, per_device(): near_rows = lax.ppermute(near_rows, BOTH, near)  4.8 us
  transfers between devices with their start and end apart: 4, of which 1 were waited for; matrix products, arithmetic and copies ran while one was open for 0% of the time, Pallas kernels for 0%

profile of v3, /device:TPU:0, one launch (start us, length us, event | category | flops | bytes accessed | tf_op | source)
XLA Modules:
  0.0 134.7 jit_solution(15170391534794780539)
XLA Ops:
  0.0 0.0 copy-start.2
  0.0 1.5 %glu.1 = (bf16[144,768]{1,0:T(8,128)(2,1)S(1)}, bf16[144,768]{1,0:T(8,128)(2,1)S(1)}, bf16[16,768]{1,0:T(8,128)(2,1)S(1)}, bf16[16,768]{1,0:T(8,128)(2,1)S(1)}, f32[32,768]{1,0:T(8,128)S(1)}) custom-call(s32[1]{0:T(128)} %bitcast.core_ref, bf16[256,768]{1,0:T(8,128)(2,1)} %value_hbm.1, bf16[256,768]{1,0:T(8,128)(2,1)} %gate_hbm.1, f32[31,768]{1,0:T(8,128)} %weight_hbm.1, ...), custom_call_target="tpu_custom_call" | custom-call | tf_op jit(solution)/shard_map/glu/pallas_call | solution.py:275
  1.6 0.6 collective-permute-start
  2.1 0.1 collective-permute-start.3
  2.2 4.8 %collective-permute-start.1 = (bf16[16,768]{1,0:T(8,128)(2,1)S(1)}, bf16[16,768]{1,0:T(8,128)(2,1)S(1)}, u32[]{:S(2)}, u32[]{:S(2)}) collective-permute-start(bf16[16,768]{1,0:T(8,128)(2,1)S(1)} %get-tuple-element.14), channel_id=1, source_target_pairs={{0,2},{2,4},{3,1},{4,6},{5,3},{6,8},{7,5},{8,10},{9,7},{10,12},{11... | collective-permute-start | bytes 73736 | tf_op jit(solution)/shard_map/ppermute | solution.py:297
  7.0 0.7 collective-permute-start.2
  7.7 0.8 collective-permute-done.1.near_ref
  8.5 0.0 collective-permute-done.2.far_ref
  8.5 0.0 collective-permute-done.3.taps_other_ref
  8.5 0.0 collective-permute-done.other_ref
  8.5 0.0 copy-start.3
  8.5 0.7 copy-done.3
  9.2 0.0 copy-start
  9.2 0.0 copy-start.1
  9.2 5.9 %module.1 = (bf16[512,2048]{1,0:T(8,128)(2,1)S(1)}, bf16[128,2048]{1,0:T(8,128)(2,1)S(1)}) custom-call(s32[1]{0:T(128)} %bitcast.core_ref, bf16[144,768]{1,0:T(8,128)(2,1)S(1)} %get-tuple-element.12.mine_ref, bf16[144,768]{1,0:T(8,128)(2,1)S(1)} %collective-permute-done.other_ref, bf16[16,768]{1,0:T(8,128)(2,1)S(1)} %collective-permute-done.1.near_ref, ...), custom_call_target="tpu_custom_call" | custom-call | tf_op jit(solution)/shard_map/module/pallas_call | solution.py:302
  15.1 58.1 %all_to_all.10 = bf16[32,16,2048]{2,1,0:T(8,128)(2,1)S(1)} all-to-all(bf16[32,16,2048]{2,1,0:T(8,128)(2,1)S(1)} %bitcast.10), channel_id=1, replica_groups=mesh['sp'=16,'tp'=2] {'sp','tp'}, dimensions={0} | all-to-all | bytes 4194304 | tf_op jit(solution)/shard_map/all_to_all | solution.py:332
  73.1 0.0 copy-done.2
  73.1 0.0 copy-done
  73.1 0.0 copy-done.1
  73.1 7.6 %experts.1 = bf16[512,2048]{1,0:T(8,128)(2,1)S(1)} custom-call(bf16[512,2048]{1,0:T(8,128)(2,1)S(1)} %bitcast.8, bf16[1,2048,1024]{2,1,0:T(8,128)(2,1)S(1)} %copy-done, bf16[1,2048,1024]{2,1,0:T(8,128)(2,1)S(1)} %copy-done.1, bf16[1,1024,2048]{2,1,0:T(8,128)(2,1)S(1)} %copy-done.2), custom_call_target="tpu_custom_call" | custom-call | tf_op jit(solution)/shard_map/experts/pallas_call | solution.py:338
  80.8 0.0 copy-start.4
  80.8 0.0 copy-start.5
  80.8 52.1 %all_to_all.11 = bf16[32,16,2048]{2,1,0:T(8,128)(2,1)S(1)} all-to-all(bf16[32,16,2048]{2,1,0:T(8,128)(2,1)S(1)} %bitcast.9), channel_id=1, replica_groups=mesh['sp'=16,'tp'=2] {'sp','tp'}, dimensions={0} | all-to-all | bytes 4194304 | tf_op jit(solution)/shard_map/all_to_all | solution.py:352
  132.9 0.0 copy-done.4
  132.9 0.0 copy-done.5
  132.9 1.8 %combine.1 = bf16[128,2048]{1,0:T(8,128)(2,1)} custom-call(bf16[512,2048]{1,0:T(8,128)(2,1)S(1)} %bitcast.7, s32[2,128]{1,0:T(2,128)S(1)} %bitcast.12, f32[2,128]{1,0:T(2,128)S(1)} %bitcast.13, bf16[128,2048]{1,0:T(8,128)(2,1)S(1)} %get-tuple-element.18.stream_ref), custom_call_target="tpu_custom_call" | custom-call | tf_op jit(solution)/shard_map/combine/pallas_call | solution.py:356
Async XLA Ops:
  0.0 73.1 %copy-start.2 = (bf16[1,1024,2048]{2,1,0:T(8,128)(2,1)S(1)}, bf16[1,1024,2048]{2,1,0:T(8,128)(2,1)}, u32[]{:S(2)}) copy-start(bf16[1,1024,2048]{2,1,0:T(8,128)(2,1)} %down_ref.1) | copy-start | bytes 12582916
  1.6 7.0 %collective-permute-start = (bf16[144,768]{1,0:T(8,128)(2,1)S(1)}, bf16[144,768]{1,0:T(8,128)(2,1)S(1)}, u32[]{:S(2)}, u32[]{:S(2)}) collective-permute-start(bf16[144,768]{1,0:T(8,128)(2,1)S(1)} %get-tuple-element.13), channel_id=1, source_target_pairs={{0,1},{1,0},{2,3},{3,2},{4,5},{5,4},{6,7},{7,6},{8,9},{9,8},{10,11... | collective-permute-start | bytes 663560 | tf_op jit(solution)/shard_map/ppermute | solution.py:299
  2.1 6.4 %collective-permute-start.3 = (f32[32,768]{1,0:T(8,128)S(1)}, f32[32,768]{1,0:T(8,128)S(1)}, u32[]{:S(2)}, u32[]{:S(2)}) collective-permute-start(f32[32,768]{1,0:T(8,128)S(1)} %get-tuple-element.16.taps_ref), channel_id=1, source_target_pairs={{0,1},{1,0},{2,3},{3,2},{4,5},{5,4},{6,7},{7,6},{8,9},{9,8},{10,11... | collective-permute-start | bytes 294920 | tf_op jit(solution)/shard_map/ppermute | solution.py:300
  2.2 6.3 %collective-permute-start.1 = (bf16[16,768]{1,0:T(8,128)(2,1)S(1)}, bf16[16,768]{1,0:T(8,128)(2,1)S(1)}, u32[]{:S(2)}, u32[]{:S(2)}) collective-permute-start(bf16[16,768]{1,0:T(8,128)(2,1)S(1)} %get-tuple-element.14), channel_id=1, source_target_pairs={{0,2},{2,4},{3,1},{4,6},{5,3},{6,8},{7,5},{8,10},{9,7},{10,12},{11... | collective-permute-start | bytes 73736 | tf_op jit(solution)/shard_map/ppermute | solution.py:297
  7.0 1.5 %collective-permute-start.2 = (bf16[16,768]{1,0:T(8,128)(2,1)S(1)}, bf16[16,768]{1,0:T(8,128)(2,1)S(1)}, u32[]{:S(2)}, u32[]{:S(2)}) collective-permute-start(bf16[16,768]{1,0:T(8,128)(2,1)S(1)} %get-tuple-element.15), channel_id=1, source_target_pairs={{1,2},{3,4},{2,1},{5,6},{4,3},{7,8},{6,5},{9,10},{8,7},{11,12},{10... | collective-permute-start | bytes 73736 | tf_op jit(solution)/shard_map/ppermute | solution.py:298
  8.5 0.7 copy-start.3
  9.2 63.9 %copy-start = (bf16[1,2048,1024]{2,1,0:T(8,128)(2,1)S(1)}, bf16[1,2048,1024]{2,1,0:T(8,128)(2,1)}, u32[]{:S(2)}) copy-start(bf16[1,2048,1024]{2,1,0:T(8,128)(2,1)} %gate_ref.1) | copy-start | bytes 12582916
  9.2 63.9 %copy-start.1 = (bf16[1,2048,1024]{2,1,0:T(8,128)(2,1)S(1)}, bf16[1,2048,1024]{2,1,0:T(8,128)(2,1)}, u32[]{:S(2)}) copy-start(bf16[1,2048,1024]{2,1,0:T(8,128)(2,1)} %up_ref.1) | copy-start | bytes 12582916
  80.8 52.2 %copy-start.4 = (s32[128,2]{0,1:T(2,128)S(1)}, s32[128,2]{0,1:T(2,128)}, u32[]{:S(2)}) copy-start(s32[128,2]{0,1:T(2,128)} %param.19) | copy-start | bytes 3076
  80.8 52.2 %copy-start.5 = (f32[128,2]{0,1:T(2,128)S(1)}, f32[128,2]{0,1:T(2,128)}, u32[]{:S(2)}) copy-start(f32[128,2]{0,1:T(2,128)} %param.20) | copy-start | bytes 3076

commit v4 on v3

v4 whole, which is shorter than its diff:
```python
import functools

import jax
import jax.numpy as jnp
from jax import lax
from jax.experimental import pallas as pl
from jax.experimental.pallas import tpu as pltpu
from jax.sharding import PartitionSpec as P


BOTH = ("sp", "tp")
LANES = 128
HALO = 16


def glu_kernel(
    core_ref,
    value_hbm,
    gate_hbm,
    weight_hbm,
    gain_hbm,
    ids_hbm,
    mix_hbm,
    mine_ref,
    give_ref,
    near_ref,
    far_ref,
    taps_ref,
    meta_ref,
    value_ref,
    gate_ref,
    glu_ref,
    weight_ref,
    gain_ref,
    ids_ref,
    mix_ref,
    sems,
):
    core = core_ref[0]
    copies = [
        pltpu.make_async_copy(source, target, sems.at[n])
        for n, (source, target) in enumerate(
            (
                (value_hbm, value_ref),
                (gate_hbm, gate_ref),
                (weight_hbm, weight_ref),
                (gain_hbm, gain_ref),
                (ids_hbm, ids_ref),
                (mix_hbm, mix_ref),
            )
        )
    ]
    for copy in copies:
        copy.start()
    copies[0].wait()
    copies[1].wait()
    value = value_ref[...].astype(jnp.float32)
    gate = gate_ref[...].astype(jnp.float32)
    glu_ref[...] = (value * jax.nn.sigmoid(gate)).astype(jnp.bfloat16)
    inner = mine_ref.shape[0]
    rows = glu_ref.shape[0]
    step = rows - inner
    last = rows - HALO
    mine_ref[...] = glu_ref[pl.ds(pl.multiple_of(core * step, HALO), inner), :]
    give_ref[...] = glu_ref[pl.ds(pl.multiple_of((1 - core) * step, HALO), inner), :]
    near_ref[...] = glu_ref[pl.ds(pl.multiple_of((1 - core) * last, HALO), HALO), :]
    far_ref[...] = glu_ref[pl.ds(pl.multiple_of(core * last, HALO), HALO), :]
    copies[2].wait()
    copies[3].wait()
    taps = weight_ref.shape[0]
    taps_ref[0:taps, :] = weight_ref[...]
    taps_ref[taps : taps + 1, :] = gain_ref[...].reshape(1, -1)
    copies[4].wait()
    copies[5].wait()
    topk = ids_ref.shape[0]
    meta_ref[0:topk, :] = ids_ref[...].astype(jnp.float32)
    meta_ref[topk : 2 * topk, :] = mix_ref[...]


def places(ids, cap, experts, where_ref, which, first, count):
    topk, rows = ids.shape
    lane = lax.broadcasted_iota(jnp.int32, (experts, rows), 0)
    named = [ids[k : k + 1, :] == lane for k in range(topk)]
    member = sum(n.astype(jnp.float32) for n in named).astype(jnp.bfloat16)
    down = lax.broadcasted_iota(jnp.int32, (rows, rows), 0)
    across = lax.broadcasted_iota(jnp.int32, (rows, rows), 1)
    before = (down < across).astype(jnp.float32).astype(jnp.bfloat16)
    rank = jnp.dot(member, before, preferred_element_type=jnp.float32)
    slot = lax.broadcasted_iota(jnp.int32, (count * 2 * cap, rows), 0) + first * 2 * cap
    found = []
    for k, n in enumerate(named):
        own = jnp.sum(jnp.where(n, rank, 0.0), axis=0, keepdims=True).astype(jnp.int32)
        chip = jnp.right_shift(ids[k : k + 1, :], 1)
        side = jnp.bitwise_and(ids[k : k + 1, :], 1)
        turned = jnp.bitwise_xor(chip, where_ref[1]) * (2 * cap) + own
        if which is None:
            target = turned + jnp.bitwise_xor(side, where_ref[0]) * cap
        else:
            target = jnp.where(side == where_ref[0], turned + which * cap, -1)
        found.append(slot == target)
    return found


def joined(refs):
    return jnp.concatenate([ref[...].astype(jnp.float32) for ref in refs], axis=0).astype(
        jnp.bfloat16
    )


def dealt(rows, refs):
    size = refs[0].shape[0]
    for n, ref in enumerate(refs):
        ref[...] = rows[n * size : (n + 1) * size, :].astype(jnp.bfloat16)


def split_meta(meta_ref):
    topk = meta_ref.shape[0] // 2
    return meta_ref[0:topk, :].astype(jnp.int32), meta_ref[topk : 2 * topk, :]


def collected(meta_ref, rows, cap, experts, where_ref, which, first, count):
    ids, mix = split_meta(meta_ref)
    topk, tokens = ids.shape
    mix = jnp.concatenate([mix, jnp.zeros((8 - topk, tokens), jnp.float32)], axis=0).T
    total = None
    for k, place in enumerate(places(ids, cap, experts, where_ref, which, first, count)):
        got = lax.dot_general(
            place.astype(jnp.float32).astype(jnp.bfloat16),
            rows,
            (((0,), (0,)), ((), ())),
            preferred_element_type=jnp.float32,
        )
        part = got * mix[:, k : k + 1]
        total = part if total is None else total + part
    return total


def module_kernel(
    cap,
    experts,
    count,
    where_ref,
    mine_ref,
    other_ref,
    near_ref,
    far_ref,
    taps_ref,
    taps_other_ref,
    meta_ref,
    out_weight_hbm,
    resid_hbm,
    ffn_gain_hbm,
    stream_hbm,
    *more,
):
    outgoing_refs = more[:count]
    (
        window_ref,
        conv_ref,
        out_weight_ref,
        resid_ref,
        ffn_gain_ref,
        stream_ref,
        weight_sems,
        sems,
    ) = more[count:]
    core = where_ref[0]
    inner, half = mine_ref.shape
    cuts = 4
    cut = half // cuts
    copies = []
    for side in range(2):
        copies.append([])
        for n in range(cuts):
            where = (core + side * (1 - 2 * core)) * half + n * cut
            copies[side].append(
                pltpu.make_async_copy(
                    out_weight_hbm.at[pl.ds(pl.multiple_of(where, HALO), cut), :],
                    out_weight_ref.at[side, n * cut : (n + 1) * cut, :],
                    weight_sems.at[side, n],
                )
            )
            copies[side][n].start()
    fetch = [
        pltpu.make_async_copy(resid_hbm, resid_ref, sems.at[0]),
        pltpu.make_async_copy(ffn_gain_hbm, ffn_gain_ref, sems.at[1]),
    ]
    for copy in fetch:
        copy.start()
    rows = resid_ref.shape[0]
    taps = taps_ref.shape[0] - 1
    blocks = half // LANES
    inner_at = pl.multiple_of((1 - core) * HALO, HALO)
    outer_at = pl.multiple_of(core * inner, HALO)
    first = HALO - taps // 2
    total = jnp.zeros((rows, LANES), jnp.float32)
    square = jnp.zeros((rows, LANES), jnp.float32)
    for b in range(2 * blocks):
        sources = (mine_ref, near_ref, taps_ref) if b < blocks else (other_ref, far_ref, taps_other_ref)
        source, outer, tap_ref = sources
        lanes = slice((b % blocks) * LANES, (b % blocks + 1) * LANES)
        window_ref[b, pl.ds(inner_at, inner), :] = source[:, lanes].astype(jnp.float32)
        window_ref[b, pl.ds(outer_at, HALO), :] = outer[:, lanes].astype(jnp.float32)
        conv = jnp.zeros((rows, LANES), jnp.float32)
        for tap in range(taps):
            conv = conv + window_ref[b, first + tap : first + tap + rows, :] * tap_ref[tap : tap + 1, lanes]
        conv_ref[b] = conv
        total = total + conv
        square = square + conv * conv
    width = 2 * half
    mean = jnp.sum(total, axis=1, keepdims=True) / width
    var = jnp.sum(square, axis=1, keepdims=True) / width - mean * mean
    scale = lax.rsqrt(var + 1e-05)
    proj = None
    for side, tap_ref in ((0, taps_ref), (1, taps_other_ref)):
        parts = []
        for b in range(blocks):
            lanes = slice(b * LANES, (b + 1) * LANES)
            v = (conv_ref[side * blocks + b] - mean) * scale * tap_ref[taps : taps + 1, lanes]
            parts.append(jax.nn.silu(v).astype(jnp.bfloat16))
        mixed = jnp.concatenate(parts, axis=1)
        for copy in copies[side]:
            copy.wait()
        part = jnp.dot(mixed, out_weight_ref[side], preferred_element_type=jnp.float32)
        proj = part if proj is None else proj + part
    for copy in fetch:
        copy.wait()
    stream = (resid_ref[...].astype(jnp.float32) + proj).astype(jnp.bfloat16)
    stream_ref[...] = stream
    keep = pltpu.make_async_copy(stream_ref, stream_hbm, sems.at[2])
    keep.start()
    wide = stream.astype(jnp.float32)
    power = jnp.mean(wide * wide, axis=1, keepdims=True)
    gain = ffn_gain_ref[...].reshape(1, -1)
    normed = (wide * lax.rsqrt(power + 1e-06) * gain).astype(jnp.bfloat16)
    ids, _ = split_meta(meta_ref)
    found = places(ids, cap, experts, where_ref, None, 0, count)
    place = sum(p.astype(jnp.float32) for p in found).astype(jnp.bfloat16)
    dealt(jnp.dot(place, normed, preferred_element_type=jnp.float32), outgoing_refs)
    keep.wait()


def pack_kernel(*refs):
    half = refs[0].shape[0] // 2
    parts = [ref[...].astype(jnp.float32)[half:, :] for ref in refs[:-1]]
    refs[-1][...] = jnp.concatenate(parts, axis=0).astype(jnp.bfloat16)


def fetch_kernel(gate_hbm, up_hbm, down_hbm, gate_ref, up_ref, down_ref, sems):
    cuts = 4
    copies = []
    for w, (source, target) in enumerate(
        ((gate_hbm, gate_ref), (up_hbm, up_ref), (down_hbm, down_ref))
    ):
        step = source.shape[1] // cuts
        for n in range(cuts):
            part = slice(n * step, (n + 1) * step)
            copies.append(
                pltpu.make_async_copy(source.at[0, part], target.at[0, part], sems.at[w, n])
            )
            copies[-1].start()
    for copy in copies:
        copy.wait()


def gather_kernel(cap, experts, first, where_ref, meta_ref, meta_other_ref, *refs):
    count = len(refs) - 2
    own_ref, other_ref = refs[count:]
    rows = joined(refs[:count])
    own_ref[...] = collected(meta_ref, rows, cap, experts, where_ref, 0, first, count)
    other_ref[...] = collected(meta_other_ref, rows, cap, experts, where_ref, 1, first, count)


def last_kernel(cap, experts, first, which, where_ref, meta_ref, base_ref, *refs):
    rows = joined(refs[:-1])
    total = collected(meta_ref, rows, cap, experts, where_ref, which, first, len(refs) - 1)
    refs[-1][...] = (base_ref[...] + total).astype(refs[-1].dtype)


def expert_kernel(gate_ref, up_ref, down_ref, got_ref, *refs):
    count = (len(refs) - 2) // 2
    rows_ref, hidden_ref = refs[2 * count :]
    cap = refs[0].shape[0] // 2
    parts = [ref[...].astype(jnp.float32)[:cap, :] for ref in refs[:count]]
    parts.append(got_ref[...].astype(jnp.float32))
    rows_ref[...] = jnp.concatenate(parts, axis=0).astype(jnp.bfloat16)
    hidden_width = gate_ref.shape[2]
    model_width = rows_ref.shape[1]
    step = min(256, hidden_width)
    for at in range(0, hidden_width, step):
        part = slice(at, at + step)
        gate = jnp.dot(rows_ref[...], gate_ref[0, :, part], preferred_element_type=jnp.float32)
        up = jnp.dot(rows_ref[...], up_ref[0, :, part], preferred_element_type=jnp.float32)
        hidden_ref[:, part] = (jax.nn.silu(gate) * up).astype(jnp.bfloat16)
    step = min(512, model_width)
    for at in range(0, model_width, step):
        part = slice(at, at + step)
        done = jnp.dot(hidden_ref[...], down_ref[0, :, part], preferred_element_type=jnp.float32)
        for n in range(count):
            pair = [done[m * cap : (m + 1) * cap, :] for m in (n, count + n)]
            refs[count + n][:, part] = jnp.concatenate(pair, axis=0).astype(jnp.bfloat16)


def combine_kernel(stream_ref, own_ref, other_ref, out_ref):
    total = own_ref[...] + other_ref[...].astype(jnp.float32)
    out_ref[...] = (stream_ref[...].astype(jnp.float32) + total).astype(jnp.bfloat16)


def vmem(count):
    return [pl.BlockSpec(memory_space=pltpu.VMEM)] * count


def hbm(count):
    return [pl.BlockSpec(memory_space=pltpu.HBM)] * count


def far(*arrays):
    return [pltpu.with_memory_space_constraint(a, pltpu.HBM) for a in arrays]


def params(mib):
    return pltpu.CompilerParams(vmem_limit_bytes=mib << 20)


def per_device(
    resid,
    value_in,
    gate_in,
    conv_weight,
    norm_gain,
    out_weight,
    ffn_gain,
    expert_ids,
    expert_mix,
    w_gate,
    w_up,
    w_down,
):
    bf16 = jnp.bfloat16
    f32 = jnp.float32
    sp_count = lax.axis_size("sp")
    tp_count = lax.axis_size("tp")
    experts = sp_count * tp_count
    rows_here, model_width = resid.shape
    topk = expert_ids.shape[1]
    cap = max(2, (2 * topk * rows_here + experts - 1) // experts)
    core = lax.axis_index("tp").astype(jnp.int32).reshape(1)
    length, half = value_in.shape
    taps_count = conv_weight.shape[0]
    inner = rows_here + HALO
    ids = expert_ids.T
    where = jnp.stack([core[0], lax.axis_index("sp").astype(jnp.int32)])

    def exchange(blocks, first):
        moved = []
        for n, block in enumerate(blocks):
            k = first + n
            pairs = [(s, s ^ k) for s in range(sp_count)]
            moved.append(lax.ppermute(block, "sp", pairs) if k else block)
        return moved

    swap = [(s * 2 + c, s * 2 + 1 - c) for s in range(sp_count) for c in range(2)]
    near = []
    cross = []
    for s in range(sp_count):
        if s + 1 < sp_count:
            near.append((s * 2, (s + 1) * 2))
            cross.append((s * 2 + 1, (s + 1) * 2))
        if s > 0:
            near.append((s * 2 + 1, (s - 1) * 2 + 1))
            cross.append((s * 2, (s - 1) * 2 + 1))

    mine, give, near_rows, far_rows, taps, meta = pl.pallas_call(
        glu_kernel,
        out_shape=(
            jax.ShapeDtypeStruct((inner, half), bf16),
            jax.ShapeDtypeStruct((inner, half), bf16),
            jax.ShapeDtypeStruct((HALO, half), bf16),
            jax.ShapeDtypeStruct((HALO, half), bf16),
            jax.ShapeDtypeStruct((taps_count + 1, half), f32),
            jax.ShapeDtypeStruct((2 * topk, rows_here), f32),
        ),
        in_specs=[pl.BlockSpec(memory_space=pltpu.SMEM)] + hbm(6),
        out_specs=vmem(6),
        scratch_shapes=[
            pltpu.VMEM((length, half), bf16),
            pltpu.VMEM((length, half), bf16),
            pltpu.VMEM((length, half), bf16),
            pltpu.VMEM((taps_count, half), f32),
            pltpu.VMEM((half,), f32),
            pltpu.VMEM((topk, rows_here), jnp.int32),
            pltpu.VMEM((topk, rows_here), f32),
            pltpu.SemaphoreType.DMA((6,)),
        ],
        compiler_params=params(8),
        name="glu",
    )(core, *far(value_in, gate_in, conv_weight, norm_gain, ids, expert_mix.T))
    other = lax.ppermute(give, BOTH, swap)
    taps_other = lax.ppermute(taps, BOTH, swap)
    near_rows = lax.ppermute(near_rows, BOTH, near)
    far_rows = lax.ppermute(far_rows, BOTH, cross)
    meta_other = lax.ppermute(meta, BOTH, swap)

    smem = [pl.BlockSpec(memory_space=pltpu.SMEM)]
    blocks = 2 * half // LANES
    tokens = jax.ShapeDtypeStruct((rows_here, model_width), bf16)
    sums = jax.ShapeDtypeStruct((rows_here, model_width), f32)
    piece = jax.ShapeDtypeStruct((2 * cap, model_width), bf16)
    sizes = (cap, experts)
    stream, *outgoing = pl.pallas_call(
        functools.partial(module_kernel, *sizes, sp_count),
        out_shape=[tokens] + [piece] * sp_count,
        in_specs=smem + vmem(7) + hbm(3),
        out_specs=hbm(1) + vmem(sp_count),
        scratch_shapes=[
            pltpu.VMEM((blocks, inner + HALO, LANES), f32),
            pltpu.VMEM((blocks, rows_here, LANES), f32),
            pltpu.VMEM((2, half, model_width), bf16),
            pltpu.VMEM((rows_here, model_width), bf16),
            pltpu.VMEM((model_width,), f32),
            pltpu.VMEM((rows_here, model_width), bf16),
            pltpu.SemaphoreType.DMA((2, 4)),
            pltpu.SemaphoreType.DMA((3,)),
        ],
        compiler_params=params(24),
        name="module",
    )(
        where,
        mine,
        other,
        near_rows,
        far_rows,
        taps,
        taps_other,
        meta,
        *far(out_weight, resid, ffn_gain),
    )

    hidden_width = w_gate.shape[2]
    near_count = sp_count // 2
    far_count = sp_count - near_count
    mid = near_count + far_count // 2

    x1_in = exchange(outgoing[near_count:mid], near_count)
    near_in = exchange(outgoing[:near_count], 0)
    x2_in = exchange(outgoing[mid:], mid)
    gate_in_hbm, _ = lax.optimization_barrier((w_gate, outgoing[0]))
    weights = pl.pallas_call(
        fetch_kernel,
        out_shape=[pltpu.VMEM(w.shape, bf16) for w in (w_gate, w_up, w_down)],
        in_specs=hbm(3),
        out_specs=vmem(3),
        scratch_shapes=[pltpu.SemaphoreType.DMA((3, 4))],
        compiler_params=params(4),
        cost_estimate=pl.CostEstimate(
            flops=6 * model_width * hidden_width,
            bytes_accessed=6 * model_width * hidden_width,
            transcendentals=0,
        ),
        name="fetch",
    )(*far(gate_in_hbm, w_up, w_down))

    def apply(rows):
        count = len(rows)
        slots = count * 2 * cap
        give = pl.pallas_call(
            pack_kernel,
            out_shape=jax.ShapeDtypeStruct((count * cap, model_width), bf16),
            in_specs=vmem(count),
            out_specs=vmem(1)[0],
            compiler_params=params(8),
            name="pack",
        )(*rows)
        got = lax.ppermute(give, BOTH, swap)
        return pl.pallas_call(
            expert_kernel,
            out_shape=[piece] * count,
            in_specs=vmem(4 + count),
            out_specs=vmem(count),
            scratch_shapes=[
                pltpu.VMEM((slots, model_width), bf16),
                pltpu.VMEM((slots, hidden_width), bf16),
            ],
            compiler_params=params(12),
            cost_estimate=pl.CostEstimate(
                flops=6 * slots * model_width * hidden_width,
                bytes_accessed=6 * model_width * hidden_width,
                transcendentals=slots * hidden_width,
            ),
        )(*weights, got, *rows)

    x1_done = apply(x1_in)
    x1_back = exchange(x1_done, near_count)
    near_done = apply(near_in)
    near_back = exchange(near_done, 0)
    x2_done = apply(x2_in)
    x2_back = exchange(x2_done, mid)
    meta_late, _ = lax.optimization_barrier((meta, x2_done[0]))
    base_own, base_other = pl.pallas_call(
        functools.partial(gather_kernel, *sizes, 0),
        out_shape=[sums] * 2,
        in_specs=smem + vmem(2 + mid),
        out_specs=vmem(2),
        compiler_params=params(16),
        name="gather",
    )(where, meta_late, meta_other, *near_back, *x1_back)

    def last(which, base, m, out):
        return pl.pallas_call(
            functools.partial(last_kernel, *sizes, mid, which),
            out_shape=out,
            in_specs=smem + vmem(2 + sp_count - mid),
            out_specs=vmem(1)[0],
            compiler_params=params(16),
        )(where, m, base, *x2_back)

    other_sum = last(1, base_other, meta_other, tokens)
    other_back = lax.ppermute(other_sum, BOTH, swap)
    meta_last, _ = lax.optimization_barrier((meta, other_sum))
    own = last(0, base_own, meta_last, sums)
    return pl.pallas_call(
        combine_kernel,
        out_shape=tokens,
        in_specs=vmem(3),
        out_specs=vmem(1)[0],
        compiler_params=params(8),
        name="combine",
    )(stream, own, other_back)


def solution(mesh):
    return jax.shard_map(
        per_device,
        mesh=mesh,
        in_specs=(
            P(("sp", "tp"), None),
            P("sp", "tp"),
            P("sp", "tp"),
            P(None, "tp"),
            P("tp"),
            P(),
            P(),
            P(("sp", "tp"), None),
            P(("sp", "tp"), None),
            P(("sp", "tp"), None, None),
            P(("sp", "tp"), None, None),
            P(("sp", "tp"), None, None),
        ),
        out_specs=P(("sp", "tp"), None),
        check_vma=False,
    )
```

time: 135 us -> 139 us (1.030)
  blocking collectives: 110 us -> 0 us
  starting transfers between devices: 6.1 us -> 73.2 us
  waiting for transfers between devices: 0.84 us -> 38.8 us
  Pallas kernels: 16.8 us -> 25.5 us
    all_to_all x2 -> x0, blocking collectives: 110 us -> none  [the longest x1 58.1 us: per_device(): lax.all_to_all(outgoing.reshape(experts, cap, model_width), BOTH, split_a...]
    ppermute x0 -> x35, starting transfers between devices: none -> 67.1 us  [the longest x30 66.8 us: exchange(): moved.append(lax.ppermute(block, 'sp', pairs) if k else block)]
    ppermute x0 -> x35, waiting for transfers between devices: none -> 38.1 us  [the longest x30 37.4 us: exchange(): moved.append(lax.ppermute(block, 'sp', pairs) if k else block)]
    pallas_call x3 -> x12, Pallas kernels: 15.3 us -> 24.1 us  [the longest x3 7.17 us: apply(): pl.pallas_call(expert_kernel, out_shape=[piece] * count, in_specs=vmem(4...]
  transfers between devices with their start and end apart: 4 -> 39, of which waited for: 1 -> 14; matrix products, arithmetic and copies ran while one was open for 0% -> 0% of each run, Pallas kernels for 0% -> 11%
where the time goes in v4:
time: 139 us; the launch traced here: 138 us
  starting transfers between devices  73.2 us (53%)
  waiting for transfers between devices  38.8 us (28%)
  Pallas kernels  25.5 us (18%)
    ppermute x30, starting transfers between devices, exchange(): moved.append(lax.ppermute(block, 'sp', pairs) if k else block)  66.8 us
    ppermute x30, waiting for transfers between devices, exchange(): moved.append(lax.ppermute(block, 'sp', pairs) if k else block)  37.4 us
    pallas_call x3, Pallas kernels, apply(): pl.pallas_call(expert_kernel, out_shape=[piece] * count, in_specs=vmem(4...  7.17 us
    pallas_call x1, Pallas kernels, per_device(): pl.pallas_call(functools.partial(module_kernel, *sizes, sp_count), out_sh...  6.37 us
    ppermute x1, starting transfers between devices, per_device(): near_rows = lax.ppermute(near_rows, BOTH, near)  4.8 us
    pallas_call x1, Pallas kernels, per_device(): pl.pallas_call(fetch_kernel, out_shape=[pltpu.VMEM(w.shape, bf16) for w i...  4.7 us
  transfers between devices with their start and end apart: 39, of which 14 were waited for; matrix products, arithmetic and copies ran while one was open for 0% of the time, Pallas kernels for 11%

profile of v4, /device:TPU:0, one launch (start us, length us, event | category | flops | bytes accessed | tf_op | source)
XLA Modules:
  0.0 137.9 jit_solution(6680170241302256642)
XLA Ops:
  0.0 1.4 %glu.1 = (bf16[144,768]{1,0:T(8,128)(2,1)S(1)}, bf16[144,768]{1,0:T(8,128)(2,1)S(1)}, bf16[16,768]{1,0:T(8,128)(2,1)S(1)}, bf16[16,768]{1,0:T(8,128)(2,1)S(1)}, ...) custom-call(s32[1]{0:T(128)} %bitcast.core_ref, bf16[256,768]{1,0:T(8,128)(2,1)} %value_hbm.1, bf16[256,768]{1,0:T(8,128)(2,1)} %gate_hbm.1, ...), custom_call_target="tpu_custom_call" | custom-call | tf_op jit(solution)/shard_map/glu/pallas_call | solution.py:373
  2.1 4.8 %collective-permute-start.1 = (bf16[16,768]{1,0:T(8,128)(2,1)S(1)}, bf16[16,768]{1,0:T(8,128)(2,1)S(1)}, u32[]{:S(2)}, u32[]{:S(2)}) collective-permute-start(bf16[16,768]{1,0:T(8,128)(2,1)S(1)} %get-tuple-element.54), channel_id=1, source_target_pairs={{0,2},{2,4},{3,1},{4,6},{5,3},{6,8},{7,5},{8,10},{9,7},{10,12},{11... | collective-permute-start | bytes 73736 | tf_op jit(solution)/shard_map/ppermute | solution.py:400
  6.9 0.7 collective-permute-start.2
  7.6 0.8 collective-permute-done.1.near_ref
  8.4 6.4 %module.1 = (bf16[128,2048]{1,0:T(8,128)(2,1)S(1)}, bf16[32,2048]{1,0:T(8,128)(2,1)S(1)}, bf16[32,2048]{1,0:T(8,128)(2,1)S(1)}, bf16[32,2048]{1,0:T(8,128)(2,1)S...) custom-call(s32[2]{0:T(128)S(1)} %pad_add_fusion.where_ref, ...), custom_call_target="tpu_custom_call" | custom-call | tf_op jit(solution)/shard_map/module/pallas_call | solution.py:410
  14.8 5.2 %collective-permute-start.10 = (bf16[32,2048]{1,0:T(8,128)(2,1)S(1)}, bf16[32,2048]{1,0:T(8,128)(2,1)S(1)}, u32[]{:S(2)}, u32[]{:S(2)}) collective-permute-start(bf16[32,2048]{1,0:T(8,128)(2,1)S(1)} %get-tuple-element.70), channel_id=1, source_target_pairs={{0,2},{2,0},{4,6},{6,4},{8,10},{10,8},{12,14},{14,12},{16,18},{18,... | collective-permute-start | bytes 393224 | tf_op jit(solution)/shard_map/ppermute | solution.py:359
  19.9 1.5 %collective-permute-start.11 = (bf16[32,2048]{1,0:T(8,128)(2,1)S(1)}, bf16[32,2048]{1,0:T(8,128)(2,1)S(1)}, u32[]{:S(2)}, u32[]{:S(2)}) collective-permute-start(bf16[32,2048]{1,0:T(8,128)(2,1)S(1)} %get-tuple-element.71), channel_id=1, source_target_pairs={{0,4},{2,6},{4,0},{6,2},{8,12},{10,14},{12,8},{14,10},{16,20},{18,... | collective-permute-start | bytes 393224 | tf_op jit(solution)/shard_map/ppermute | solution.py:359
  21.5 0.9 collective-permute-start.12
  22.3 3.0 %collective-permute-start.13 = (bf16[32,2048]{1,0:T(8,128)(2,1)S(1)}, bf16[32,2048]{1,0:T(8,128)(2,1)S(1)}, u32[]{:S(2)}, u32[]{:S(2)}) collective-permute-start(bf16[32,2048]{1,0:T(8,128)(2,1)S(1)} %get-tuple-element.73), channel_id=1, source_target_pairs={{0,8},{2,10},{4,12},{6,14},{8,0},{10,2},{12,4},{14,6},{16,24},{18,... | collective-permute-start | bytes 393224 | tf_op jit(solution)/shard_map/ppermute | solution.py:359
  25.3 2.1 %collective-permute-start.15 = (bf16[32,2048]{1,0:T(8,128)(2,1)S(1)}, bf16[32,2048]{1,0:T(8,128)(2,1)S(1)}, u32[]{:S(2)}, u32[]{:S(2)}) collective-permute-start(bf16[32,2048]{1,0:T(8,128)(2,1)S(1)} %get-tuple-element.75), channel_id=1, source_target_pairs={{0,12},{2,14},{4,8},{6,10},{8,4},{10,6},{12,0},{14,2},{16,28},{18,... | collective-permute-start | bytes 393224 | tf_op jit(solution)/shard_map/ppermute | solution.py:359
  27.4 0.7 collective-permute-done.11.refs_2_
  28.1 2.1 %collective-permute-start.16 = (bf16[32,2048]{1,0:T(8,128)(2,1)S(1)}, bf16[32,2048]{1,0:T(8,128)(2,1)S(1)}, u32[]{:S(2)}, u32[]{:S(2)}) collective-permute-start(bf16[32,2048]{1,0:T(8,128)(2,1)S(1)} %get-tuple-element.76), channel_id=1, source_target_pairs={{0,14},{2,12},{4,10},{6,8},{8,6},{10,4},{12,2},{14,0},{16,30},{18,... | collective-permute-start | bytes 393224 | tf_op jit(solution)/shard_map/ppermute | solution.py:359
  30.2 2.6 %collective-permute-start.25 = (bf16[32,2048]{1,0:T(8,128)(2,1)S(1)}, bf16[32,2048]{1,0:T(8,128)(2,1)S(1)}, u32[]{:S(2)}, u32[]{:S(2)}) collective-permute-start(bf16[32,2048]{1,0:T(8,128)(2,1)S(1)} %get-tuple-element.85), channel_id=1, source_target_pairs={{0,16},{2,18},{4,20},{6,22},{8,24},{10,26},{12,28},{14,30},{16,0},... | collective-permute-start | bytes 393224 | tf_op jit(solution)/shard_map/ppermute | solution.py:359
  32.8 0.6 collective-permute-start.26
  33.4 4.5 %collective-permute-start.27 = (bf16[32,2048]{1,0:T(8,128)(2,1)S(1)}, bf16[32,2048]{1,0:T(8,128)(2,1)S(1)}, u32[]{:S(2)}, u32[]{:S(2)}) collective-permute-start(bf16[32,2048]{1,0:T(8,128)(2,1)S(1)} %get-tuple-element.87), channel_id=1, source_target_pairs={{0,20},{2,22},{4,16},{6,18},{8,28},{10,30},{12,24},{14,26},{16,4},... | collective-permute-start | bytes 393224 | tf_op jit(solution)/shard_map/ppermute | solution.py:359
  37.9 3.5 %collective-permute-done.15.refs_6_ = bf16[32,2048]{1,0:T(8,128)(2,1)S(1)} collective-permute-done((bf16[32,2048]{1,0:T(8,128)(2,1)S(1)}, bf16[32,2048]{1,0:T(8,128)(2,1)S(1)}, u32[]{:S(2)}, u32[]{:S(2)}) %collective-permute-start.15) | collective-permute-done | bytes 131104 | tf_op jit(solution)/shard_map/ppermute | solution.py:359
  41.9 1.4 %collective-permute-done.16.refs_7_ = bf16[32,2048]{1,0:T(8,128)(2,1)S(1)} collective-permute-done((bf16[32,2048]{1,0:T(8,128)(2,1)S(1)}, bf16[32,2048]{1,0:T(8,128)(2,1)S(1)}, u32[]{:S(2)}, u32[]{:S(2)}) %collective-permute-start.16) | collective-permute-done | bytes 131104 | tf_op jit(solution)/shard_map/ppermute | solution.py:359
  43.4 9.3 %collective-permute-start.5 = (bf16[32,2048]{1,0:T(8,128)(2,1)S(1)}, bf16[32,2048]{1,0:T(8,128)(2,1)S(1)}, u32[]{:S(2)}, u32[]{:S(2)}) collective-permute-start(bf16[32,2048]{1,0:T(8,128)(2,1)S(1)} %get-tuple-element.64), channel_id=1, source_target_pairs={{0,24},{2,26},{4,28},{6,30},{8,16},{10,18},{12,20},{14,22},{16,8},... | collective-permute-start | bytes 393224 | tf_op jit(solution)/shard_map/ppermute | solution.py:359
  53.2 3.9 %collective-permute-done.27.refs_2_ = bf16[32,2048]{1,0:T(8,128)(2,1)S(1)} collective-permute-done((bf16[32,2048]{1,0:T(8,128)(2,1)S(1)}, bf16[32,2048]{1,0:T(8,128)(2,1)S(1)}, u32[]{:S(2)}, u32[]{:S(2)}) %collective-permute-start.27) | collective-permute-done | bytes 131104 | tf_op jit(solution)/shard_map/ppermute | solution.py:359
  57.1 3.2 %collective-permute-done.28.refs_3_ = bf16[32,2048]{1,0:T(8,128)(2,1)S(1)} collective-permute-done((bf16[32,2048]{1,0:T(8,128)(2,1)S(1)}, bf16[32,2048]{1,0:T(8,128)(2,1)S(1)}, u32[]{:S(2)}, u32[]{:S(2)}) %collective-permute-start.28) | collective-permute-done | bytes 131104 | tf_op jit(solution)/shard_map/ppermute | solution.py:359
  60.5 2.5 %collective-permute-start.6 = (bf16[32,2048]{1,0:T(8,128)(2,1)S(1)}, bf16[32,2048]{1,0:T(8,128)(2,1)S(1)}, u32[]{:S(2)}, u32[]{:S(2)}) collective-permute-start(bf16[32,2048]{1,0:T(8,128)(2,1)S(1)} %get-tuple-element.65), channel_id=1, source_target_pairs={{0,26},{2,24},{4,30},{6,28},{8,18},{10,16},{12,22},{14,20},{16,10}... | collective-permute-start | bytes 393224 | tf_op jit(solution)/shard_map/ppermute | solution.py:359
  63.0 1.8 %collective-permute-start.7 = (bf16[32,2048]{1,0:T(8,128)(2,1)S(1)}, bf16[32,2048]{1,0:T(8,128)(2,1)S(1)}, u32[]{:S(2)}, u32[]{:S(2)}) collective-permute-start(bf16[32,2048]{1,0:T(8,128)(2,1)S(1)} %get-tuple-element.66), channel_id=1, source_target_pairs={{0,28},{2,30},{4,24},{6,26},{8,20},{10,22},{12,16},{14,18},{16,12}... | collective-permute-start | bytes 393224 | tf_op jit(solution)/shard_map/ppermute | solution.py:359
  64.8 3.1 %collective-permute-start.8 = (bf16[32,2048]{1,0:T(8,128)(2,1)S(1)}, bf16[32,2048]{1,0:T(8,128)(2,1)S(1)}, u32[]{:S(2)}, u32[]{:S(2)}) collective-permute-start(bf16[32,2048]{1,0:T(8,128)(2,1)S(1)} %get-tuple-element.67), channel_id=1, source_target_pairs={{0,30},{2,28},{4,26},{6,24},{8,22},{10,20},{12,18},{14,16},{16,14}... | collective-permute-start | bytes 393224 | tf_op jit(solution)/shard_map/ppermute | solution.py:359
  67.9 4.7 %fetch.1 = (bf16[1,2048,1024]{2,1,0:T(8,128)(2,1)S(1)}, bf16[1,2048,1024]{2,1,0:T(8,128)(2,1)S(1)}, bf16[1,1024,2048]{2,1,0:T(8,128)(2,1)S(1)}) custom-call(bf16[1,2048,1024]{2,1,0:T(8,128)(2,1)} %gate_hbm.2, bf16[1,2048,1024]{2,1,0:T(8,128)(2,1)} %up_hbm.1, bf16[1,1024,2048]{2,1,0:T(8,128)(2,1)} %down_hbm.1), custom_call_target="tpu_custom_call" | custom-call | flops 12582912 | bytes 12582912 | tf_op jit(solution)/shard_map/fetch/pallas_call | solution.py:448
  72.7 2.8 %collective-permute-done.8.refs_3_ = bf16[32,2048]{1,0:T(8,128)(2,1)S(1)} collective-permute-done((bf16[32,2048]{1,0:T(8,128)(2,1)S(1)}, bf16[32,2048]{1,0:T(8,128)(2,1)S(1)}, u32[]{:S(2)}, u32[]{:S(2)}) %collective-permute-start.8) | collective-permute-done | bytes 131104 | tf_op jit(solution)/shard_map/ppermute | solution.py:359
  75.6 1.9 %shard_map.120 = (bf16[32,2048]{1,0:T(8,128)(2,1)S(1)}, bf16[32,2048]{1,0:T(8,128)(2,1)S(1)}, bf16[32,2048]{1,0:T(8,128)(2,1)S(1)}, bf16[32,2048]{1,0:T(8,128)(2,1)S(1)}) custom-call(bf16[1,2048,1024]{2,1,0:T(8,128)(2,1)S(1)} %get-tuple-element.61.gate_ref, bf16[1,2048,1024]{2,1,0:T(8,128)(2,1)S(1)} %get-tuple-element.62.up_ref, ...), custom_call_target="tpu_custom_call" | custom-call | flops 1610612736 | bytes 12582912 | tf_op jit(solution)/shard_map/pallas_call | solution.py:475
  77.5 4.4 %collective-permute-start.30 = (bf16[32,2048]{1,0:T(8,128)(2,1)S(1)}, bf16[32,2048]{1,0:T(8,128)(2,1)S(1)}, u32[]{:S(2)}, u32[]{:S(2)}) collective-permute-start(bf16[32,2048]{1,0:T(8,128)(2,1)S(1)} %get-tuple-element.89), channel_id=1, source_target_pairs={{0,16},{2,18},{4,20},{6,22},{8,24},{10,26},{12,28},{14,30},{16,0},... | collective-permute-start | bytes 393224 | tf_op jit(solution)/shard_map/ppermute | solution.py:359
  82.0 1.0 collective-permute-start.31
  83.0 3.6 %collective-permute-start.32 = (bf16[32,2048]{1,0:T(8,128)(2,1)S(1)}, bf16[32,2048]{1,0:T(8,128)(2,1)S(1)}, u32[]{:S(2)}, u32[]{:S(2)}) collective-permute-start(bf16[32,2048]{1,0:T(8,128)(2,1)S(1)} %get-tuple-element.91), channel_id=1, source_target_pairs={{0,20},{2,22},{4,16},{6,18},{8,28},{10,30},{12,24},{14,26},{16,4},... | collective-permute-start | bytes 393224 | tf_op jit(solution)/shard_map/ppermute | solution.py:359
  86.6 3.5 %shard_map.119 = (bf16[32,2048]{1,0:T(8,128)(2,1)S(1)}, bf16[32,2048]{1,0:T(8,128)(2,1)S(1)}, bf16[32,2048]{1,0:T(8,128)(2,1)S(1)}, bf16[32,2048]{1,0:T(8,128)(2...) custom-call(bf16[1,2048,1024]{2,1,0:T(8,128)(2,1)S(1)} %get-tuple-el, ...), custom_call_target="tpu_custom_call" | custom-call | flops 3221225472 | bytes 12582912 | tf_op jit(solution)/shard_map/pallas_call | solution.py:475
  90.3 1.5 %collective-permute-start.18 = (bf16[32,2048]{1,0:T(8,128)(2,1)S(1)}, bf16[32,2048]{1,0:T(8,128)(2,1)S(1)}, u32[]{:S(2)}, u32[]{:S(2)}) collective-permute-start(bf16[32,2048]{1,0:T(8,128)(2,1)S(1)} %get-tuple-element.78), channel_id=1, source_target_pairs={{0,2},{2,0},{4,6},{6,4},{8,10},{10,8},{12,14},{14,12},{16,18},{18,... | collective-permute-start | bytes 393224 | tf_op jit(solution)/shard_map/ppermute | solution.py:359
  91.8 5.7 %collective-permute-done.30.refs_8_ = bf16[32,2048]{1,0:T(8,128)(2,1)S(1)} collective-permute-done((bf16[32,2048]{1,0:T(8,128)(2,1)S(1)}, bf16[32,2048]{1,0:T(8,128)(2,1)S(1)}, u32[]{:S(2)}, u32[]{:S(2)}) %collective-permute-start.30) | collective-permute-done | bytes 131104 | tf_op jit(solution)/shard_map/ppermute | solution.py:359
  97.5 3.8 %collective-permute-done.31.refs_9_ = bf16[32,2048]{1,0:T(8,128)(2,1)S(1)} collective-permute-done((bf16[32,2048]{1,0:T(8,128)(2,1)S(1)}, bf16[32,2048]{1,0:T(8,128)(2,1)S(1)}, u32[]{:S(2)}, u32[]{:S(2)}) %collective-permute-start.31) | collective-permute-done | bytes 131104 | tf_op jit(solution)/shard_map/ppermute | solution.py:359
  101.3 1.1 collective-permute-start.20
  102.4 1.4 %collective-permute-done.32.refs_10_ = bf16[32,2048]{1,0:T(8,128)(2,1)S(1)} collective-permute-done((bf16[32,2048]{1,0:T(8,128)(2,1)S(1)}, bf16[32,2048]{1,0:T(8,128)(2,1)S(1)}, u32[]{:S(2)}, u32[]{:S(2)}) %collective-permute-start.32) | collective-permute-done | bytes 131104 | tf_op jit(solution)/shard_map/ppermute | solution.py:359
  103.9 3.8 %collective-permute-done.33.refs_11_ = bf16[32,2048]{1,0:T(8,128)(2,1)S(1)} collective-permute-done((bf16[32,2048]{1,0:T(8,128)(2,1)S(1)}, bf16[32,2048]{1,0:T(8,128)(2,1)S(1)}, u32[]{:S(2)}, u32[]{:S(2)}) %collective-permute-start.33) | collective-permute-done | bytes 131104 | tf_op jit(solution)/shard_map/ppermute | solution.py:359
  107.7 2.1 %collective-permute-start.23 = (bf16[32,2048]{1,0:T(8,128)(2,1)S(1)}, bf16[32,2048]{1,0:T(8,128)(2,1)S(1)}, u32[]{:S(2)}, u32[]{:S(2)}) collective-permute-start(bf16[32,2048]{1,0:T(8,128)(2,1)S(1)} %get-tuple-element.83), channel_id=1, source_target_pairs={{0,12},{2,14},{4,8},{6,10},{8,4},{10,6},{12,0},{14,2},{16,28},{18,... | collective-permute-start | bytes 393224 | tf_op jit(solution)/shard_map/ppermute | solution.py:359
  109.9 1.9 %shard_map.118 = (bf16[32,2048]{1,0:T(8,128)(2,1)S(1)}, bf16[32,2048]{1,0:T(8,128)(2,1)S(1)}, bf16[32,2048]{1,0:T(8,128)(2,1)S(1)}, bf16[32,2048]{1,0:T(8,128)(2,1)S(1)}) custom-call(bf16[1,2048,1024]{2,1,0:T(8,128)(2,1)S(1)} %get-tuple-element.61.gate_ref, bf16[1,2048,1024]{2,1,0:T(8,128)(2,1)S(1)} %get-tuple-element.62.up_ref, ...), custom_call_target="tpu_custom_call" | custom-call | flops 1610612736 | bytes 12582912 | tf_op jit(solution)/shard_map/pallas_call | solution.py:475
  111.7 2.4 %collective-permute-start.34 = (bf16[32,2048]{1,0:T(8,128)(2,1)S(1)}, bf16[32,2048]{1,0:T(8,128)(2,1)S(1)}, u32[]{:S(2)}, u32[]{:S(2)}) collective-permute-start(bf16[32,2048]{1,0:T(8,128)(2,1)S(1)} %get-tuple-element.68), channel_id=1, source_target_pairs={{0,24},{2,26},{4,28},{6,30},{8,16},{10,18},{12,20},{14,22},{16,8},... | collective-permute-start | bytes 393224 | tf_op jit(solution)/shard_map/ppermute | solution.py:359
  114.7 1.9 %collective-permute-start.35 = (bf16[32,2048]{1,0:T(8,128)(2,1)S(1)}, bf16[32,2048]{1,0:T(8,128)(2,1)S(1)}, u32[]{:S(2)}, u32[]{:S(2)}) collective-permute-start(bf16[32,2048]{1,0:T(8,128)(2,1)S(1)} %get-tuple-element.94), channel_id=1, source_target_pairs={{0,26},{2,24},{4,30},{6,28},{8,18},{10,16},{12,22},{14,20},{16,10}... | collective-permute-start | bytes 393224 | tf_op jit(solution)/shard_map/ppermute | solution.py:359
  116.7 3.4 %collective-permute-start.36 = (bf16[32,2048]{1,0:T(8,128)(2,1)S(1)}, bf16[32,2048]{1,0:T(8,128)(2,1)S(1)}, u32[]{:S(2)}, u32[]{:S(2)}) collective-permute-start(bf16[32,2048]{1,0:T(8,128)(2,1)S(1)} %get-tuple-element.95), channel_id=1, source_target_pairs={{0,28},{2,30},{4,24},{6,26},{8,20},{10,22},{12,16},{14,18},{16,12}... | collective-permute-start | bytes 393224 | tf_op jit(solution)/shard_map/ppermute | solution.py:359
  120.1 4.7 %collective-permute-start.37 = (bf16[32,2048]{1,0:T(8,128)(2,1)S(1)}, bf16[32,2048]{1,0:T(8,128)(2,1)S(1)}, u32[]{:S(2)}, u32[]{:S(2)}) collective-permute-start(bf16[32,2048]{1,0:T(8,128)(2,1)S(1)} %get-tuple-element.96), channel_id=1, source_target_pairs={{0,30},{2,28},{4,26},{6,24},{8,22},{10,20},{12,18},{14,16},{16,14}... | collective-permute-start | bytes 393224 | tf_op jit(solution)/shard_map/ppermute | solution.py:359
  124.8 6.5 %collective-permute-done.24.refs_7_ = bf16[32,2048]{1,0:T(8,128)(2,1)S(1)} collective-permute-done((bf16[32,2048]{1,0:T(8,128)(2,1)S(1)}, bf16[32,2048]{1,0:T(8,128)(2,1)S(1)}, u32[]{:S(2)}, u32[]{:S(2)}) %collective-permute-start.24) | collective-permute-done | bytes 131104 | tf_op jit(solution)/shard_map/ppermute | solution.py:359
  131.3 2.3 %gather.1 = (f32[128,2048]{1,0:T(8,128)S(1)}, f32[128,2048]{1,0:T(8,128)S(1)}) custom-call(s32[2]{0:T(128)S(1)} %pad_add_fusion.where_ref, f32[4,128]{1,0:T(4,128)S(1)} %get-tuple-element.97.meta_ref, f32[4,128]{1,0:T(4,128)S(1)} %collective-permute-done.4.meta_other_ref.meta_ref, bf16[32,2048]{1,0:T(8,128)(2,1)S(1)} %get-tuple-element.77.refs_0_, ...), custom_call_target="tpu_custom_call" | custom-call | tf_op jit(solution)/shard_map/gather/pallas_call | solution.py:499
  133.7 1.2 shard_map.121
  135.0 1.2 shard_map.122.own_ref
  136.2 0.7 collective-permute-done.38.other_ref
  136.9 1.0 combine.1
  (44 shorter events, 3.0 us)
Async XLA Ops:
  1.4 7.0 %collective-permute-start = (bf16[144,768]{1,0:T(8,128)(2,1)S(1)}, bf16[144,768]{1,0:T(8,128)(2,1)S(1)}, u32[]{:S(2)}, u32[]{:S(2)}) collective-permute-start(bf16[144,768]{1,0:T(8,128)(2,1)S(1)} %get-tuple-element.53), channel_id=1, source_target_pairs={{0,1},{1,0},{2,3},{3,2},{4,5},{5,4},{6,7},{7,6},{8,9},{9,8},{10,11... | collective-permute-start | bytes 663560 | tf_op jit(solution)/shard_map/ppermute | solution.py:398
  2.0 6.4 %collective-permute-start.3 = (f32[32,768]{1,0:T(8,128)S(1)}, f32[32,768]{1,0:T(8,128)S(1)}, u32[]{:S(2)}, u32[]{:S(2)}) collective-permute-start(f32[32,768]{1,0:T(8,128)S(1)} %get-tuple-element.56.taps_ref), channel_id=1, source_target_pairs={{0,1},{1,0},{2,3},{3,2},{4,5},{5,4},{6,7},{7,6},{8,9},{9,8},{10,11... | collective-permute-start | bytes 294920 | tf_op jit(solution)/shard_map/ppermute | solution.py:399
  2.1 6.3 %collective-permute-start.1 = (bf16[16,768]{1,0:T(8,128)(2,1)S(1)}, bf16[16,768]{1,0:T(8,128)(2,1)S(1)}, u32[]{:S(2)}, u32[]{:S(2)}) collective-permute-start(bf16[16,768]{1,0:T(8,128)(2,1)S(1)} %get-tuple-element.54), channel_id=1, source_target_pairs={{0,2},{2,4},{3,1},{4,6},{5,3},{6,8},{7,5},{8,10},{9,7},{10,12},{11... | collective-permute-start | bytes 73736 | tf_op jit(solution)/shard_map/ppermute | solution.py:400
  6.9 1.5 %collective-permute-start.2 = (bf16[16,768]{1,0:T(8,128)(2,1)S(1)}, bf16[16,768]{1,0:T(8,128)(2,1)S(1)}, u32[]{:S(2)}, u32[]{:S(2)}) collective-permute-start(bf16[16,768]{1,0:T(8,128)(2,1)S(1)} %get-tuple-element.55), channel_id=1, source_target_pairs={{1,2},{3,4},{2,1},{5,6},{4,3},{7,8},{6,5},{9,10},{8,7},{11,12},{10... | collective-permute-start | bytes 73736 | tf_op jit(solution)/shard_map/ppermute | solution.py:401
  14.8 10.6 %collective-permute-start.10 = (bf16[32,2048]{1,0:T(8,128)(2,1)S(1)}, bf16[32,2048]{1,0:T(8,128)(2,1)S(1)}, u32[]{:S(2)}, u32[]{:S(2)}) collective-permute-start(bf16[32,2048]{1,0:T(8,128)(2,1)S(1)} %get-tuple-element.70), channel_id=1, source_target_pairs={{0,2},{2,0},{4,6},{6,4},{8,10},{10,8},{12,14},{14,12},{16,18},{18,... | collective-permute-start | bytes 393224 | tf_op jit(solution)/shard_map/ppermute | solution.py:359
  19.9 8.1 %collective-permute-start.11 = (bf16[32,2048]{1,0:T(8,128)(2,1)S(1)}, bf16[32,2048]{1,0:T(8,128)(2,1)S(1)}, u32[]{:S(2)}, u32[]{:S(2)}) collective-permute-start(bf16[32,2048]{1,0:T(8,128)(2,1)S(1)} %get-tuple-element.71), channel_id=1, source_target_pairs={{0,4},{2,6},{4,0},{6,2},{8,12},{10,14},{12,8},{14,10},{16,20},{18,... | collective-permute-start | bytes 393224 | tf_op jit(solution)/shard_map/ppermute | solution.py:359
  21.5 8.7 %collective-permute-start.12 = (bf16[32,2048]{1,0:T(8,128)(2,1)S(1)}, bf16[32,2048]{1,0:T(8,128)(2,1)S(1)}, u32[]{:S(2)}, u32[]{:S(2)}) collective-permute-start(bf16[32,2048]{1,0:T(8,128)(2,1)S(1)} %get-tuple-element.72), channel_id=1, source_target_pairs={{0,6},{2,4},{4,2},{6,0},{8,14},{10,12},{12,10},{14,8},{16,22},{18,... | collective-permute-start | bytes 393224 | tf_op jit(solution)/shard_map/ppermute | solution.py:359
  22.3 10.4 %collective-permute-start.13 = (bf16[32,2048]{1,0:T(8,128)(2,1)S(1)}, bf16[32,2048]{1,0:T(8,128)(2,1)S(1)}, u32[]{:S(2)}, u32[]{:S(2)}) collective-permute-start(bf16[32,2048]{1,0:T(8,128)(2,1)S(1)} %get-tuple-element.73), channel_id=1, source_target_pairs={{0,8},{2,10},{4,12},{6,14},{8,0},{10,2},{12,4},{14,6},{16,24},{18,... | collective-permute-start | bytes 393224 | tf_op jit(solution)/shard_map/ppermute | solution.py:359
  25.3 8.1 %collective-permute-start.14 = (bf16[32,2048]{1,0:T(8,128)(2,1)S(1)}, bf16[32,2048]{1,0:T(8,128)(2,1)S(1)}, u32[]{:S(2)}, u32[]{:S(2)}) collective-permute-start(bf16[32,2048]{1,0:T(8,128)(2,1)S(1)} %get-tuple-element.74), channel_id=1, source_target_pairs={{0,10},{2,8},{4,14},{6,12},{8,2},{10,0},{12,6},{14,4},{16,26},{18,... | collective-permute-start | bytes 393224 | tf_op jit(solution)/shard_map/ppermute | solution.py:359
  25.3 16.1 %collective-permute-start.15 = (bf16[32,2048]{1,0:T(8,128)(2,1)S(1)}, bf16[32,2048]{1,0:T(8,128)(2,1)S(1)}, u32[]{:S(2)}, u32[]{:S(2)}) collective-permute-start(bf16[32,2048]{1,0:T(8,128)(2,1)S(1)} %get-tuple-element.75), channel_id=1, source_target_pairs={{0,12},{2,14},{4,8},{6,10},{8,4},{10,6},{12,0},{14,2},{16,28},{18,... | collective-permute-start | bytes 393224 | tf_op jit(solution)/shard_map/ppermute | solution.py:359
  28.1 15.2 %collective-permute-start.16 = (bf16[32,2048]{1,0:T(8,128)(2,1)S(1)}, bf16[32,2048]{1,0:T(8,128)(2,1)S(1)}, u32[]{:S(2)}, u32[]{:S(2)}) collective-permute-start(bf16[32,2048]{1,0:T(8,128)(2,1)S(1)} %get-tuple-element.76), channel_id=1, source_target_pairs={{0,14},{2,12},{4,10},{6,8},{8,6},{10,4},{12,2},{14,0},{16,30},{18,... | collective-permute-start | bytes 393224 | tf_op jit(solution)/shard_map/ppermute | solution.py:359
  30.2 13.2 %collective-permute-start.25 = (bf16[32,2048]{1,0:T(8,128)(2,1)S(1)}, bf16[32,2048]{1,0:T(8,128)(2,1)S(1)}, u32[]{:S(2)}, u32[]{:S(2)}) collective-permute-start(bf16[32,2048]{1,0:T(8,128)(2,1)S(1)} %get-tuple-element.85), channel_id=1, source_target_pairs={{0,16},{2,18},{4,20},{6,22},{8,24},{10,26},{12,28},{14,30},{16,0},... | collective-permute-start | bytes 393224 | tf_op jit(solution)/shard_map/ppermute | solution.py:359
  32.8 20.4 %collective-permute-start.26 = (bf16[32,2048]{1,0:T(8,128)(2,1)S(1)}, bf16[32,2048]{1,0:T(8,128)(2,1)S(1)}, u32[]{:S(2)}, u32[]{:S(2)}) collective-permute-start(bf16[32,2048]{1,0:T(8,128)(2,1)S(1)} %get-tuple-element.86), channel_id=1, source_target_pairs={{0,18},{2,16},{4,22},{6,20},{8,26},{10,24},{12,30},{14,28},{16,2},... | collective-permute-start | bytes 393224 | tf_op jit(solution)/shard_map/ppermute | solution.py:359
  33.4 23.7 %collective-permute-start.27 = (bf16[32,2048]{1,0:T(8,128)(2,1)S(1)}, bf16[32,2048]{1,0:T(8,128)(2,1)S(1)}, u32[]{:S(2)}, u32[]{:S(2)}) collective-permute-start(bf16[32,2048]{1,0:T(8,128)(2,1)S(1)} %get-tuple-element.87), channel_id=1, source_target_pairs={{0,20},{2,22},{4,16},{6,18},{8,28},{10,30},{12,24},{14,26},{16,4},... | collective-permute-start | bytes 393224 | tf_op jit(solution)/shard_map/ppermute | solution.py:359
  41.4 19.0 %collective-permute-start.28 = (bf16[32,2048]{1,0:T(8,128)(2,1)S(1)}, bf16[32,2048]{1,0:T(8,128)(2,1)S(1)}, u32[]{:S(2)}, u32[]{:S(2)}) collective-permute-start(bf16[32,2048]{1,0:T(8,128)(2,1)S(1)} %get-tuple-element.88), channel_id=1, source_target_pairs={{0,22},{2,20},{4,18},{6,16},{8,30},{10,28},{12,26},{14,24},{16,6},... | collective-permute-start | bytes 393224 | tf_op jit(solution)/shard_map/ppermute | solution.py:359
  43.3 39.7 %collective-permute-start.17 = (bf16[128,2048]{1,0:T(8,128)(2,1)S(1)}, bf16[128,2048]{1,0:T(8,128)(2,1)S(1)}, u32[]{:S(2)}, u32[]{:S(2)}) collective-permute-start(bf16[128,2048]{1,0:T(8,128)(2,1)S(1)} %pack.4), channel_id=1, source_target_pairs={{0,1},{1,0},{2,3},{3,2},{4,5},{5,4},{6,7},{7,6},{8,9},{9,8},{10,11... | collective-permute-start | bytes 1572872 | tf_op jit(solution)/shard_map/ppermute | solution.py:474
  43.4 21.4 %collective-permute-start.5 = (bf16[32,2048]{1,0:T(8,128)(2,1)S(1)}, bf16[32,2048]{1,0:T(8,128)(2,1)S(1)}, u32[]{:S(2)}, u32[]{:S(2)}) collective-permute-start(bf16[32,2048]{1,0:T(8,128)(2,1)S(1)} %get-tuple-element.64), channel_id=1, source_target_pairs={{0,24},{2,26},{4,28},{6,30},{8,16},{10,18},{12,20},{14,22},{16,8},... | collective-permute-start | bytes 393224 | tf_op jit(solution)/shard_map/ppermute | solution.py:359
  60.4 15.2 %collective-permute-start.29 = (bf16[64,2048]{1,0:T(8,128)(2,1)S(1)}, bf16[64,2048]{1,0:T(8,128)(2,1)S(1)}, u32[]{:S(2)}, u32[]{:S(2)}) collective-permute-start(bf16[64,2048]{1,0:T(8,128)(2,1)S(1)} %pack.5), channel_id=1, source_target_pairs={{0,1},{1,0},{2,3},{3,2},{4,5},{5,4},{6,7},{7,6},{8,9},{9,8},{10,11... | collective-permute-start | bytes 786440 | tf_op jit(solution)/shard_map/ppermute | solution.py:474
  60.5 12.1 %collective-permute-start.6 = (bf16[32,2048]{1,0:T(8,128)(2,1)S(1)}, bf16[32,2048]{1,0:T(8,128)(2,1)S(1)}, u32[]{:S(2)}, u32[]{:S(2)}) collective-permute-start(bf16[32,2048]{1,0:T(8,128)(2,1)S(1)} %get-tuple-element.65), channel_id=1, source_target_pairs={{0,26},{2,24},{4,30},{6,28},{8,18},{10,16},{12,22},{14,20},{16,10}... | collective-permute-start | bytes 393224 | tf_op jit(solution)/shard_map/ppermute | solution.py:359
  63.0 9.7 %collective-permute-start.7 = (bf16[32,2048]{1,0:T(8,128)(2,1)S(1)}, bf16[32,2048]{1,0:T(8,128)(2,1)S(1)}, u32[]{:S(2)}, u32[]{:S(2)}) collective-permute-start(bf16[32,2048]{1,0:T(8,128)(2,1)S(1)} %get-tuple-element.66), channel_id=1, source_target_pairs={{0,28},{2,30},{4,24},{6,26},{8,20},{10,22},{12,16},{14,18},{16,12}... | collective-permute-start | bytes 393224 | tf_op jit(solution)/shard_map/ppermute | solution.py:359
  64.8 10.7 %collective-permute-start.8 = (bf16[32,2048]{1,0:T(8,128)(2,1)S(1)}, bf16[32,2048]{1,0:T(8,128)(2,1)S(1)}, u32[]{:S(2)}, u32[]{:S(2)}) collective-permute-start(bf16[32,2048]{1,0:T(8,128)(2,1)S(1)} %get-tuple-element.67), channel_id=1, source_target_pairs={{0,30},{2,28},{4,26},{6,24},{8,22},{10,20},{12,18},{14,16},{16,14}... | collective-permute-start | bytes 393224 | tf_op jit(solution)/shard_map/ppermute | solution.py:359
  72.6 17.4 %collective-permute-start.4 = (f32[4,128]{1,0:T(4,128)S(1)}, f32[4,128]{1,0:T(4,128)S(1)}, u32[]{:S(2)}, u32[]{:S(2)}) collective-permute-start(f32[4,128]{1,0:T(4,128)S(1)} %get-tuple-element.97.meta_ref), channel_id=1, source_target_pairs={{0,1},{1,0},{2,3},{3,2},{4,5},{5,4},{6,7},{7,6},{8,9},{9,8},{10,11... | collective-permute-start | bytes 6152 | tf_op jit(solution)/shard_map/ppermute | solution.py:402
  75.6 14.8 %collective-permute-start.9 = (bf16[64,2048]{1,0:T(8,128)(2,1)S(1)}, bf16[64,2048]{1,0:T(8,128)(2,1)S(1)}, u32[]{:S(2)}, u32[]{:S(2)}) collective-permute-start(bf16[64,2048]{1,0:T(8,128)(2,1)S(1)} %pack.3), channel_id=1, source_target_pairs={{0,1},{1,0},{2,3},{3,2},{4,5},{5,4},{6,7},{7,6},{8,9},{9,8},{10,11... | collective-permute-start | bytes 786440 | tf_op jit(solution)/shard_map/ppermute | solution.py:474
  77.5 20.0 %collective-permute-start.30 = (bf16[32,2048]{1,0:T(8,128)(2,1)S(1)}, bf16[32,2048]{1,0:T(8,128)(2,1)S(1)}, u32[]{:S(2)}, u32[]{:S(2)}) collective-permute-start(bf16[32,2048]{1,0:T(8,128)(2,1)S(1)} %get-tuple-element.89), channel_id=1, source_target_pairs={{0,16},{2,18},{4,20},{6,22},{8,24},{10,26},{12,28},{14,30},{16,0},... | collective-permute-start | bytes 393224 | tf_op jit(solution)/shard_map/ppermute | solution.py:359
  82.0 19.4 %collective-permute-start.31 = (bf16[32,2048]{1,0:T(8,128)(2,1)S(1)}, bf16[32,2048]{1,0:T(8,128)(2,1)S(1)}, u32[]{:S(2)}, u32[]{:S(2)}) collective-permute-start(bf16[32,2048]{1,0:T(8,128)(2,1)S(1)} %get-tuple-element.90), channel_id=1, source_target_pairs={{0,18},{2,16},{4,22},{6,20},{8,26},{10,24},{12,30},{14,28},{16,2},... | collective-permute-start | bytes 393224 | tf_op jit(solution)/shard_map/ppermute | solution.py:359
  83.0 20.9 %collective-permute-start.32 = (bf16[32,2048]{1,0:T(8,128)(2,1)S(1)}, bf16[32,2048]{1,0:T(8,128)(2,1)S(1)}, u32[]{:S(2)}, u32[]{:S(2)}) collective-permute-start(bf16[32,2048]{1,0:T(8,128)(2,1)S(1)} %get-tuple-element.91), channel_id=1, source_target_pairs={{0,20},{2,22},{4,16},{6,18},{8,28},{10,30},{12,24},{14,26},{16,4},... | collective-permute-start | bytes 393224 | tf_op jit(solution)/shard_map/ppermute | solution.py:359
  90.1 17.7 %collective-permute-start.33 = (bf16[32,2048]{1,0:T(8,128)(2,1)S(1)}, bf16[32,2048]{1,0:T(8,128)(2,1)S(1)}, u32[]{:S(2)}, u32[]{:S(2)}) collective-permute-start(bf16[32,2048]{1,0:T(8,128)(2,1)S(1)} %get-tuple-element.92), channel_id=1, source_target_pairs={{0,22},{2,20},{4,18},{6,16},{8,30},{10,28},{12,26},{14,24},{16,6},... | collective-permute-start | bytes 393224 | tf_op jit(solution)/shard_map/ppermute | solution.py:359
  90.3 17.4 %collective-permute-start.18 = (bf16[32,2048]{1,0:T(8,128)(2,1)S(1)}, bf16[32,2048]{1,0:T(8,128)(2,1)S(1)}, u32[]{:S(2)}, u32[]{:S(2)}) collective-permute-start(bf16[32,2048]{1,0:T(8,128)(2,1)S(1)} %get-tuple-element.78), channel_id=1, source_target_pairs={{0,2},{2,0},{4,6},{6,4},{8,10},{10,8},{12,14},{14,12},{16,18},{18,... | collective-permute-start | bytes 393224 | tf_op jit(solution)/shard_map/ppermute | solution.py:359
  97.5 14.2 %collective-permute-start.19 = (bf16[32,2048]{1,0:T(8,128)(2,1)S(1)}, bf16[32,2048]{1,0:T(8,128)(2,1)S(1)}, u32[]{:S(2)}, u32[]{:S(2)}) collective-permute-start(bf16[32,2048]{1,0:T(8,128)(2,1)S(1)} %get-tuple-element.79), channel_id=1, source_target_pairs={{0,4},{2,6},{4,0},{6,2},{8,12},{10,14},{12,8},{14,10},{16,20},{18,... | collective-permute-start | bytes 393224 | tf_op jit(solution)/shard_map/ppermute | solution.py:359
  101.3 12.9 %collective-permute-start.20 = (bf16[32,2048]{1,0:T(8,128)(2,1)S(1)}, bf16[32,2048]{1,0:T(8,128)(2,1)S(1)}, u32[]{:S(2)}, u32[]{:S(2)}) collective-permute-start(bf16[32,2048]{1,0:T(8,128)(2,1)S(1)} %get-tuple-element.80), channel_id=1, source_target_pairs={{0,6},{2,4},{4,2},{6,0},{8,14},{10,12},{12,10},{14,8},{16,22},{18,... | collective-permute-start | bytes 393224 | tf_op jit(solution)/shard_map/ppermute | solution.py:359
  103.9 10.9 %collective-permute-start.21 = (bf16[32,2048]{1,0:T(8,128)(2,1)S(1)}, bf16[32,2048]{1,0:T(8,128)(2,1)S(1)}, u32[]{:S(2)}, u32[]{:S(2)}) collective-permute-start(bf16[32,2048]{1,0:T(8,128)(2,1)S(1)} %get-tuple-element.81), channel_id=1, source_target_pairs={{0,8},{2,10},{4,12},{6,14},{8,0},{10,2},{12,4},{14,6},{16,24},{18,... | collective-permute-start | bytes 393224 | tf_op jit(solution)/shard_map/ppermute | solution.py:359
  107.7 8.9 %collective-permute-start.22 = (bf16[32,2048]{1,0:T(8,128)(2,1)S(1)}, bf16[32,2048]{1,0:T(8,128)(2,1)S(1)}, u32[]{:S(2)}, u32[]{:S(2)}) collective-permute-start(bf16[32,2048]{1,0:T(8,128)(2,1)S(1)} %get-tuple-element.82), channel_id=1, source_target_pairs={{0,10},{2,8},{4,14},{6,12},{8,2},{10,0},{12,6},{14,4},{16,26},{18,... | collective-permute-start | bytes 393224 | tf_op jit(solution)/shard_map/ppermute | solution.py:359
  107.7 12.4 %collective-permute-start.23 = (bf16[32,2048]{1,0:T(8,128)(2,1)S(1)}, bf16[32,2048]{1,0:T(8,128)(2,1)S(1)}, u32[]{:S(2)}, u32[]{:S(2)}) collective-permute-start(bf16[32,2048]{1,0:T(8,128)(2,1)S(1)} %get-tuple-element.83), channel_id=1, source_target_pairs={{0,12},{2,14},{4,8},{6,10},{8,4},{10,6},{12,0},{14,2},{16,28},{18,... | collective-permute-start | bytes 393224 | tf_op jit(solution)/shard_map/ppermute | solution.py:359
  111.7 21.9 %collective-permute-start.34 = (bf16[32,2048]{1,0:T(8,128)(2,1)S(1)}, bf16[32,2048]{1,0:T(8,128)(2,1)S(1)}, u32[]{:S(2)}, u32[]{:S(2)}) collective-permute-start(bf16[32,2048]{1,0:T(8,128)(2,1)S(1)} %get-tuple-element.68), channel_id=1, source_target_pairs={{0,24},{2,26},{4,28},{6,30},{8,16},{10,18},{12,20},{14,22},{16,8},... | collective-permute-start | bytes 393224 | tf_op jit(solution)/shard_map/ppermute | solution.py:359
  114.2 17.1 %collective-permute-start.24 = (bf16[32,2048]{1,0:T(8,128)(2,1)S(1)}, bf16[32,2048]{1,0:T(8,128)(2,1)S(1)}, u32[]{:S(2)}, u32[]{:S(2)}) collective-permute-start(bf16[32,2048]{1,0:T(8,128)(2,1)S(1)} %get-tuple-element.84), channel_id=1, source_target_pairs={{0,14},{2,12},{4,10},{6,8},{8,6},{10,4},{12,2},{14,0},{16,30},{18,... | collective-permute-start | bytes 393224 | tf_op jit(solution)/shard_map/ppermute | solution.py:359
  114.7 18.9 %collective-permute-start.35 = (bf16[32,2048]{1,0:T(8,128)(2,1)S(1)}, bf16[32,2048]{1,0:T(8,128)(2,1)S(1)}, u32[]{:S(2)}, u32[]{:S(2)}) collective-permute-start(bf16[32,2048]{1,0:T(8,128)(2,1)S(1)} %get-tuple-element.94), channel_id=1, source_target_pairs={{0,26},{2,24},{4,30},{6,28},{8,18},{10,16},{12,22},{14,20},{16,10}... | collective-permute-start | bytes 393224 | tf_op jit(solution)/shard_map/ppermute | solution.py:359
  116.7 17.0 %collective-permute-start.36 = (bf16[32,2048]{1,0:T(8,128)(2,1)S(1)}, bf16[32,2048]{1,0:T(8,128)(2,1)S(1)}, u32[]{:S(2)}, u32[]{:S(2)}) collective-permute-start(bf16[32,2048]{1,0:T(8,128)(2,1)S(1)} %get-tuple-element.95), channel_id=1, source_target_pairs={{0,28},{2,30},{4,24},{6,26},{8,20},{10,22},{12,16},{14,18},{16,12}... | collective-permute-start | bytes 393224 | tf_op jit(solution)/shard_map/ppermute | solution.py:359
  120.1 13.6 %collective-permute-start.37 = (bf16[32,2048]{1,0:T(8,128)(2,1)S(1)}, bf16[32,2048]{1,0:T(8,128)(2,1)S(1)}, u32[]{:S(2)}, u32[]{:S(2)}) collective-permute-start(bf16[32,2048]{1,0:T(8,128)(2,1)S(1)} %get-tuple-element.96), channel_id=1, source_target_pairs={{0,30},{2,28},{4,26},{6,24},{8,22},{10,20},{12,18},{14,16},{16,14}... | collective-permute-start | bytes 393224 | tf_op jit(solution)/shard_map/ppermute | solution.py:359
  134.9 2.0 %collective-permute-start.38 = (bf16[128,2048]{1,0:T(8,128)(2,1)S(1)}, bf16[128,2048]{1,0:T(8,128)(2,1)S(1)}, u32[]{:S(2)}, u32[]{:S(2)}) collective-permute-start(bf16[128,2048]{1,0:T(8,128)(2,1)S(1)} %shard_map.121), channel_id=1, source_target_pairs={{0,1},{1,0},{2,3},{3,2},{4,5},{5,4},{6,7},{7,6},{8,9},{9,8},{10,11... | collective-permute-start | bytes 1572872 | tf_op jit(solution)/shard_map/ppermute | solution.py:518

commit v5 on v4

--- a/solution.py
+++ b/solution.py
@@ -135,52 +135,74 @@
     return total
 
 
+def conv_kernel(
+    where_ref,
+    mine_ref,
+    other_ref,
+    taps_ref,
+    taps_other_ref,
+    out_weight_hbm,
+    conv_ref,
+    out_weight_ref,
+    window_ref,
+    weight_sems,
+):
+    core = where_ref[0]
+    inner, half = mine_ref.shape
+    cuts = 4
+    cut = half // cuts
+    copies = []
+    for side in range(2):
+        for n in range(cuts):
+            where = (core + side * (1 - 2 * core)) * half + n * cut
+            copies.append(
+                pltpu.make_async_copy(
+                    out_weight_hbm.at[pl.ds(pl.multiple_of(where, HALO), cut), :],
+                    out_weight_ref.at[side, n * cut : (n + 1) * cut, :],
+                    weight_sems.at[side, n],
+                )
+            )
+            copies[-1].start()
+    rows = conv_ref.shape[1]
+    taps = taps_ref.shape[0] - 1
+    blocks = half // LANES
+    inner_at = pl.multiple_of((1 - core) * HALO, HALO)
+    outer_at = pl.multiple_of(core * inner, HALO)
+    first = HALO - taps // 2
+    for b in range(2 * blocks):
+        source, tap_ref = (mine_ref, taps_ref) if b < blocks else (other_ref, taps_other_ref)
+        lanes = slice((b % blocks) * LANES, (b % blocks + 1) * LANES)
+        window_ref[b, pl.ds(inner_at, inner), :] = source[:, lanes].astype(jnp.float32)
+        window_ref[b, pl.ds(outer_at, HALO), :] = jnp.zeros((HALO, LANES), jnp.float32)
+        conv = jnp.zeros((rows, LANES), jnp.float32)
+        for tap in range(taps):
+            conv = conv + window_ref[b, first + tap : first + tap + rows, :] * tap_ref[tap : tap + 1, lanes]
+        conv_ref[b] = conv
+    for copy in copies:
+        copy.wait()
+
+
 def module_kernel(
     cap,
     experts,
     count,
     where_ref,
-    mine_ref,
-    other_ref,
+    part_ref,
     near_ref,
     far_ref,
     taps_ref,
     taps_other_ref,
     meta_ref,
-    out_weight_hbm,
+    out_weight_ref,
     resid_hbm,
     ffn_gain_hbm,
     stream_hbm,
     *more,
 ):
     outgoing_refs = more[:count]
-    (
-        window_ref,
-        conv_ref,
-        out_weight_ref,
-        resid_ref,
-        ffn_gain_ref,
-        stream_ref,
-        weight_sems,
-        sems,
-    ) = more[count:]
+    edge_ref, conv_ref, resid_ref, ffn_gain_ref, stream_ref, sems = more[count:]
     core = where_ref[0]
-    inner, half = mine_ref.shape
-    cuts = 4
-    cut = half // cuts
-    copies = []
-    for side in range(2):
-        copies.append([])
-        for n in range(cuts):
-            where = (core + side * (1 - 2 * core)) * half + n * cut
-            copies[side].append(
-                pltpu.make_async_copy(
-                    out_weight_hbm.at[pl.ds(pl.multiple_of(where, HALO), cut), :],
-                    out_weight_ref.at[side, n * cut : (n + 1) * cut, :],
-                    weight_sems.at[side, n],
-                )
-            )
-            copies[side][n].start()
+    half = near_ref.shape[1]
     fetch = [
         pltpu.make_async_copy(resid_hbm, resid_ref, sems.at[0]),
         pltpu.make_async_copy(ffn_gain_hbm, ffn_gain_ref, sems.at[1]),
@@ -189,22 +211,26 @@
         copy.start()
     rows = resid_ref.shape[0]
     taps = taps_ref.shape[0] - 1
+    reach = taps // 2
     blocks = half // LANES
-    inner_at = pl.multiple_of((1 - core) * HALO, HALO)
-    outer_at = pl.multiple_of(core * inner, HALO)
-    first = HALO - taps // 2
+    outer_at = pl.multiple_of(core * HALO, HALO)
+    blank_at = pl.multiple_of((1 - core) * HALO, HALO)
+    touched = pl.multiple_of(core * (rows - HALO), HALO)
+    tap_at = pl.multiple_of(core * (taps - reach), 8)
     total = jnp.zeros((rows, LANES), jnp.float32)
     square = jnp.zeros((rows, LANES), jnp.float32)
     for b in range(2 * blocks):
-        sources = (mine_ref, near_ref, taps_ref) if b < blocks else (other_ref, far_ref, taps_other_ref)
-        source, outer, tap_ref = sources
+        outer, tap_ref = (near_ref, taps_ref) if b < blocks else (far_ref, taps_other_ref)
         lanes = slice((b % blocks) * LANES, (b % blocks + 1) * LANES)
-        window_ref[b, pl.ds(inner_at, inner), :] = source[:, lanes].astype(jnp.float32)
-        window_ref[b, pl.ds(outer_at, HALO), :] = outer[:, lanes].astype(jnp.float32)
-        conv = jnp.zeros((rows, LANES), jnp.float32)
-        for tap in range(taps):
-            conv = conv + window_ref[b, first + tap : first + tap + rows, :] * tap_ref[tap : tap + 1, lanes]
-        conv_ref[b] = conv
+        edge_ref[b, pl.ds(outer_at, HALO), :] = outer[:, lanes].astype(jnp.float32)
+        edge_ref[b, pl.ds(blank_at, HALO), :] = jnp.zeros((HALO, LANES), jnp.float32)
+        weights = tap_ref[pl.ds(tap_at, HALO), lanes]
+        conv_ref[b] = part_ref[b]
+        extra = jnp.zeros((HALO, LANES), jnp.float32)
+        for tap in range(reach):
+            extra = extra + edge_ref[b, 1 + tap : 1 + tap + HALO, :] * weights[tap : tap + 1, :]
+        conv_ref[b, pl.ds(touched, HALO), :] += extra
+        conv = conv_ref[b]
         total = total + conv
         square = square + conv * conv
     width = 2 * half
@@ -219,8 +245,6 @@
             v = (conv_ref[side * blocks + b] - mean) * scale * tap_ref[taps : taps + 1, lanes]
             parts.append(jax.nn.silu(v).astype(jnp.bfloat16))
         mixed = jnp.concatenate(parts, axis=1)
-        for copy in copies[side]:
-            copy.wait()
         part = jnp.dot(mixed, out_weight_ref[side], preferred_element_type=jnp.float32)
         proj = part if proj is None else proj + part
     for copy in fetch:
@@ -407,33 +431,51 @@
     sums = jax.ShapeDtypeStruct((rows_here, model_width), f32)
     piece = jax.ShapeDtypeStruct((2 * cap, model_width), bf16)
     sizes = (cap, experts)
+    conv, weight_near = pl.pallas_call(
+        conv_kernel,
+        out_shape=[
+            jax.ShapeDtypeStruct((blocks, rows_here, LANES), f32),
+            pltpu.VMEM((2, half, model_width), bf16),
+        ],
+        in_specs=smem + vmem(4) + hbm(1),
+        out_specs=vmem(2),
+        scratch_shapes=[
+            pltpu.VMEM((blocks, inner + HALO, LANES), f32),
+            pltpu.SemaphoreType.DMA((2, 4)),
+        ],
+        compiler_params=params(8),
+        cost_estimate=pl.CostEstimate(
+            flops=4 * taps_count * rows_here * half,
+            bytes_accessed=8 * rows_here * half,
+            transcendentals=0,
+        ),
+        name="conv",
+    )(where, mine, other, taps, taps_other, *far(out_weight))
     stream, *outgoing = pl.pallas_call(
         functools.partial(module_kernel, *sizes, sp_count),
         out_shape=[tokens] + [piece] * sp_count,
-        in_specs=smem + vmem(7) + hbm(3),
+        in_specs=smem + vmem(7) + hbm(2),
         out_specs=hbm(1) + vmem(sp_count),
         scratch_shapes=[
-            pltpu.VMEM((blocks, inner + HALO, LANES), f32),
+            pltpu.VMEM((blocks, 2 * HALO, LANES), f32),
             pltpu.VMEM((blocks, rows_here, LANES), f32),
-            pltpu.VMEM((2, half, model_width), bf16),
             pltpu.VMEM((rows_here, model_width), bf16),
             pltpu.VMEM((model_width,), f32),
             pltpu.VMEM((rows_here, model_width), bf16),
-            pltpu.SemaphoreType.DMA((2, 4)),
             pltpu.SemaphoreType.DMA((3,)),
         ],
-        compiler_params=params(24),
+        compiler_params=params(16),
         name="module",
     )(
         where,
-        mine,
-        other,
+        conv,
         near_rows,
         far_rows,
         taps,
         taps_other,
         meta,
-        *far(out_weight, resid, ffn_gain),
+        weight_near,
+        *far(resid, ffn_gain),
     )
 
     hidden_width = w_gate.shape[2]

time: 139 us -> 140 us (level)
  waiting for transfers between devices: 38.8 us -> 36.8 us
    pallas_call x0 -> x1, Pallas kernels: none -> 3.41 us  [per_device(): pl.pallas_call(conv_kernel, out_shape=[jax.ShapeDtypeStruct((blocks, rows...]
    pallas_call x1, Pallas kernels: 6.37 us -> 4.06 us  [per_device(): pl.pallas_call(functools.partial(module_kernel, *sizes, sp_count), out_sh...]
  transfers between devices with their start and end apart: 39 -> 39, of which waited for: 14 -> 11; matrix products, arithmetic and copies ran while one was open for 0% -> 0% of each run, Pallas kernels for 11% -> 14%
where the time goes in v5:
time: 140 us; the launch traced here: 138 us
  starting transfers between devices  73.9 us (53%)
  waiting for transfers between devices  36.8 us (26%)
  Pallas kernels  26.6 us (19%)
    ppermute x30, starting transfers between devices, exchange(): moved.append(lax.ppermute(block, 'sp', pairs) if k else block)  67.4 us
    ppermute x30, waiting for transfers between devices, exchange(): moved.append(lax.ppermute(block, 'sp', pairs) if k else block)  36.1 us
    pallas_call x3, Pallas kernels, apply(): pl.pallas_call(expert_kernel, out_shape=[piece] * count, in_specs=vmem(4...  7.2 us
    ppermute x1, starting transfers between devices, per_device(): near_rows = lax.ppermute(near_rows, BOTH, near)  4.8 us
    pallas_call x1, Pallas kernels, per_device(): pl.pallas_call(fetch_kernel, out_shape=[pltpu.VMEM(w.shape, bf16) for w i...  4.7 us
    pallas_call x1, Pallas kernels, per_device(): pl.pallas_call(functools.partial(module_kernel, *sizes, sp_count), out_sh...  4.06 us
    pallas_call x1, Pallas kernels, per_device(): pl.pallas_call(conv_kernel, out_shape=[jax.ShapeDtypeStruct((blocks, rows...  3.41 us
  transfers between devices with their start and end apart: 39, of which 11 were waited for; matrix products, arithmetic and copies ran while one was open for 0% of the time, Pallas kernels for 14%

profile of v5, /device:TPU:0, one launch (start us, length us, event | category | flops | bytes accessed | tf_op | source)
XLA Modules:
  0.0 137.6 jit_solution(2119664522870495002)
XLA Ops:
  0.0 1.4 %glu.1 = (bf16[144,768]{1,0:T(8,128)(2,1)S(1)}, bf16[144,768]{1,0:T(8,128)(2,1)S(1)}, bf16[16,768]{1,0:T(8,128)(2,1)S(1)}, bf16[16,768]{1,0:T(8,128)(2,1)S(1)}, ...) custom-call(s32[1]{0:T(128)} %bitcast.core_ref, bf16[256,768]{1,0:T(8,128)(2,1)} %value_hbm.1, bf16[256,768]{1,0:T(8,128)(2,1)} %gate_hbm.1, ...), custom_call_target="tpu_custom_call" | custom-call | tf_op jit(solution)/shard_map/glu/pallas_call | solution.py:397
  2.1 4.8 %collective-permute-start.2 = (bf16[16,768]{1,0:T(8,128)(2,1)S(1)}, bf16[16,768]{1,0:T(8,128)(2,1)S(1)}, u32[]{:S(2)}, u32[]{:S(2)}) collective-permute-start(bf16[16,768]{1,0:T(8,128)(2,1)S(1)} %get-tuple-element.58), channel_id=1, source_target_pairs={{0,2},{2,4},{3,1},{4,6},{5,3},{6,8},{7,5},{8,10},{9,7},{10,12},{11... | collective-permute-start | bytes 73736 | tf_op jit(solution)/shard_map/ppermute | solution.py:424
  6.9 0.7 collective-permute-start.3
  7.6 3.4 %conv.1 = (f32[12,128,128]{2,1,0:T(8,128)S(1)}, bf16[2,768,2048]{2,1,0:T(8,128)(2,1)S(1)}) custom-call(s32[2]{0:T(128)S(1)} %pad_add_fusion.where_ref, bf16[144,768]{1,0:T(8,128)(2,1)S(1)} %get-tuple-element.54.mine_ref, bf16[144,768]{1,0:T(8,128)(2,1)S(1)} %collective-permute-done.other_ref, f32[32,768]{1,0:T(8,128)S(1)} %get-tuple-element.56.taps_ref, ...), custom_call_target="tpu_custom_call" | custom-call | flops 12189696 | bytes 786432 | tf_op jit(solution)/shard_map/conv/pallas_call | solution.py:434
  11.1 4.1 %module.1 = (bf16[128,2048]{1,0:T(8,128)(2,1)S(1)}, bf16[32,2048]{1,0:T(8,128)(2,1)S(1)}, bf16[32,2048]{1,0:T(8,128)(2,1)S(1)}, bf16[32,2048]{1,0:T(8,128)(2,1)S...) custom-call(s32[2]{0:T(128)S(1)} %pad_add_fusion.where_ref, ...), custom_call_target="tpu_custom_call" | custom-call | tf_op jit(solution)/shard_map/module/pallas_call | solution.py:454
  15.1 2.8 %collective-permute-start.10 = (bf16[32,2048]{1,0:T(8,128)(2,1)S(1)}, bf16[32,2048]{1,0:T(8,128)(2,1)S(1)}, u32[]{:S(2)}, u32[]{:S(2)}) collective-permute-start(bf16[32,2048]{1,0:T(8,128)(2,1)S(1)} %get-tuple-element.74), channel_id=1, source_target_pairs={{0,2},{2,0},{4,6},{6,4},{8,10},{10,8},{12,14},{14,12},{16,18},{18,... | collective-permute-start | bytes 393224 | tf_op jit(solution)/shard_map/ppermute | solution.py:383
  17.9 1.5 %collective-permute-start.11 = (bf16[32,2048]{1,0:T(8,128)(2,1)S(1)}, bf16[32,2048]{1,0:T(8,128)(2,1)S(1)}, u32[]{:S(2)}, u32[]{:S(2)}) collective-permute-start(bf16[32,2048]{1,0:T(8,128)(2,1)S(1)} %get-tuple-element.75), channel_id=1, source_target_pairs={{0,4},{2,6},{4,0},{6,2},{8,12},{10,14},{12,8},{14,10},{16,20},{18,... | collective-permute-start | bytes 393224 | tf_op jit(solution)/shard_map/ppermute | solution.py:383
  20.0 3.0 %collective-permute-start.13 = (bf16[32,2048]{1,0:T(8,128)(2,1)S(1)}, bf16[32,2048]{1,0:T(8,128)(2,1)S(1)}, u32[]{:S(2)}, u32[]{:S(2)}) collective-permute-start(bf16[32,2048]{1,0:T(8,128)(2,1)S(1)} %get-tuple-element.77), channel_id=1, source_target_pairs={{0,8},{2,10},{4,12},{6,14},{8,0},{10,2},{12,4},{14,6},{16,24},{18,... | collective-permute-start | bytes 393224 | tf_op jit(solution)/shard_map/ppermute | solution.py:383
  23.2 2.8 %collective-permute-start.15 = (bf16[32,2048]{1,0:T(8,128)(2,1)S(1)}, bf16[32,2048]{1,0:T(8,128)(2,1)S(1)}, u32[]{:S(2)}, u32[]{:S(2)}) collective-permute-start(bf16[32,2048]{1,0:T(8,128)(2,1)S(1)} %get-tuple-element.79), channel_id=1, source_target_pairs={{0,12},{2,14},{4,8},{6,10},{8,4},{10,6},{12,0},{14,2},{16,28},{18,... | collective-permute-start | bytes 393224 | tf_op jit(solution)/shard_map/ppermute | solution.py:383
  26.1 2.4 %collective-permute-start.16 = (bf16[32,2048]{1,0:T(8,128)(2,1)S(1)}, bf16[32,2048]{1,0:T(8,128)(2,1)S(1)}, u32[]{:S(2)}, u32[]{:S(2)}) collective-permute-start(bf16[32,2048]{1,0:T(8,128)(2,1)S(1)} %get-tuple-element.80), channel_id=1, source_target_pairs={{0,14},{2,12},{4,10},{6,8},{8,6},{10,4},{12,2},{14,0},{16,30},{18,... | collective-permute-start | bytes 393224 | tf_op jit(solution)/shard_map/ppermute | solution.py:383
  28.4 2.2 %collective-permute-start.25 = (bf16[32,2048]{1,0:T(8,128)(2,1)S(1)}, bf16[32,2048]{1,0:T(8,128)(2,1)S(1)}, u32[]{:S(2)}, u32[]{:S(2)}) collective-permute-start(bf16[32,2048]{1,0:T(8,128)(2,1)S(1)} %get-tuple-element.89), channel_id=1, source_target_pairs={{0,16},{2,18},{4,20},{6,22},{8,24},{10,26},{12,28},{14,30},{16,0},... | collective-permute-start | bytes 393224 | tf_op jit(solution)/shard_map/ppermute | solution.py:383
  30.6 2.5 %collective-permute-start.26 = (bf16[32,2048]{1,0:T(8,128)(2,1)S(1)}, bf16[32,2048]{1,0:T(8,128)(2,1)S(1)}, u32[]{:S(2)}, u32[]{:S(2)}) collective-permute-start(bf16[32,2048]{1,0:T(8,128)(2,1)S(1)} %get-tuple-element.90), channel_id=1, source_target_pairs={{0,18},{2,16},{4,22},{6,20},{8,26},{10,24},{12,30},{14,28},{16,2},... | collective-permute-start | bytes 393224 | tf_op jit(solution)/shard_map/ppermute | solution.py:383
  33.1 3.2 %collective-permute-start.27 = (bf16[32,2048]{1,0:T(8,128)(2,1)S(1)}, bf16[32,2048]{1,0:T(8,128)(2,1)S(1)}, u32[]{:S(2)}, u32[]{:S(2)}) collective-permute-start(bf16[32,2048]{1,0:T(8,128)(2,1)S(1)} %get-tuple-element.91), channel_id=1, source_target_pairs={{0,20},{2,22},{4,16},{6,18},{8,28},{10,30},{12,24},{14,26},{16,4},... | collective-permute-start | bytes 393224 | tf_op jit(solution)/shard_map/ppermute | solution.py:383
  36.4 0.7 collective-permute-start.28
  37.1 3.9 %collective-permute-done.16.refs_7_ = bf16[32,2048]{1,0:T(8,128)(2,1)S(1)} collective-permute-done((bf16[32,2048]{1,0:T(8,128)(2,1)S(1)}, bf16[32,2048]{1,0:T(8,128)(2,1)S(1)}, u32[]{:S(2)}, u32[]{:S(2)}) %collective-permute-start.16) | collective-permute-done | bytes 131104 | tf_op jit(solution)/shard_map/ppermute | solution.py:383
  41.2 10.6 %collective-permute-start.5 = (bf16[32,2048]{1,0:T(8,128)(2,1)S(1)}, bf16[32,2048]{1,0:T(8,128)(2,1)S(1)}, u32[]{:S(2)}, u32[]{:S(2)}) collective-permute-start(bf16[32,2048]{1,0:T(8,128)(2,1)S(1)} %get-tuple-element.68), channel_id=1, source_target_pairs={{0,24},{2,26},{4,28},{6,30},{8,16},{10,18},{12,20},{14,22},{16,8},... | collective-permute-start | bytes 393224 | tf_op jit(solution)/shard_map/ppermute | solution.py:383
  51.7 1.2 collective-permute-done.26.refs_1_
  53.0 3.9 %collective-permute-done.27.refs_2_ = bf16[32,2048]{1,0:T(8,128)(2,1)S(1)} collective-permute-done((bf16[32,2048]{1,0:T(8,128)(2,1)S(1)}, bf16[32,2048]{1,0:T(8,128)(2,1)S(1)}, u32[]{:S(2)}, u32[]{:S(2)}) %collective-permute-start.27) | collective-permute-done | bytes 131104 | tf_op jit(solution)/shard_map/ppermute | solution.py:383
  56.9 3.6 %collective-permute-done.28.refs_3_ = bf16[32,2048]{1,0:T(8,128)(2,1)S(1)} collective-permute-done((bf16[32,2048]{1,0:T(8,128)(2,1)S(1)}, bf16[32,2048]{1,0:T(8,128)(2,1)S(1)}, u32[]{:S(2)}, u32[]{:S(2)}) %collective-permute-start.28) | collective-permute-done | bytes 131104 | tf_op jit(solution)/shard_map/ppermute | solution.py:383
  60.6 0.9 collective-permute-start.6
  61.5 2.7 %collective-permute-start.7 = (bf16[32,2048]{1,0:T(8,128)(2,1)S(1)}, bf16[32,2048]{1,0:T(8,128)(2,1)S(1)}, u32[]{:S(2)}, u32[]{:S(2)}) collective-permute-start(bf16[32,2048]{1,0:T(8,128)(2,1)S(1)} %get-tuple-element.70), channel_id=1, source_target_pairs={{0,28},{2,30},{4,24},{6,26},{8,20},{10,22},{12,16},{14,18},{16,12}... | collective-permute-start | bytes 393224 | tf_op jit(solution)/shard_map/ppermute | solution.py:383
  64.2 4.7 %collective-permute-start.8 = (bf16[32,2048]{1,0:T(8,128)(2,1)S(1)}, bf16[32,2048]{1,0:T(8,128)(2,1)S(1)}, u32[]{:S(2)}, u32[]{:S(2)}) collective-permute-start(bf16[32,2048]{1,0:T(8,128)(2,1)S(1)} %get-tuple-element.71), channel_id=1, source_target_pairs={{0,30},{2,28},{4,26},{6,24},{8,22},{10,20},{12,18},{14,16},{16,14}... | collective-permute-start | bytes 393224 | tf_op jit(solution)/shard_map/ppermute | solution.py:383
  68.9 4.7 %fetch.1 = (bf16[1,2048,1024]{2,1,0:T(8,128)(2,1)S(1)}, bf16[1,2048,1024]{2,1,0:T(8,128)(2,1)S(1)}, bf16[1,1024,2048]{2,1,0:T(8,128)(2,1)S(1)}) custom-call(bf16[1,2048,1024]{2,1,0:T(8,128)(2,1)} %gate_hbm.2, bf16[1,2048,1024]{2,1,0:T(8,128)(2,1)} %up_hbm.1, bf16[1,1024,2048]{2,1,0:T(8,128)(2,1)} %down_hbm.1), custom_call_target="tpu_custom_call" | custom-call | flops 12582912 | bytes 12582912 | tf_op jit(solution)/shard_map/fetch/pallas_call | solution.py:490
  73.7 1.6 %collective-permute-done.8.refs_3_ = bf16[32,2048]{1,0:T(8,128)(2,1)S(1)} collective-permute-done((bf16[32,2048]{1,0:T(8,128)(2,1)S(1)}, bf16[32,2048]{1,0:T(8,128)(2,1)S(1)}, u32[]{:S(2)}, u32[]{:S(2)}) %collective-permute-start.8) | collective-permute-done | bytes 131104 | tf_op jit(solution)/shard_map/ppermute | solution.py:383
  75.4 1.9 %shard_map.120 = (bf16[32,2048]{1,0:T(8,128)(2,1)S(1)}, bf16[32,2048]{1,0:T(8,128)(2,1)S(1)}, bf16[32,2048]{1,0:T(8,128)(2,1)S(1)}, bf16[32,2048]{1,0:T(8,128)(2,1)S(1)}) custom-call(bf16[1,2048,1024]{2,1,0:T(8,128)(2,1)S(1)} %get-tuple-element.65.gate_ref, bf16[1,2048,1024]{2,1,0:T(8,128)(2,1)S(1)} %get-tuple-element.66.up_ref, ...), custom_call_target="tpu_custom_call" | custom-call | flops 1610612736 | bytes 12582912 | tf_op jit(solution)/shard_map/pallas_call | solution.py:517
  77.3 5.4 %collective-permute-start.30 = (bf16[32,2048]{1,0:T(8,128)(2,1)S(1)}, bf16[32,2048]{1,0:T(8,128)(2,1)S(1)}, u32[]{:S(2)}, u32[]{:S(2)}) collective-permute-start(bf16[32,2048]{1,0:T(8,128)(2,1)S(1)} %get-tuple-element.93), channel_id=1, source_target_pairs={{0,16},{2,18},{4,20},{6,22},{8,24},{10,26},{12,28},{14,30},{16,0},... | collective-permute-start | bytes 393224 | tf_op jit(solution)/shard_map/ppermute | solution.py:383
  83.1 3.4 %collective-permute-start.32 = (bf16[32,2048]{1,0:T(8,128)(2,1)S(1)}, bf16[32,2048]{1,0:T(8,128)(2,1)S(1)}, u32[]{:S(2)}, u32[]{:S(2)}) collective-permute-start(bf16[32,2048]{1,0:T(8,128)(2,1)S(1)} %get-tuple-element.95), channel_id=1, source_target_pairs={{0,20},{2,22},{4,16},{6,18},{8,28},{10,30},{12,24},{14,26},{16,4},... | collective-permute-start | bytes 393224 | tf_op jit(solution)/shard_map/ppermute | solution.py:383
  86.5 3.5 %shard_map.119 = (bf16[32,2048]{1,0:T(8,128)(2,1)S(1)}, bf16[32,2048]{1,0:T(8,128)(2,1)S(1)}, bf16[32,2048]{1,0:T(8,128)(2,1)S(1)}, bf16[32,2048]{1,0:T(8,128)(2...) custom-call(bf16[1,2048,1024]{2,1,0:T(8,128)(2,1)S(1)} %get-tuple-el, ...), custom_call_target="tpu_custom_call" | custom-call | flops 3221225472 | bytes 12582912 | tf_op jit(solution)/shard_map/pallas_call | solution.py:517
  90.0 1.1 collective-permute-start.33
  91.1 0.9 collective-permute-start.18
  91.9 6.4 %collective-permute-done.30.refs_8_ = bf16[32,2048]{1,0:T(8,128)(2,1)S(1)} collective-permute-done((bf16[32,2048]{1,0:T(8,128)(2,1)S(1)}, bf16[32,2048]{1,0:T(8,128)(2,1)S(1)}, u32[]{:S(2)}, u32[]{:S(2)}) %collective-permute-start.30) | collective-permute-done | bytes 131104 | tf_op jit(solution)/shard_map/ppermute | solution.py:383
  98.3 1.2 collective-permute-start.19
  99.4 2.0 %collective-permute-done.31.refs_9_ = bf16[32,2048]{1,0:T(8,128)(2,1)S(1)} collective-permute-done((bf16[32,2048]{1,0:T(8,128)(2,1)S(1)}, bf16[32,2048]{1,0:T(8,128)(2,1)S(1)}, u32[]{:S(2)}, u32[]{:S(2)}) %collective-permute-start.31) | collective-permute-done | bytes 131104 | tf_op jit(solution)/shard_map/ppermute | solution.py:383
  101.4 1.7 %collective-permute-start.20 = (bf16[32,2048]{1,0:T(8,128)(2,1)S(1)}, bf16[32,2048]{1,0:T(8,128)(2,1)S(1)}, u32[]{:S(2)}, u32[]{:S(2)}) collective-permute-start(bf16[32,2048]{1,0:T(8,128)(2,1)S(1)} %get-tuple-element.84), channel_id=1, source_target_pairs={{0,6},{2,4},{4,2},{6,0},{8,14},{10,12},{12,10},{14,8},{16,22},{18,... | collective-permute-start | bytes 393224 | tf_op jit(solution)/shard_map/ppermute | solution.py:383
  103.2 1.4 %collective-permute-done.32.refs_10_ = bf16[32,2048]{1,0:T(8,128)(2,1)S(1)} collective-permute-done((bf16[32,2048]{1,0:T(8,128)(2,1)S(1)}, bf16[32,2048]{1,0:T(8,128)(2,1)S(1)}, u32[]{:S(2)}, u32[]{:S(2)}) %collective-permute-start.32) | collective-permute-done | bytes 131104 | tf_op jit(solution)/shard_map/ppermute | solution.py:383
  104.6 2.9 %collective-permute-done.33.refs_11_ = bf16[32,2048]{1,0:T(8,128)(2,1)S(1)} collective-permute-done((bf16[32,2048]{1,0:T(8,128)(2,1)S(1)}, bf16[32,2048]{1,0:T(8,128)(2,1)S(1)}, u32[]{:S(2)}, u32[]{:S(2)}) %collective-permute-start.33) | collective-permute-done | bytes 131104 | tf_op jit(solution)/shard_map/ppermute | solution.py:383
  107.5 3.0 %collective-permute-start.23 = (bf16[32,2048]{1,0:T(8,128)(2,1)S(1)}, bf16[32,2048]{1,0:T(8,128)(2,1)S(1)}, u32[]{:S(2)}, u32[]{:S(2)}) collective-permute-start(bf16[32,2048]{1,0:T(8,128)(2,1)S(1)} %get-tuple-element.87), channel_id=1, source_target_pairs={{0,12},{2,14},{4,8},{6,10},{8,4},{10,6},{12,0},{14,2},{16,28},{18,... | collective-permute-start | bytes 393224 | tf_op jit(solution)/shard_map/ppermute | solution.py:383
  110.5 1.9 %shard_map.118 = (bf16[32,2048]{1,0:T(8,128)(2,1)S(1)}, bf16[32,2048]{1,0:T(8,128)(2,1)S(1)}, bf16[32,2048]{1,0:T(8,128)(2,1)S(1)}, bf16[32,2048]{1,0:T(8,128)(2,1)S(1)}) custom-call(bf16[1,2048,1024]{2,1,0:T(8,128)(2,1)S(1)} %get-tuple-element.65.gate_ref, bf16[1,2048,1024]{2,1,0:T(8,128)(2,1)S(1)} %get-tuple-element.66.up_ref, ...), custom_call_target="tpu_custom_call" | custom-call | flops 1610612736 | bytes 12582912 | tf_op jit(solution)/shard_map/pallas_call | solution.py:517
  112.4 2.3 %collective-permute-start.34 = (bf16[32,2048]{1,0:T(8,128)(2,1)S(1)}, bf16[32,2048]{1,0:T(8,128)(2,1)S(1)}, u32[]{:S(2)}, u32[]{:S(2)}) collective-permute-start(bf16[32,2048]{1,0:T(8,128)(2,1)S(1)} %get-tuple-element.72), channel_id=1, source_target_pairs={{0,24},{2,26},{4,28},{6,30},{8,16},{10,18},{12,20},{14,22},{16,8},... | collective-permute-start | bytes 393224 | tf_op jit(solution)/shard_map/ppermute | solution.py:383
  114.6 2.0 %collective-permute-start.35 = (bf16[32,2048]{1,0:T(8,128)(2,1)S(1)}, bf16[32,2048]{1,0:T(8,128)(2,1)S(1)}, u32[]{:S(2)}, u32[]{:S(2)}) collective-permute-start(bf16[32,2048]{1,0:T(8,128)(2,1)S(1)} %get-tuple-element.98), channel_id=1, source_target_pairs={{0,26},{2,24},{4,30},{6,28},{8,18},{10,16},{12,22},{14,20},{16,10}... | collective-permute-start | bytes 393224 | tf_op jit(solution)/shard_map/ppermute | solution.py:383
  116.6 3.0 %collective-permute-start.36 = (bf16[32,2048]{1,0:T(8,128)(2,1)S(1)}, bf16[32,2048]{1,0:T(8,128)(2,1)S(1)}, u32[]{:S(2)}, u32[]{:S(2)}) collective-permute-start(bf16[32,2048]{1,0:T(8,128)(2,1)S(1)} %get-tuple-element.99), channel_id=1, source_target_pairs={{0,28},{2,30},{4,24},{6,26},{8,20},{10,22},{12,16},{14,18},{16,12}... | collective-permute-start | bytes 393224 | tf_op jit(solution)/shard_map/ppermute | solution.py:383
  119.6 2.3 %collective-permute-start.37 = (bf16[32,2048]{1,0:T(8,128)(2,1)S(1)}, bf16[32,2048]{1,0:T(8,128)(2,1)S(1)}, u32[]{:S(2)}, u32[]{:S(2)}) collective-permute-start(bf16[32,2048]{1,0:T(8,128)(2,1)S(1)} %get-tuple-element.100), channel_id=1, source_target_pairs={{0,30},{2,28},{4,26},{6,24},{8,22},{10,20},{12,18},{14,16},{16,14}... | collective-permute-start | bytes 393224 | tf_op jit(solution)/shard_map/ppermute | solution.py:383
  122.0 9.1 %collective-permute-done.24.refs_7_ = bf16[32,2048]{1,0:T(8,128)(2,1)S(1)} collective-permute-done((bf16[32,2048]{1,0:T(8,128)(2,1)S(1)}, bf16[32,2048]{1,0:T(8,128)(2,1)S(1)}, u32[]{:S(2)}, u32[]{:S(2)}) %collective-permute-start.24) | collective-permute-done | bytes 131104 | tf_op jit(solution)/shard_map/ppermute | solution.py:383
  131.0 2.3 %gather.1 = (f32[128,2048]{1,0:T(8,128)S(1)}, f32[128,2048]{1,0:T(8,128)S(1)}) custom-call(s32[2]{0:T(128)S(1)} %pad_add_fusion.where_ref, f32[4,128]{1,0:T(4,128)S(1)} %get-tuple-element.101.meta_ref, f32[4,128]{1,0:T(4,128)S(1)} %collective-permute-done.4.meta_other_ref.meta_ref, bf16[32,2048]{1,0:T(8,128)(2,1)S(1)} %get-tuple-element.81.refs_0_, ...), custom_call_target="tpu_custom_call" | custom-call | tf_op jit(solution)/shard_map/gather/pallas_call | solution.py:541
  133.4 1.2 shard_map.121
  134.8 1.2 shard_map.122.own_ref
  136.0 0.7 collective-permute-done.38.other_ref
  136.7 0.9 combine.1
  (45 shorter events, 2.4 us)
Async XLA Ops:
  1.4 6.2 %collective-permute-start = (bf16[144,768]{1,0:T(8,128)(2,1)S(1)}, bf16[144,768]{1,0:T(8,128)(2,1)S(1)}, u32[]{:S(2)}, u32[]{:S(2)}) collective-permute-start(bf16[144,768]{1,0:T(8,128)(2,1)S(1)} %get-tuple-element.55), channel_id=1, source_target_pairs={{0,1},{1,0},{2,3},{3,2},{4,5},{5,4},{6,7},{7,6},{8,9},{9,8},{10,11... | collective-permute-start | bytes 663560 | tf_op jit(solution)/shard_map/ppermute | solution.py:422
  2.0 5.6 %collective-permute-start.1 = (f32[32,768]{1,0:T(8,128)S(1)}, f32[32,768]{1,0:T(8,128)S(1)}, u32[]{:S(2)}, u32[]{:S(2)}) collective-permute-start(f32[32,768]{1,0:T(8,128)S(1)} %get-tuple-element.56.taps_ref), channel_id=1, source_target_pairs={{0,1},{1,0},{2,3},{3,2},{4,5},{5,4},{6,7},{7,6},{8,9},{9,8},{10,11... | collective-permute-start | bytes 294920 | tf_op jit(solution)/shard_map/ppermute | solution.py:423
  2.1 9.0 %collective-permute-start.2 = (bf16[16,768]{1,0:T(8,128)(2,1)S(1)}, bf16[16,768]{1,0:T(8,128)(2,1)S(1)}, u32[]{:S(2)}, u32[]{:S(2)}) collective-permute-start(bf16[16,768]{1,0:T(8,128)(2,1)S(1)} %get-tuple-element.58), channel_id=1, source_target_pairs={{0,2},{2,4},{3,1},{4,6},{5,3},{6,8},{7,5},{8,10},{9,7},{10,12},{11... | collective-permute-start | bytes 73736 | tf_op jit(solution)/shard_map/ppermute | solution.py:424
  6.9 4.2 %collective-permute-start.3 = (bf16[16,768]{1,0:T(8,128)(2,1)S(1)}, bf16[16,768]{1,0:T(8,128)(2,1)S(1)}, u32[]{:S(2)}, u32[]{:S(2)}) collective-permute-start(bf16[16,768]{1,0:T(8,128)(2,1)S(1)} %get-tuple-element.59), channel_id=1, source_target_pairs={{1,2},{3,4},{2,1},{5,6},{4,3},{7,8},{6,5},{9,10},{8,7},{11,12},{10... | collective-permute-start | bytes 73736 | tf_op jit(solution)/shard_map/ppermute | solution.py:425
  15.1 8.1 %collective-permute-start.10 = (bf16[32,2048]{1,0:T(8,128)(2,1)S(1)}, bf16[32,2048]{1,0:T(8,128)(2,1)S(1)}, u32[]{:S(2)}, u32[]{:S(2)}) collective-permute-start(bf16[32,2048]{1,0:T(8,128)(2,1)S(1)} %get-tuple-element.74), channel_id=1, source_target_pairs={{0,2},{2,0},{4,6},{6,4},{8,10},{10,8},{12,14},{14,12},{16,18},{18,... | collective-permute-start | bytes 393224 | tf_op jit(solution)/shard_map/ppermute | solution.py:383
  17.9 8.1 %collective-permute-start.11 = (bf16[32,2048]{1,0:T(8,128)(2,1)S(1)}, bf16[32,2048]{1,0:T(8,128)(2,1)S(1)}, u32[]{:S(2)}, u32[]{:S(2)}) collective-permute-start(bf16[32,2048]{1,0:T(8,128)(2,1)S(1)} %get-tuple-element.75), channel_id=1, source_target_pairs={{0,4},{2,6},{4,0},{6,2},{8,12},{10,14},{12,8},{14,10},{16,20},{18,... | collective-permute-start | bytes 393224 | tf_op jit(solution)/shard_map/ppermute | solution.py:383
  19.5 9.0 %collective-permute-start.12 = (bf16[32,2048]{1,0:T(8,128)(2,1)S(1)}, bf16[32,2048]{1,0:T(8,128)(2,1)S(1)}, u32[]{:S(2)}, u32[]{:S(2)}) collective-permute-start(bf16[32,2048]{1,0:T(8,128)(2,1)S(1)} %get-tuple-element.76), channel_id=1, source_target_pairs={{0,6},{2,4},{4,2},{6,0},{8,14},{10,12},{12,10},{14,8},{16,22},{18,... | collective-permute-start | bytes 393224 | tf_op jit(solution)/shard_map/ppermute | solution.py:383
  20.0 10.6 %collective-permute-start.13 = (bf16[32,2048]{1,0:T(8,128)(2,1)S(1)}, bf16[32,2048]{1,0:T(8,128)(2,1)S(1)}, u32[]{:S(2)}, u32[]{:S(2)}) collective-permute-start(bf16[32,2048]{1,0:T(8,128)(2,1)S(1)} %get-tuple-element.77), channel_id=1, source_target_pairs={{0,8},{2,10},{4,12},{6,14},{8,0},{10,2},{12,4},{14,6},{16,24},{18,... | collective-permute-start | bytes 393224 | tf_op jit(solution)/shard_map/ppermute | solution.py:383
  23.0 10.1 %collective-permute-start.14 = (bf16[32,2048]{1,0:T(8,128)(2,1)S(1)}, bf16[32,2048]{1,0:T(8,128)(2,1)S(1)}, u32[]{:S(2)}, u32[]{:S(2)}) collective-permute-start(bf16[32,2048]{1,0:T(8,128)(2,1)S(1)} %get-tuple-element.78), channel_id=1, source_target_pairs={{0,10},{2,8},{4,14},{6,12},{8,2},{10,0},{12,6},{14,4},{16,26},{18,... | collective-permute-start | bytes 393224 | tf_op jit(solution)/shard_map/ppermute | solution.py:383
  23.2 13.2 %collective-permute-start.15 = (bf16[32,2048]{1,0:T(8,128)(2,1)S(1)}, bf16[32,2048]{1,0:T(8,128)(2,1)S(1)}, u32[]{:S(2)}, u32[]{:S(2)}) collective-permute-start(bf16[32,2048]{1,0:T(8,128)(2,1)S(1)} %get-tuple-element.79), channel_id=1, source_target_pairs={{0,12},{2,14},{4,8},{6,10},{8,4},{10,6},{12,0},{14,2},{16,28},{18,... | collective-permute-start | bytes 393224 | tf_op jit(solution)/shard_map/ppermute | solution.py:383
  26.1 15.0 %collective-permute-start.16 = (bf16[32,2048]{1,0:T(8,128)(2,1)S(1)}, bf16[32,2048]{1,0:T(8,128)(2,1)S(1)}, u32[]{:S(2)}, u32[]{:S(2)}) collective-permute-start(bf16[32,2048]{1,0:T(8,128)(2,1)S(1)} %get-tuple-element.80), channel_id=1, source_target_pairs={{0,14},{2,12},{4,10},{6,8},{8,6},{10,4},{12,2},{14,0},{16,30},{18,... | collective-permute-start | bytes 393224 | tf_op jit(solution)/shard_map/ppermute | solution.py:383
  28.4 12.7 %collective-permute-start.25 = (bf16[32,2048]{1,0:T(8,128)(2,1)S(1)}, bf16[32,2048]{1,0:T(8,128)(2,1)S(1)}, u32[]{:S(2)}, u32[]{:S(2)}) collective-permute-start(bf16[32,2048]{1,0:T(8,128)(2,1)S(1)} %get-tuple-element.89), channel_id=1, source_target_pairs={{0,16},{2,18},{4,20},{6,22},{8,24},{10,26},{12,28},{14,30},{16,0},... | collective-permute-start | bytes 393224 | tf_op jit(solution)/shard_map/ppermute | solution.py:383
  30.6 22.4 %collective-permute-start.26 = (bf16[32,2048]{1,0:T(8,128)(2,1)S(1)}, bf16[32,2048]{1,0:T(8,128)(2,1)S(1)}, u32[]{:S(2)}, u32[]{:S(2)}) collective-permute-start(bf16[32,2048]{1,0:T(8,128)(2,1)S(1)} %get-tuple-element.90), channel_id=1, source_target_pairs={{0,18},{2,16},{4,22},{6,20},{8,26},{10,24},{12,30},{14,28},{16,2},... | collective-permute-start | bytes 393224 | tf_op jit(solution)/shard_map/ppermute | solution.py:383
  33.1 23.8 %collective-permute-start.27 = (bf16[32,2048]{1,0:T(8,128)(2,1)S(1)}, bf16[32,2048]{1,0:T(8,128)(2,1)S(1)}, u32[]{:S(2)}, u32[]{:S(2)}) collective-permute-start(bf16[32,2048]{1,0:T(8,128)(2,1)S(1)} %get-tuple-element.91), channel_id=1, source_target_pairs={{0,20},{2,22},{4,16},{6,18},{8,28},{10,30},{12,24},{14,26},{16,4},... | collective-permute-start | bytes 393224 | tf_op jit(solution)/shard_map/ppermute | solution.py:383
  36.4 24.1 %collective-permute-start.28 = (bf16[32,2048]{1,0:T(8,128)(2,1)S(1)}, bf16[32,2048]{1,0:T(8,128)(2,1)S(1)}, u32[]{:S(2)}, u32[]{:S(2)}) collective-permute-start(bf16[32,2048]{1,0:T(8,128)(2,1)S(1)} %get-tuple-element.92), channel_id=1, source_target_pairs={{0,22},{2,20},{4,18},{6,16},{8,30},{10,28},{12,26},{14,24},{16,6},... | collective-permute-start | bytes 393224 | tf_op jit(solution)/shard_map/ppermute | solution.py:383
  41.1 42.0 %collective-permute-start.17 = (bf16[128,2048]{1,0:T(8,128)(2,1)S(1)}, bf16[128,2048]{1,0:T(8,128)(2,1)S(1)}, u32[]{:S(2)}, u32[]{:S(2)}) collective-permute-start(bf16[128,2048]{1,0:T(8,128)(2,1)S(1)} %pack.4), channel_id=1, source_target_pairs={{0,1},{1,0},{2,3},{3,2},{4,5},{5,4},{6,7},{7,6},{8,9},{9,8},{10,11... | collective-permute-start | bytes 1572872 | tf_op jit(solution)/shard_map/ppermute | solution.py:516
  41.2 23.0 %collective-permute-start.5 = (bf16[32,2048]{1,0:T(8,128)(2,1)S(1)}, bf16[32,2048]{1,0:T(8,128)(2,1)S(1)}, u32[]{:S(2)}, u32[]{:S(2)}) collective-permute-start(bf16[32,2048]{1,0:T(8,128)(2,1)S(1)} %get-tuple-element.68), channel_id=1, source_target_pairs={{0,24},{2,26},{4,28},{6,30},{8,16},{10,18},{12,20},{14,22},{16,8},... | collective-permute-start | bytes 393224 | tf_op jit(solution)/shard_map/ppermute | solution.py:383
  60.5 14.9 %collective-permute-start.29 = (bf16[64,2048]{1,0:T(8,128)(2,1)S(1)}, bf16[64,2048]{1,0:T(8,128)(2,1)S(1)}, u32[]{:S(2)}, u32[]{:S(2)}) collective-permute-start(bf16[64,2048]{1,0:T(8,128)(2,1)S(1)} %pack.5), channel_id=1, source_target_pairs={{0,1},{1,0},{2,3},{3,2},{4,5},{5,4},{6,7},{7,6},{8,9},{9,8},{10,11... | collective-permute-start | bytes 786440 | tf_op jit(solution)/shard_map/ppermute | solution.py:516
  60.6 13.0 %collective-permute-start.6 = (bf16[32,2048]{1,0:T(8,128)(2,1)S(1)}, bf16[32,2048]{1,0:T(8,128)(2,1)S(1)}, u32[]{:S(2)}, u32[]{:S(2)}) collective-permute-start(bf16[32,2048]{1,0:T(8,128)(2,1)S(1)} %get-tuple-element.69), channel_id=1, source_target_pairs={{0,26},{2,24},{4,30},{6,28},{8,18},{10,16},{12,22},{14,20},{16,10}... | collective-permute-start | bytes 393224 | tf_op jit(solution)/shard_map/ppermute | solution.py:383
  61.5 12.2 %collective-permute-start.7 = (bf16[32,2048]{1,0:T(8,128)(2,1)S(1)}, bf16[32,2048]{1,0:T(8,128)(2,1)S(1)}, u32[]{:S(2)}, u32[]{:S(2)}) collective-permute-start(bf16[32,2048]{1,0:T(8,128)(2,1)S(1)} %get-tuple-element.70), channel_id=1, source_target_pairs={{0,28},{2,30},{4,24},{6,26},{8,20},{10,22},{12,16},{14,18},{16,12}... | collective-permute-start | bytes 393224 | tf_op jit(solution)/shard_map/ppermute | solution.py:383
  64.2 11.1 %collective-permute-start.8 = (bf16[32,2048]{1,0:T(8,128)(2,1)S(1)}, bf16[32,2048]{1,0:T(8,128)(2,1)S(1)}, u32[]{:S(2)}, u32[]{:S(2)}) collective-permute-start(bf16[32,2048]{1,0:T(8,128)(2,1)S(1)} %get-tuple-element.71), channel_id=1, source_target_pairs={{0,30},{2,28},{4,26},{6,24},{8,22},{10,20},{12,18},{14,16},{16,14}... | collective-permute-start | bytes 393224 | tf_op jit(solution)/shard_map/ppermute | solution.py:383
  73.6 16.4 %collective-permute-start.4 = (f32[4,128]{1,0:T(4,128)S(1)}, f32[4,128]{1,0:T(4,128)S(1)}, u32[]{:S(2)}, u32[]{:S(2)}) collective-permute-start(f32[4,128]{1,0:T(4,128)S(1)} %get-tuple-element.101.meta_ref), channel_id=1, source_target_pairs={{0,1},{1,0},{2,3},{3,2},{4,5},{5,4},{6,7},{7,6},{8,9},{9,8},{10,11... | collective-permute-start | bytes 6152 | tf_op jit(solution)/shard_map/ppermute | solution.py:426
  75.3 15.7 %collective-permute-start.9 = (bf16[64,2048]{1,0:T(8,128)(2,1)S(1)}, bf16[64,2048]{1,0:T(8,128)(2,1)S(1)}, u32[]{:S(2)}, u32[]{:S(2)}) collective-permute-start(bf16[64,2048]{1,0:T(8,128)(2,1)S(1)} %pack.3), channel_id=1, source_target_pairs={{0,1},{1,0},{2,3},{3,2},{4,5},{5,4},{6,7},{7,6},{8,9},{9,8},{10,11... | collective-permute-start | bytes 786440 | tf_op jit(solution)/shard_map/ppermute | solution.py:516
  77.3 21.0 %collective-permute-start.30 = (bf16[32,2048]{1,0:T(8,128)(2,1)S(1)}, bf16[32,2048]{1,0:T(8,128)(2,1)S(1)}, u32[]{:S(2)}, u32[]{:S(2)}) collective-permute-start(bf16[32,2048]{1,0:T(8,128)(2,1)S(1)} %get-tuple-element.93), channel_id=1, source_target_pairs={{0,16},{2,18},{4,20},{6,22},{8,24},{10,26},{12,28},{14,30},{16,0},... | collective-permute-start | bytes 393224 | tf_op jit(solution)/shard_map/ppermute | solution.py:383
  82.7 18.7 %collective-permute-start.31 = (bf16[32,2048]{1,0:T(8,128)(2,1)S(1)}, bf16[32,2048]{1,0:T(8,128)(2,1)S(1)}, u32[]{:S(2)}, u32[]{:S(2)}) collective-permute-start(bf16[32,2048]{1,0:T(8,128)(2,1)S(1)} %get-tuple-element.94), channel_id=1, source_target_pairs={{0,18},{2,16},{4,22},{6,20},{8,26},{10,24},{12,30},{14,28},{16,2},... | collective-permute-start | bytes 393224 | tf_op jit(solution)/shard_map/ppermute | solution.py:383
  83.1 21.5 %collective-permute-start.32 = (bf16[32,2048]{1,0:T(8,128)(2,1)S(1)}, bf16[32,2048]{1,0:T(8,128)(2,1)S(1)}, u32[]{:S(2)}, u32[]{:S(2)}) collective-permute-start(bf16[32,2048]{1,0:T(8,128)(2,1)S(1)} %get-tuple-element.95), channel_id=1, source_target_pairs={{0,20},{2,22},{4,16},{6,18},{8,28},{10,30},{12,24},{14,26},{16,4},... | collective-permute-start | bytes 393224 | tf_op jit(solution)/shard_map/ppermute | solution.py:383
  90.0 17.5 %collective-permute-start.33 = (bf16[32,2048]{1,0:T(8,128)(2,1)S(1)}, bf16[32,2048]{1,0:T(8,128)(2,1)S(1)}, u32[]{:S(2)}, u32[]{:S(2)}) collective-permute-start(bf16[32,2048]{1,0:T(8,128)(2,1)S(1)} %get-tuple-element.96), channel_id=1, source_target_pairs={{0,22},{2,20},{4,18},{6,16},{8,30},{10,28},{12,26},{14,24},{16,6},... | collective-permute-start | bytes 393224 | tf_op jit(solution)/shard_map/ppermute | solution.py:383
  91.1 16.4 %collective-permute-start.18 = (bf16[32,2048]{1,0:T(8,128)(2,1)S(1)}, bf16[32,2048]{1,0:T(8,128)(2,1)S(1)}, u32[]{:S(2)}, u32[]{:S(2)}) collective-permute-start(bf16[32,2048]{1,0:T(8,128)(2,1)S(1)} %get-tuple-element.82), channel_id=1, source_target_pairs={{0,2},{2,0},{4,6},{6,4},{8,10},{10,8},{12,14},{14,12},{16,18},{18,... | collective-permute-start | bytes 393224 | tf_op jit(solution)/shard_map/ppermute | solution.py:383
  98.3 14.1 %collective-permute-start.19 = (bf16[32,2048]{1,0:T(8,128)(2,1)S(1)}, bf16[32,2048]{1,0:T(8,128)(2,1)S(1)}, u32[]{:S(2)}, u32[]{:S(2)}) collective-permute-start(bf16[32,2048]{1,0:T(8,128)(2,1)S(1)} %get-tuple-element.83), channel_id=1, source_target_pairs={{0,4},{2,6},{4,0},{6,2},{8,12},{10,14},{12,8},{14,10},{16,20},{18,... | collective-permute-start | bytes 393224 | tf_op jit(solution)/shard_map/ppermute | solution.py:383
  101.4 13.2 %collective-permute-start.20 = (bf16[32,2048]{1,0:T(8,128)(2,1)S(1)}, bf16[32,2048]{1,0:T(8,128)(2,1)S(1)}, u32[]{:S(2)}, u32[]{:S(2)}) collective-permute-start(bf16[32,2048]{1,0:T(8,128)(2,1)S(1)} %get-tuple-element.84), channel_id=1, source_target_pairs={{0,6},{2,4},{4,2},{6,0},{8,14},{10,12},{12,10},{14,8},{16,22},{18,... | collective-permute-start | bytes 393224 | tf_op jit(solution)/shard_map/ppermute | solution.py:383
  104.6 10.1 %collective-permute-start.21 = (bf16[32,2048]{1,0:T(8,128)(2,1)S(1)}, bf16[32,2048]{1,0:T(8,128)(2,1)S(1)}, u32[]{:S(2)}, u32[]{:S(2)}) collective-permute-start(bf16[32,2048]{1,0:T(8,128)(2,1)S(1)} %get-tuple-element.85), channel_id=1, source_target_pairs={{0,8},{2,10},{4,12},{6,14},{8,0},{10,2},{12,4},{14,6},{16,24},{18,... | collective-permute-start | bytes 393224 | tf_op jit(solution)/shard_map/ppermute | solution.py:383
  107.5 9.2 %collective-permute-start.22 = (bf16[32,2048]{1,0:T(8,128)(2,1)S(1)}, bf16[32,2048]{1,0:T(8,128)(2,1)S(1)}, u32[]{:S(2)}, u32[]{:S(2)}) collective-permute-start(bf16[32,2048]{1,0:T(8,128)(2,1)S(1)} %get-tuple-element.86), channel_id=1, source_target_pairs={{0,10},{2,8},{4,14},{6,12},{8,2},{10,0},{12,6},{14,4},{16,26},{18,... | collective-permute-start | bytes 393224 | tf_op jit(solution)/shard_map/ppermute | solution.py:383
  107.5 12.1 %collective-permute-start.23 = (bf16[32,2048]{1,0:T(8,128)(2,1)S(1)}, bf16[32,2048]{1,0:T(8,128)(2,1)S(1)}, u32[]{:S(2)}, u32[]{:S(2)}) collective-permute-start(bf16[32,2048]{1,0:T(8,128)(2,1)S(1)} %get-tuple-element.87), channel_id=1, source_target_pairs={{0,12},{2,14},{4,8},{6,10},{8,4},{10,6},{12,0},{14,2},{16,28},{18,... | collective-permute-start | bytes 393224 | tf_op jit(solution)/shard_map/ppermute | solution.py:383
  112.4 21.0 %collective-permute-start.34 = (bf16[32,2048]{1,0:T(8,128)(2,1)S(1)}, bf16[32,2048]{1,0:T(8,128)(2,1)S(1)}, u32[]{:S(2)}, u32[]{:S(2)}) collective-permute-start(bf16[32,2048]{1,0:T(8,128)(2,1)S(1)} %get-tuple-element.72), channel_id=1, source_target_pairs={{0,24},{2,26},{4,28},{6,30},{8,16},{10,18},{12,20},{14,22},{16,8},... | collective-permute-start | bytes 393224 | tf_op jit(solution)/shard_map/ppermute | solution.py:383
  114.6 16.4 %collective-permute-start.24 = (bf16[32,2048]{1,0:T(8,128)(2,1)S(1)}, bf16[32,2048]{1,0:T(8,128)(2,1)S(1)}, u32[]{:S(2)}, u32[]{:S(2)}) collective-permute-start(bf16[32,2048]{1,0:T(8,128)(2,1)S(1)} %get-tuple-element.88), channel_id=1, source_target_pairs={{0,14},{2,12},{4,10},{6,8},{8,6},{10,4},{12,2},{14,0},{16,30},{18,... | collective-permute-start | bytes 393224 | tf_op jit(solution)/shard_map/ppermute | solution.py:383
  114.6 18.8 %collective-permute-start.35 = (bf16[32,2048]{1,0:T(8,128)(2,1)S(1)}, bf16[32,2048]{1,0:T(8,128)(2,1)S(1)}, u32[]{:S(2)}, u32[]{:S(2)}) collective-permute-start(bf16[32,2048]{1,0:T(8,128)(2,1)S(1)} %get-tuple-element.98), channel_id=1, source_target_pairs={{0,26},{2,24},{4,30},{6,28},{8,18},{10,16},{12,22},{14,20},{16,10}... | collective-permute-start | bytes 393224 | tf_op jit(solution)/shard_map/ppermute | solution.py:383
  116.6 16.8 %collective-permute-start.36 = (bf16[32,2048]{1,0:T(8,128)(2,1)S(1)}, bf16[32,2048]{1,0:T(8,128)(2,1)S(1)}, u32[]{:S(2)}, u32[]{:S(2)}) collective-permute-start(bf16[32,2048]{1,0:T(8,128)(2,1)S(1)} %get-tuple-element.99), channel_id=1, source_target_pairs={{0,28},{2,30},{4,24},{6,26},{8,20},{10,22},{12,16},{14,18},{16,12}... | collective-permute-start | bytes 393224 | tf_op jit(solution)/shard_map/ppermute | solution.py:383
  119.6 13.8 %collective-permute-start.37 = (bf16[32,2048]{1,0:T(8,128)(2,1)S(1)}, bf16[32,2048]{1,0:T(8,128)(2,1)S(1)}, u32[]{:S(2)}, u32[]{:S(2)}) collective-permute-start(bf16[32,2048]{1,0:T(8,128)(2,1)S(1)} %get-tuple-element.100), channel_id=1, source_target_pairs={{0,30},{2,28},{4,26},{6,24},{8,22},{10,20},{12,18},{14,16},{16,14}... | collective-permute-start | bytes 393224 | tf_op jit(solution)/shard_map/ppermute | solution.py:383
  134.7 2.0 %collective-permute-start.38 = (bf16[128,2048]{1,0:T(8,128)(2,1)S(1)}, bf16[128,2048]{1,0:T(8,128)(2,1)S(1)}, u32[]{:S(2)}, u32[]{:S(2)}) collective-permute-start(bf16[128,2048]{1,0:T(8,128)(2,1)S(1)} %shard_map.121), channel_id=1, source_target_pairs={{0,1},{1,0},{2,3},{3,2},{4,5},{5,4},{6,7},{7,6},{8,9},{9,8},{10,11... | collective-permute-start | bytes 1572872 | tf_op jit(solution)/shard_map/ppermute | solution.py:560

commit v6 on v5

--- a/solution.py
+++ b/solution.py
@@ -77,7 +77,7 @@
     meta_ref[topk : 2 * topk, :] = mix_ref[...]
 
 
-def places(ids, cap, experts, where_ref, which, first, count):
+def places(ids, cap, experts, where_ref, which, first, count, gap=(0, 0)):
     topk, rows = ids.shape
     lane = lax.broadcasted_iota(jnp.int32, (experts, rows), 0)
     named = [ids[k : k + 1, :] == lane for k in range(topk)]
@@ -97,6 +97,10 @@
             target = turned + jnp.bitwise_xor(side, where_ref[0]) * cap
         else:
             target = jnp.where(side == where_ref[0], turned + which * cap, -1)
+        start, end = (2 * cap * edge for edge in gap)
+        if end > start:
+            inside = jnp.where(target >= start, -1, target)
+            target = jnp.where(target >= end, target - (end - start), inside)
         found.append(slot == target)
     return found
 
@@ -118,12 +122,12 @@
     return meta_ref[0:topk, :].astype(jnp.int32), meta_ref[topk : 2 * topk, :]
 
 
-def collected(meta_ref, rows, cap, experts, where_ref, which, first, count):
+def collected(meta_ref, rows, cap, experts, where_ref, which, first, count, gap=(0, 0)):
     ids, mix = split_meta(meta_ref)
     topk, tokens = ids.shape
     mix = jnp.concatenate([mix, jnp.zeros((8 - topk, tokens), jnp.float32)], axis=0).T
     total = None
-    for k, place in enumerate(places(ids, cap, experts, where_ref, which, first, count)):
+    for k, place in enumerate(places(ids, cap, experts, where_ref, which, first, count, gap)):
         got = lax.dot_general(
             place.astype(jnp.float32).astype(jnp.bfloat16),
             rows,
@@ -295,9 +299,9 @@
     other_ref[...] = collected(meta_other_ref, rows, cap, experts, where_ref, 1, first, count)
 
 
-def last_kernel(cap, experts, first, which, where_ref, meta_ref, base_ref, *refs):
+def last_kernel(cap, experts, gap, which, where_ref, meta_ref, base_ref, *refs):
     rows = joined(refs[:-1])
-    total = collected(meta_ref, rows, cap, experts, where_ref, which, first, len(refs) - 1)
+    total = collected(meta_ref, rows, cap, experts, where_ref, which, 0, len(refs) - 1, gap)
     refs[-1][...] = (base_ref[...] + total).astype(refs[-1].dtype)
 
 
@@ -539,22 +543,22 @@
     x2_back = exchange(x2_done, mid)
     meta_late, _ = lax.optimization_barrier((meta, x2_done[0]))
     base_own, base_other = pl.pallas_call(
-        functools.partial(gather_kernel, *sizes, 0),
+        functools.partial(gather_kernel, *sizes, near_count),
         out_shape=[sums] * 2,
-        in_specs=smem + vmem(2 + mid),
+        in_specs=smem + vmem(2 + mid - near_count),
         out_specs=vmem(2),
         compiler_params=params(16),
         name="gather",
-    )(where, meta_late, meta_other, *near_back, *x1_back)
+    )(where, meta_late, meta_other, *x1_back)
 
     def last(which, base, m, out):
         return pl.pallas_call(
-            functools.partial(last_kernel, *sizes, mid, which),
+            functools.partial(last_kernel, *sizes, (near_count, mid), which),
             out_shape=out,
-            in_specs=smem + vmem(2 + sp_count - mid),
+            in_specs=smem + vmem(2 + near_count + sp_count - mid),
             out_specs=vmem(1)[0],
             compiler_params=params(16),
-        )(where, m, base, *x2_back)
+        )(where, m, base, *near_back, *x2_back)
 
     other_sum = last(1, base_other, meta_other, tokens)
     other_back = lax.ppermute(other_sum, BOTH, swap)

time: 140 us -> 147 us (1.050); the launches traced: 138 us -> 146 us
  starting transfers between devices: 73.9 us -> 80.5 us
  waiting for transfers between devices: 36.8 us -> 38.9 us
    ppermute x30, starting transfers between devices: 67.4 us -> 73.6 us  [exchange(): moved.append(lax.ppermute(block, 'sp', pairs) if k else block)]
    ppermute x30, waiting for transfers between devices: 36.1 us -> 38.5 us  [exchange(): moved.append(lax.ppermute(block, 'sp', pairs) if k else block)]
  transfers between devices with their start and end apart: 39 -> 39, of which waited for: 11 -> 13; matrix products, arithmetic and copies ran while one was open for 0% -> 0% of each run, Pallas kernels for 14% -> 13%
where the time goes in v6:
time: 147 us; the launch traced here: 146 us
  starting transfers between devices  80.5 us (55%)
  waiting for transfers between devices  38.9 us (26%)
  Pallas kernels  26.6 us (18%)
    ppermute x30, starting transfers between devices, exchange(): moved.append(lax.ppermute(block, 'sp', pairs) if k else block)  73.6 us
    ppermute x30, waiting for transfers between devices, exchange(): moved.append(lax.ppermute(block, 'sp', pairs) if k else block)  38.5 us
    pallas_call x3, Pallas kernels, apply(): pl.pallas_call(expert_kernel, out_shape=[piece] * count, in_specs=vmem(4...  7.18 us
    ppermute x1, starting transfers between devices, per_device(): near_rows = lax.ppermute(near_rows, BOTH, near)  4.8 us
    pallas_call x1, Pallas kernels, per_device(): pl.pallas_call(fetch_kernel, out_shape=[pltpu.VMEM(w.shape, bf16) for w i...  4.7 us
    pallas_call x1, Pallas kernels, per_device(): pl.pallas_call(functools.partial(module_kernel, *sizes, sp_count), out_sh...  4.06 us
    pallas_call x1, Pallas kernels, per_device(): pl.pallas_call(conv_kernel, out_shape=[jax.ShapeDtypeStruct((blocks, rows...  3.41 us
    pallas_call x2, Pallas kernels, last(): pl.pallas_call(functools.partial(last_kernel, *sizes, (near_count, mid),...  3.01 us
  transfers between devices with their start and end apart: 39, of which 13 were waited for; matrix products, arithmetic and copies ran while one was open for 0% of the time, Pallas kernels for 13%

profile of v6, /device:TPU:0, one launch (start us, length us, event | category | flops | bytes accessed | tf_op | source)
XLA Modules:
  0.0 146.4 jit_solution(17717627253917140881)
XLA Ops:
  0.0 1.4 glu.1
  2.1 4.8 %collective-permute-start.2 = (bf16[16,768]{1,0:T(8,128)(2,1)S(1)}, bf16[16,768]{1,0:T(8,128)(2,1)S(1)}, u32[]{:S(2)}, u32[]{:S(2)}) collective-permute-start(bf16[16,768]{1,0:T(8,128)(2,1)S(1)} %get-tuple-element.58), channel_id=1, source_target_pairs={{0,2},{2,4},{3,1},{4,6},{5,3},{6,8},{7,5},{8,10},{9,7},{10,12},{11... | collective-permute-start | bytes 73736 | tf_op jit(solution)/shard_map/ppermute | solution.py:428
  6.9 0.7 collective-permute-start.3
  7.6 3.4 %conv.1 = (f32[12,128,128]{2,1,0:T(8,128)S(1)}, bf16[2,768,2048]{2,1,0:T(8,128)(2,1)S(1)}) custom-call(s32[2]{0:T(128)S(1)} %pad_add_fusion.where_ref, bf16[144,768]{1,0:T(8,128)(2,1)S(1)} %get-tuple-element.54.mine_ref, bf16[144,768]{1,0:T(8,128)(2,1)S(1)} %collective-permute-done.other_ref, f32[32,768]{1,0:T(8,128)S(1)} %get-tuple-element.56.taps_ref, ...), custom_call_target="tpu_custom_call" | custom-call | flops 12189696 | bytes 786432 | tf_op jit(solution)/shard_map/conv/pallas_call | solution.py:438
  11.1 4.1 %module.1 = (bf16[128,2048]{1,0:T(8,128)(2,1)S(1)}, bf16[32,2048]{1,0:T(8,128)(2,1)S(1)}, bf16[32,2048]{1,0:T(8,128)(2,1)S(1)}, bf16[32,2048]{1,0:T(8,128)(2,1)S...) custom-call(s32[2]{0:T(128)S(1)} %pad_add_fusion.where_ref, ...), custom_call_target="tpu_custom_call" | custom-call | tf_op jit(solution)/shard_map/module/pallas_call | solution.py:458
  15.1 2.8 %collective-permute-start.19 = (bf16[32,2048]{1,0:T(8,128)(2,1)S(1)}, bf16[32,2048]{1,0:T(8,128)(2,1)S(1)}, u32[]{:S(2)}, u32[]{:S(2)}) collective-permute-start(bf16[32,2048]{1,0:T(8,128)(2,1)S(1)} %get-tuple-element.83), channel_id=1, source_target_pairs={{0,2},{2,0},{4,6},{6,4},{8,10},{10,8},{12,14},{14,12},{16,18},{18,... | collective-permute-start | bytes 393224 | tf_op jit(solution)/shard_map/ppermute | solution.py:387
  17.9 1.5 %collective-permute-start.20 = (bf16[32,2048]{1,0:T(8,128)(2,1)S(1)}, bf16[32,2048]{1,0:T(8,128)(2,1)S(1)}, u32[]{:S(2)}, u32[]{:S(2)}) collective-permute-start(bf16[32,2048]{1,0:T(8,128)(2,1)S(1)} %get-tuple-element.84), channel_id=1, source_target_pairs={{0,4},{2,6},{4,0},{6,2},{8,12},{10,14},{12,8},{14,10},{16,20},{18,... | collective-permute-start | bytes 393224 | tf_op jit(solution)/shard_map/ppermute | solution.py:387
  20.0 4.0 %collective-permute-start.10 = (bf16[32,2048]{1,0:T(8,128)(2,1)S(1)}, bf16[32,2048]{1,0:T(8,128)(2,1)S(1)}, u32[]{:S(2)}, u32[]{:S(2)}) collective-permute-start(bf16[32,2048]{1,0:T(8,128)(2,1)S(1)} %get-tuple-element.74), channel_id=1, source_target_pairs={{0,16},{2,18},{4,20},{6,22},{8,24},{10,26},{12,28},{14,30},{16,0},... | collective-permute-start | bytes 393224 | tf_op jit(solution)/shard_map/ppermute | solution.py:387
  24.2 3.1 %collective-permute-start.12 = (bf16[32,2048]{1,0:T(8,128)(2,1)S(1)}, bf16[32,2048]{1,0:T(8,128)(2,1)S(1)}, u32[]{:S(2)}, u32[]{:S(2)}) collective-permute-start(bf16[32,2048]{1,0:T(8,128)(2,1)S(1)} %get-tuple-element.76), channel_id=1, source_target_pairs={{0,20},{2,22},{4,16},{6,18},{8,28},{10,30},{12,24},{14,26},{16,4},... | collective-permute-start | bytes 393224 | tf_op jit(solution)/shard_map/ppermute | solution.py:387
  27.3 3.1 %collective-permute-start.13 = (bf16[32,2048]{1,0:T(8,128)(2,1)S(1)}, bf16[32,2048]{1,0:T(8,128)(2,1)S(1)}, u32[]{:S(2)}, u32[]{:S(2)}) collective-permute-start(bf16[32,2048]{1,0:T(8,128)(2,1)S(1)} %get-tuple-element.77), channel_id=1, source_target_pairs={{0,22},{2,20},{4,18},{6,16},{8,30},{10,28},{12,26},{14,24},{16,6},... | collective-permute-start | bytes 393224 | tf_op jit(solution)/shard_map/ppermute | solution.py:387
  30.7 8.7 %collective-permute-done.10.refs_0_ = bf16[32,2048]{1,0:T(8,128)(2,1)S(1)} collective-permute-done((bf16[32,2048]{1,0:T(8,128)(2,1)S(1)}, bf16[32,2048]{1,0:T(8,128)(2,1)S(1)}, u32[]{:S(2)}, u32[]{:S(2)}) %collective-permute-start.10) | collective-permute-done | bytes 131104 | tf_op jit(solution)/shard_map/ppermute | solution.py:387
  39.3 0.6 collective-permute-start.23
  39.9 2.8 %collective-permute-done.11.refs_1_ = bf16[32,2048]{1,0:T(8,128)(2,1)S(1)} collective-permute-done((bf16[32,2048]{1,0:T(8,128)(2,1)S(1)}, bf16[32,2048]{1,0:T(8,128)(2,1)S(1)}, u32[]{:S(2)}, u32[]{:S(2)}) %collective-permute-start.11) | collective-permute-done | bytes 131104 | tf_op jit(solution)/shard_map/ppermute | solution.py:387
  42.8 2.9 %collective-permute-done.12.refs_2_ = bf16[32,2048]{1,0:T(8,128)(2,1)S(1)} collective-permute-done((bf16[32,2048]{1,0:T(8,128)(2,1)S(1)}, bf16[32,2048]{1,0:T(8,128)(2,1)S(1)}, u32[]{:S(2)}, u32[]{:S(2)}) %collective-permute-start.12) | collective-permute-done | bytes 131104 | tf_op jit(solution)/shard_map/ppermute | solution.py:387
  45.7 0.9 collective-permute-start.25
  46.5 2.1 %collective-permute-done.13.refs_3_ = bf16[32,2048]{1,0:T(8,128)(2,1)S(1)} collective-permute-done((bf16[32,2048]{1,0:T(8,128)(2,1)S(1)}, bf16[32,2048]{1,0:T(8,128)(2,1)S(1)}, u32[]{:S(2)}, u32[]{:S(2)}) %collective-permute-start.13) | collective-permute-done | bytes 131104 | tf_op jit(solution)/shard_map/ppermute | solution.py:387
  48.6 2.4 %collective-permute-start.5 = (bf16[32,2048]{1,0:T(8,128)(2,1)S(1)}, bf16[32,2048]{1,0:T(8,128)(2,1)S(1)}, u32[]{:S(2)}, u32[]{:S(2)}) collective-permute-start(bf16[32,2048]{1,0:T(8,128)(2,1)S(1)} %get-tuple-element.68), channel_id=1, source_target_pairs={{0,24},{2,26},{4,28},{6,30},{8,16},{10,18},{12,20},{14,22},{16,8},... | collective-permute-start | bytes 393224 | tf_op jit(solution)/shard_map/ppermute | solution.py:387
  51.1 2.8 %collective-permute-start.6 = (bf16[32,2048]{1,0:T(8,128)(2,1)S(1)}, bf16[32,2048]{1,0:T(8,128)(2,1)S(1)}, u32[]{:S(2)}, u32[]{:S(2)}) collective-permute-start(bf16[32,2048]{1,0:T(8,128)(2,1)S(1)} %get-tuple-element.69), channel_id=1, source_target_pairs={{0,26},{2,24},{4,30},{6,28},{8,18},{10,16},{12,22},{14,20},{16,10}... | collective-permute-start | bytes 393224 | tf_op jit(solution)/shard_map/ppermute | solution.py:387
  54.0 2.2 %collective-permute-done.24.refs_6_ = bf16[32,2048]{1,0:T(8,128)(2,1)S(1)} collective-permute-done((bf16[32,2048]{1,0:T(8,128)(2,1)S(1)}, bf16[32,2048]{1,0:T(8,128)(2,1)S(1)}, u32[]{:S(2)}, u32[]{:S(2)}) %collective-permute-start.24) | collective-permute-done | bytes 131104 | tf_op jit(solution)/shard_map/ppermute | solution.py:387
  56.1 6.2 %collective-permute-start.7 = (bf16[32,2048]{1,0:T(8,128)(2,1)S(1)}, bf16[32,2048]{1,0:T(8,128)(2,1)S(1)}, u32[]{:S(2)}, u32[]{:S(2)}) collective-permute-start(bf16[32,2048]{1,0:T(8,128)(2,1)S(1)} %get-tuple-element.70), channel_id=1, source_target_pairs={{0,28},{2,30},{4,24},{6,26},{8,20},{10,22},{12,16},{14,18},{16,12}... | collective-permute-start | bytes 393224 | tf_op jit(solution)/shard_map/ppermute | solution.py:387
  62.6 3.4 %collective-permute-start.8 = (bf16[32,2048]{1,0:T(8,128)(2,1)S(1)}, bf16[32,2048]{1,0:T(8,128)(2,1)S(1)}, u32[]{:S(2)}, u32[]{:S(2)}) collective-permute-start(bf16[32,2048]{1,0:T(8,128)(2,1)S(1)} %get-tuple-element.71), channel_id=1, source_target_pairs={{0,30},{2,28},{4,26},{6,24},{8,22},{10,20},{12,18},{14,16},{16,14}... | collective-permute-start | bytes 393224 | tf_op jit(solution)/shard_map/ppermute | solution.py:387
  66.2 5.5 %collective-permute-done.8.refs_3_ = bf16[32,2048]{1,0:T(8,128)(2,1)S(1)} collective-permute-done((bf16[32,2048]{1,0:T(8,128)(2,1)S(1)}, bf16[32,2048]{1,0:T(8,128)(2,1)S(1)}, u32[]{:S(2)}, u32[]{:S(2)}) %collective-permute-start.8) | collective-permute-done | bytes 131104 | tf_op jit(solution)/shard_map/ppermute | solution.py:387
  72.3 4.7 %fetch.1 = (bf16[1,2048,1024]{2,1,0:T(8,128)(2,1)S(1)}, bf16[1,2048,1024]{2,1,0:T(8,128)(2,1)S(1)}, bf16[1,1024,2048]{2,1,0:T(8,128)(2,1)S(1)}) custom-call(bf16[1,2048,1024]{2,1,0:T(8,128)(2,1)} %gate_hbm.2, bf16[1,2048,1024]{2,1,0:T(8,128)(2,1)} %up_hbm.1, bf16[1,1024,2048]{2,1,0:T(8,128)(2,1)} %down_hbm.1), custom_call_target="tpu_custom_call" | custom-call | flops 12582912 | bytes 12582912 | tf_op jit(solution)/shard_map/fetch/pallas_call | solution.py:494
  77.0 1.9 %shard_map.119 = (bf16[32,2048]{1,0:T(8,128)(2,1)S(1)}, bf16[32,2048]{1,0:T(8,128)(2,1)S(1)}, bf16[32,2048]{1,0:T(8,128)(2,1)S(1)}, bf16[32,2048]{1,0:T(8,128)(2,1)S(1)}) custom-call(bf16[1,2048,1024]{2,1,0:T(8,128)(2,1)S(1)} %get-tuple-element.65.gate_ref, bf16[1,2048,1024]{2,1,0:T(8,128)(2,1)S(1)} %get-tuple-element.66.up_ref, ...), custom_call_target="tpu_custom_call" | custom-call | flops 1610612736 | bytes 12582912 | tf_op jit(solution)/shard_map/pallas_call | solution.py:521
  78.9 1.3 collective-permute-start.15
  80.2 3.5 %collective-permute-start.16 = (bf16[32,2048]{1,0:T(8,128)(2,1)S(1)}, bf16[32,2048]{1,0:T(8,128)(2,1)S(1)}, u32[]{:S(2)}, u32[]{:S(2)}) collective-permute-start(bf16[32,2048]{1,0:T(8,128)(2,1)S(1)} %get-tuple-element.79), channel_id=1, source_target_pairs={{0,18},{2,16},{4,22},{6,20},{8,26},{10,24},{12,30},{14,28},{16,2},... | collective-permute-start | bytes 393224 | tf_op jit(solution)/shard_map/ppermute | solution.py:387
  83.7 2.9 %collective-permute-start.17 = (bf16[32,2048]{1,0:T(8,128)(2,1)S(1)}, bf16[32,2048]{1,0:T(8,128)(2,1)S(1)}, u32[]{:S(2)}, u32[]{:S(2)}) collective-permute-start(bf16[32,2048]{1,0:T(8,128)(2,1)S(1)} %get-tuple-element.80), channel_id=1, source_target_pairs={{0,20},{2,22},{4,16},{6,18},{8,28},{10,30},{12,24},{14,26},{16,4},... | collective-permute-start | bytes 393224 | tf_op jit(solution)/shard_map/ppermute | solution.py:387
  86.6 1.9 %shard_map.118 = (bf16[32,2048]{1,0:T(8,128)(2,1)S(1)}, bf16[32,2048]{1,0:T(8,128)(2,1)S(1)}, bf16[32,2048]{1,0:T(8,128)(2,1)S(1)}, bf16[32,2048]{1,0:T(8,128)(2,1)S(1)}) custom-call(bf16[1,2048,1024]{2,1,0:T(8,128)(2,1)S(1)} %get-tuple-element.65.gate_ref, bf16[1,2048,1024]{2,1,0:T(8,128)(2,1)S(1)} %get-tuple-element.66.up_ref, ...), custom_call_target="tpu_custom_call" | custom-call | flops 1610612736 | bytes 12582912 | tf_op jit(solution)/shard_map/pallas_call | solution.py:521
  88.4 1.0 collective-permute-start.18
  89.4 3.9 %collective-permute-start.34 = (bf16[32,2048]{1,0:T(8,128)(2,1)S(1)}, bf16[32,2048]{1,0:T(8,128)(2,1)S(1)}, u32[]{:S(2)}, u32[]{:S(2)}) collective-permute-start(bf16[32,2048]{1,0:T(8,128)(2,1)S(1)} %get-tuple-element.72), channel_id=1, source_target_pairs={{0,24},{2,26},{4,28},{6,30},{8,16},{10,18},{12,20},{14,22},{16,8},... | collective-permute-start | bytes 393224 | tf_op jit(solution)/shard_map/ppermute | solution.py:387
  93.3 3.5 %shard_map.120 = (bf16[32,2048]{1,0:T(8,128)(2,1)S(1)}, bf16[32,2048]{1,0:T(8,128)(2,1)S(1)}, bf16[32,2048]{1,0:T(8,128)(2,1)S(1)}, bf16[32,2048]{1,0:T(8,128)(2...) custom-call(bf16[1,2048,1024]{2,1,0:T(8,128)(2,1)S(1)} %get-tuple-el, ...), custom_call_target="tpu_custom_call" | custom-call | flops 3221225472 | bytes 12582912 | tf_op jit(solution)/shard_map/pallas_call | solution.py:521
  96.8 3.2 %collective-permute-done.15.refs_0_ = bf16[32,2048]{1,0:T(8,128)(2,1)S(1)} collective-permute-done((bf16[32,2048]{1,0:T(8,128)(2,1)S(1)}, bf16[32,2048]{1,0:T(8,128)(2,1)S(1)}, u32[]{:S(2)}, u32[]{:S(2)}) %collective-permute-start.15) | collective-permute-done | bytes 131104 | tf_op jit(solution)/shard_map/ppermute | solution.py:387
  100.0 5.1 %collective-permute-start.35 = (bf16[32,2048]{1,0:T(8,128)(2,1)S(1)}, bf16[32,2048]{1,0:T(8,128)(2,1)S(1)}, u32[]{:S(2)}, u32[]{:S(2)}) collective-permute-start(bf16[32,2048]{1,0:T(8,128)(2,1)S(1)} %get-tuple-element.98), channel_id=1, source_target_pairs={{0,26},{2,24},{4,30},{6,28},{8,18},{10,16},{12,22},{14,20},{16,10}... | collective-permute-start | bytes 393224 | tf_op jit(solution)/shard_map/ppermute | solution.py:387
  105.1 1.2 collective-permute-start.36
  106.2 6.6 %collective-permute-done.17.refs_2_ = bf16[32,2048]{1,0:T(8,128)(2,1)S(1)} collective-permute-done((bf16[32,2048]{1,0:T(8,128)(2,1)S(1)}, bf16[32,2048]{1,0:T(8,128)(2,1)S(1)}, u32[]{:S(2)}, u32[]{:S(2)}) %collective-permute-start.17) | collective-permute-done | bytes 131104 | tf_op jit(solution)/shard_map/ppermute | solution.py:387
  112.9 4.9 %collective-permute-start.37 = (bf16[32,2048]{1,0:T(8,128)(2,1)S(1)}, bf16[32,2048]{1,0:T(8,128)(2,1)S(1)}, u32[]{:S(2)}, u32[]{:S(2)}) collective-permute-start(bf16[32,2048]{1,0:T(8,128)(2,1)S(1)} %get-tuple-element.100), channel_id=1, source_target_pairs={{0,30},{2,28},{4,26},{6,24},{8,22},{10,20},{12,18},{14,16},{16,14}... | collective-permute-start | bytes 393224 | tf_op jit(solution)/shard_map/ppermute | solution.py:387
  118.0 2.3 %collective-permute-start.28 = (bf16[32,2048]{1,0:T(8,128)(2,1)S(1)}, bf16[32,2048]{1,0:T(8,128)(2,1)S(1)}, u32[]{:S(2)}, u32[]{:S(2)}) collective-permute-start(bf16[32,2048]{1,0:T(8,128)(2,1)S(1)} %get-tuple-element.92), channel_id=1, source_target_pairs={{0,4},{2,6},{4,0},{6,2},{8,12},{10,14},{12,8},{14,10},{16,20},{18,... | collective-permute-start | bytes 393224 | tf_op jit(solution)/shard_map/ppermute | solution.py:387
  120.3 1.5 %collective-permute-start.29 = (bf16[32,2048]{1,0:T(8,128)(2,1)S(1)}, bf16[32,2048]{1,0:T(8,128)(2,1)S(1)}, u32[]{:S(2)}, u32[]{:S(2)}) collective-permute-start(bf16[32,2048]{1,0:T(8,128)(2,1)S(1)} %get-tuple-element.93), channel_id=1, source_target_pairs={{0,6},{2,4},{4,2},{6,0},{8,14},{10,12},{12,10},{14,8},{16,22},{18,... | collective-permute-start | bytes 393224 | tf_op jit(solution)/shard_map/ppermute | solution.py:387
  121.8 5.7 %collective-permute-start.30 = (bf16[32,2048]{1,0:T(8,128)(2,1)S(1)}, bf16[32,2048]{1,0:T(8,128)(2,1)S(1)}, u32[]{:S(2)}, u32[]{:S(2)}) collective-permute-start(bf16[32,2048]{1,0:T(8,128)(2,1)S(1)} %get-tuple-element.94), channel_id=1, source_target_pairs={{0,8},{2,10},{4,12},{6,14},{8,0},{10,2},{12,4},{14,6},{16,24},{18,... | collective-permute-start | bytes 393224 | tf_op jit(solution)/shard_map/ppermute | solution.py:387
  127.5 4.1 %collective-permute-start.31 = (bf16[32,2048]{1,0:T(8,128)(2,1)S(1)}, bf16[32,2048]{1,0:T(8,128)(2,1)S(1)}, u32[]{:S(2)}, u32[]{:S(2)}) collective-permute-start(bf16[32,2048]{1,0:T(8,128)(2,1)S(1)} %get-tuple-element.95), channel_id=1, source_target_pairs={{0,10},{2,8},{4,14},{6,12},{8,2},{10,0},{12,6},{14,4},{16,26},{18,... | collective-permute-start | bytes 393224 | tf_op jit(solution)/shard_map/ppermute | solution.py:387
  131.6 1.8 %collective-permute-start.32 = (bf16[32,2048]{1,0:T(8,128)(2,1)S(1)}, bf16[32,2048]{1,0:T(8,128)(2,1)S(1)}, u32[]{:S(2)}, u32[]{:S(2)}) collective-permute-start(bf16[32,2048]{1,0:T(8,128)(2,1)S(1)} %get-tuple-element.96), channel_id=1, source_target_pairs={{0,12},{2,14},{4,8},{6,10},{8,4},{10,6},{12,0},{14,2},{16,28},{18,... | collective-permute-start | bytes 393224 | tf_op jit(solution)/shard_map/ppermute | solution.py:387
  133.4 2.8 %collective-permute-start.33 = (bf16[32,2048]{1,0:T(8,128)(2,1)S(1)}, bf16[32,2048]{1,0:T(8,128)(2,1)S(1)}, u32[]{:S(2)}, u32[]{:S(2)}) collective-permute-start(bf16[32,2048]{1,0:T(8,128)(2,1)S(1)} %get-tuple-element.97), channel_id=1, source_target_pairs={{0,14},{2,12},{4,10},{6,8},{8,6},{10,4},{12,2},{14,0},{16,30},{18,... | collective-permute-start | bytes 393224 | tf_op jit(solution)/shard_map/ppermute | solution.py:387
  136.1 1.8 %gather.1 = (f32[128,2048]{1,0:T(8,128)S(1)}, f32[128,2048]{1,0:T(8,128)S(1)}) custom-call(s32[2]{0:T(128)S(1)} %pad_add_fusion.where_ref, f32[4,128]{1,0:T(4,128)S(1)} %get-tuple-element.101.meta_ref, f32[4,128]{1,0:T(4,128)S(1)} %collective-permute-done.4.meta_other_ref.meta_ref, bf16[32,2048]{1,0:T(8,128)(2,1)S(1)} %collective-permute-done.15.refs_0_, ...), custom_call_target="tpu_custom_call" | custom-call | tf_op jit(solution)/shard_map/gather/pallas_call | solution.py:545
  138.0 2.2 %collective-permute-done.32.refs_6_ = bf16[32,2048]{1,0:T(8,128)(2,1)S(1)} collective-permute-done((bf16[32,2048]{1,0:T(8,128)(2,1)S(1)}, bf16[32,2048]{1,0:T(8,128)(2,1)S(1)}, u32[]{:S(2)}, u32[]{:S(2)}) %collective-permute-start.32) | collective-permute-done | bytes 131104 | tf_op jit(solution)/shard_map/ppermute | solution.py:387
  140.1 1.8 %collective-permute-done.33.refs_7_ = bf16[32,2048]{1,0:T(8,128)(2,1)S(1)} collective-permute-done((bf16[32,2048]{1,0:T(8,128)(2,1)S(1)}, bf16[32,2048]{1,0:T(8,128)(2,1)S(1)}, u32[]{:S(2)}, u32[]{:S(2)}) %collective-permute-start.33) | collective-permute-done | bytes 131104 | tf_op jit(solution)/shard_map/ppermute | solution.py:387
  141.9 1.5 %shard_map.121 = bf16[128,2048]{1,0:T(8,128)(2,1)S(1)} custom-call(s32[2]{0:T(128)S(1)} %pad_add_fusion.where_ref, f32[4,128]{1,0:T(4,128)S(1)} %collective-permute-done.4.meta_other_ref.meta_ref, f32[128,2048]{1,0:T(8,128)S(1)} %get-tuple-element.82.base_ref, bf16[32,2048]{1,0:T(8,128)(2,1)S(1)} %get-tuple-element.90.refs_0_, ...), custom_call_target="tpu_custom_call" | custom-call | tf_op jit(solution)/shard_map/pallas_call | solution.py:555
  143.5 1.5 %shard_map.122.own_ref = f32[128,2048]{1,0:T(8,128)S(1)} custom-call(s32[2]{0:T(128)S(1)} %pad_add_fusion.where_ref, f32[4,128]{1,0:T(4,128)S(1)} %get-tuple-element.101.meta_ref, f32[128,2048]{1,0:T(8,128)S(1)} %get-tuple-element.102.base_ref, bf16[32,2048]{1,0:T(8,128)(2,1)S(1)} %get-tuple-element.90.refs_0_, ...), custom_call_target="tpu_custom_call" | custom-call | tf_op jit(solution)/shard_map/pallas_call | solution.py:555
  145.4 0.9 combine.1
  (45 shorter events, 3.5 us)
Async XLA Ops:
  1.4 6.2 %collective-permute-start = (bf16[144,768]{1,0:T(8,128)(2,1)S(1)}, bf16[144,768]{1,0:T(8,128)(2,1)S(1)}, u32[]{:S(2)}, u32[]{:S(2)}) collective-permute-start(bf16[144,768]{1,0:T(8,128)(2,1)S(1)} %get-tuple-element.55), channel_id=1, source_target_pairs={{0,1},{1,0},{2,3},{3,2},{4,5},{5,4},{6,7},{7,6},{8,9},{9,8},{10,11... | collective-permute-start | bytes 663560 | tf_op jit(solution)/shard_map/ppermute | solution.py:426
  2.0 5.6 %collective-permute-start.1 = (f32[32,768]{1,0:T(8,128)S(1)}, f32[32,768]{1,0:T(8,128)S(1)}, u32[]{:S(2)}, u32[]{:S(2)}) collective-permute-start(f32[32,768]{1,0:T(8,128)S(1)} %get-tuple-element.56.taps_ref), channel_id=1, source_target_pairs={{0,1},{1,0},{2,3},{3,2},{4,5},{5,4},{6,7},{7,6},{8,9},{9,8},{10,11... | collective-permute-start | bytes 294920 | tf_op jit(solution)/shard_map/ppermute | solution.py:427
  2.1 9.0 %collective-permute-start.2 = (bf16[16,768]{1,0:T(8,128)(2,1)S(1)}, bf16[16,768]{1,0:T(8,128)(2,1)S(1)}, u32[]{:S(2)}, u32[]{:S(2)}) collective-permute-start(bf16[16,768]{1,0:T(8,128)(2,1)S(1)} %get-tuple-element.58), channel_id=1, source_target_pairs={{0,2},{2,4},{3,1},{4,6},{5,3},{6,8},{7,5},{8,10},{9,7},{10,12},{11... | collective-permute-start | bytes 73736 | tf_op jit(solution)/shard_map/ppermute | solution.py:428
  6.9 4.2 %collective-permute-start.3 = (bf16[16,768]{1,0:T(8,128)(2,1)S(1)}, bf16[16,768]{1,0:T(8,128)(2,1)S(1)}, u32[]{:S(2)}, u32[]{:S(2)}) collective-permute-start(bf16[16,768]{1,0:T(8,128)(2,1)S(1)} %get-tuple-element.59), channel_id=1, source_target_pairs={{1,2},{3,4},{2,1},{5,6},{4,3},{7,8},{6,5},{9,10},{8,7},{11,12},{10... | collective-permute-start | bytes 73736 | tf_op jit(solution)/shard_map/ppermute | solution.py:429
  15.1 9.1 %collective-permute-start.19 = (bf16[32,2048]{1,0:T(8,128)(2,1)S(1)}, bf16[32,2048]{1,0:T(8,128)(2,1)S(1)}, u32[]{:S(2)}, u32[]{:S(2)}) collective-permute-start(bf16[32,2048]{1,0:T(8,128)(2,1)S(1)} %get-tuple-element.83), channel_id=1, source_target_pairs={{0,2},{2,0},{4,6},{6,4},{8,10},{10,8},{12,14},{14,12},{16,18},{18,... | collective-permute-start | bytes 393224 | tf_op jit(solution)/shard_map/ppermute | solution.py:387
  17.9 9.4 %collective-permute-start.20 = (bf16[32,2048]{1,0:T(8,128)(2,1)S(1)}, bf16[32,2048]{1,0:T(8,128)(2,1)S(1)}, u32[]{:S(2)}, u32[]{:S(2)}) collective-permute-start(bf16[32,2048]{1,0:T(8,128)(2,1)S(1)} %get-tuple-element.84), channel_id=1, source_target_pairs={{0,4},{2,6},{4,0},{6,2},{8,12},{10,14},{12,8},{14,10},{16,20},{18,... | collective-permute-start | bytes 393224 | tf_op jit(solution)/shard_map/ppermute | solution.py:387
  19.5 11.0 %collective-permute-start.21 = (bf16[32,2048]{1,0:T(8,128)(2,1)S(1)}, bf16[32,2048]{1,0:T(8,128)(2,1)S(1)}, u32[]{:S(2)}, u32[]{:S(2)}) collective-permute-start(bf16[32,2048]{1,0:T(8,128)(2,1)S(1)} %get-tuple-element.85), channel_id=1, source_target_pairs={{0,6},{2,4},{4,2},{6,0},{8,14},{10,12},{12,10},{14,8},{16,22},{18,... | collective-permute-start | bytes 393224 | tf_op jit(solution)/shard_map/ppermute | solution.py:387
  20.0 19.3 %collective-permute-start.10 = (bf16[32,2048]{1,0:T(8,128)(2,1)S(1)}, bf16[32,2048]{1,0:T(8,128)(2,1)S(1)}, u32[]{:S(2)}, u32[]{:S(2)}) collective-permute-start(bf16[32,2048]{1,0:T(8,128)(2,1)S(1)} %get-tuple-element.74), channel_id=1, source_target_pairs={{0,16},{2,18},{4,20},{6,22},{8,24},{10,26},{12,28},{14,30},{16,0},... | collective-permute-start | bytes 393224 | tf_op jit(solution)/shard_map/ppermute | solution.py:387
  24.0 18.7 %collective-permute-start.11 = (bf16[32,2048]{1,0:T(8,128)(2,1)S(1)}, bf16[32,2048]{1,0:T(8,128)(2,1)S(1)}, u32[]{:S(2)}, u32[]{:S(2)}) collective-permute-start(bf16[32,2048]{1,0:T(8,128)(2,1)S(1)} %get-tuple-element.75), channel_id=1, source_target_pairs={{0,18},{2,16},{4,22},{6,20},{8,26},{10,24},{12,30},{14,28},{16,2},... | collective-permute-start | bytes 393224 | tf_op jit(solution)/shard_map/ppermute | solution.py:387
  24.2 21.5 %collective-permute-start.12 = (bf16[32,2048]{1,0:T(8,128)(2,1)S(1)}, bf16[32,2048]{1,0:T(8,128)(2,1)S(1)}, u32[]{:S(2)}, u32[]{:S(2)}) collective-permute-start(bf16[32,2048]{1,0:T(8,128)(2,1)S(1)} %get-tuple-element.76), channel_id=1, source_target_pairs={{0,20},{2,22},{4,16},{6,18},{8,28},{10,30},{12,24},{14,26},{16,4},... | collective-permute-start | bytes 393224 | tf_op jit(solution)/shard_map/ppermute | solution.py:387
  27.3 21.3 %collective-permute-start.13 = (bf16[32,2048]{1,0:T(8,128)(2,1)S(1)}, bf16[32,2048]{1,0:T(8,128)(2,1)S(1)}, u32[]{:S(2)}, u32[]{:S(2)}) collective-permute-start(bf16[32,2048]{1,0:T(8,128)(2,1)S(1)} %get-tuple-element.77), channel_id=1, source_target_pairs={{0,22},{2,20},{4,18},{6,16},{8,30},{10,28},{12,26},{14,24},{16,6},... | collective-permute-start | bytes 393224 | tf_op jit(solution)/shard_map/ppermute | solution.py:387
  30.5 20.6 %collective-permute-start.22 = (bf16[32,2048]{1,0:T(8,128)(2,1)S(1)}, bf16[32,2048]{1,0:T(8,128)(2,1)S(1)}, u32[]{:S(2)}, u32[]{:S(2)}) collective-permute-start(bf16[32,2048]{1,0:T(8,128)(2,1)S(1)} %get-tuple-element.86), channel_id=1, source_target_pairs={{0,8},{2,10},{4,12},{6,14},{8,0},{10,2},{12,4},{14,6},{16,24},{18,... | collective-permute-start | bytes 393224 | tf_op jit(solution)/shard_map/ppermute | solution.py:387
  39.3 11.8 %collective-permute-start.23 = (bf16[32,2048]{1,0:T(8,128)(2,1)S(1)}, bf16[32,2048]{1,0:T(8,128)(2,1)S(1)}, u32[]{:S(2)}, u32[]{:S(2)}) collective-permute-start(bf16[32,2048]{1,0:T(8,128)(2,1)S(1)} %get-tuple-element.87), channel_id=1, source_target_pairs={{0,10},{2,8},{4,14},{6,12},{8,2},{10,0},{12,6},{14,4},{16,26},{18,... | collective-permute-start | bytes 393224 | tf_op jit(solution)/shard_map/ppermute | solution.py:387
  42.7 13.4 %collective-permute-start.24 = (bf16[32,2048]{1,0:T(8,128)(2,1)S(1)}, bf16[32,2048]{1,0:T(8,128)(2,1)S(1)}, u32[]{:S(2)}, u32[]{:S(2)}) collective-permute-start(bf16[32,2048]{1,0:T(8,128)(2,1)S(1)} %get-tuple-element.88), channel_id=1, source_target_pairs={{0,12},{2,14},{4,8},{6,10},{8,4},{10,6},{12,0},{14,2},{16,28},{18,... | collective-permute-start | bytes 393224 | tf_op jit(solution)/shard_map/ppermute | solution.py:387
  45.7 16.9 %collective-permute-start.25 = (bf16[32,2048]{1,0:T(8,128)(2,1)S(1)}, bf16[32,2048]{1,0:T(8,128)(2,1)S(1)}, u32[]{:S(2)}, u32[]{:S(2)}) collective-permute-start(bf16[32,2048]{1,0:T(8,128)(2,1)S(1)} %get-tuple-element.89), channel_id=1, source_target_pairs={{0,14},{2,12},{4,10},{6,8},{8,6},{10,4},{12,2},{14,0},{16,30},{18,... | collective-permute-start | bytes 393224 | tf_op jit(solution)/shard_map/ppermute | solution.py:387
  48.6 17.4 %collective-permute-start.5 = (bf16[32,2048]{1,0:T(8,128)(2,1)S(1)}, bf16[32,2048]{1,0:T(8,128)(2,1)S(1)}, u32[]{:S(2)}, u32[]{:S(2)}) collective-permute-start(bf16[32,2048]{1,0:T(8,128)(2,1)S(1)} %get-tuple-element.68), channel_id=1, source_target_pairs={{0,24},{2,26},{4,28},{6,30},{8,16},{10,18},{12,20},{14,22},{16,8},... | collective-permute-start | bytes 393224 | tf_op jit(solution)/shard_map/ppermute | solution.py:387
  51.0 26.0 %collective-permute-start.14 = (bf16[64,2048]{1,0:T(8,128)(2,1)S(1)}, bf16[64,2048]{1,0:T(8,128)(2,1)S(1)}, u32[]{:S(2)}, u32[]{:S(2)}) collective-permute-start(bf16[64,2048]{1,0:T(8,128)(2,1)S(1)} %pack.4), channel_id=1, source_target_pairs={{0,1},{1,0},{2,3},{3,2},{4,5},{5,4},{6,7},{7,6},{8,9},{9,8},{10,11... | collective-permute-start | bytes 786440 | tf_op jit(solution)/shard_map/ppermute | solution.py:520
  51.1 15.0 %collective-permute-start.6 = (bf16[32,2048]{1,0:T(8,128)(2,1)S(1)}, bf16[32,2048]{1,0:T(8,128)(2,1)S(1)}, u32[]{:S(2)}, u32[]{:S(2)}) collective-permute-start(bf16[32,2048]{1,0:T(8,128)(2,1)S(1)} %get-tuple-element.69), channel_id=1, source_target_pairs={{0,26},{2,24},{4,30},{6,28},{8,18},{10,16},{12,22},{14,20},{16,10}... | collective-permute-start | bytes 393224 | tf_op jit(solution)/shard_map/ppermute | solution.py:387
  56.1 10.0 %collective-permute-start.7 = (bf16[32,2048]{1,0:T(8,128)(2,1)S(1)}, bf16[32,2048]{1,0:T(8,128)(2,1)S(1)}, u32[]{:S(2)}, u32[]{:S(2)}) collective-permute-start(bf16[32,2048]{1,0:T(8,128)(2,1)S(1)} %get-tuple-element.70), channel_id=1, source_target_pairs={{0,28},{2,30},{4,24},{6,26},{8,20},{10,22},{12,16},{14,18},{16,12}... | collective-permute-start | bytes 393224 | tf_op jit(solution)/shard_map/ppermute | solution.py:387
  62.6 9.1 %collective-permute-start.8 = (bf16[32,2048]{1,0:T(8,128)(2,1)S(1)}, bf16[32,2048]{1,0:T(8,128)(2,1)S(1)}, u32[]{:S(2)}, u32[]{:S(2)}) collective-permute-start(bf16[32,2048]{1,0:T(8,128)(2,1)S(1)} %get-tuple-element.71), channel_id=1, source_target_pairs={{0,30},{2,28},{4,26},{6,24},{8,22},{10,20},{12,18},{14,16},{16,14}... | collective-permute-start | bytes 393224 | tf_op jit(solution)/shard_map/ppermute | solution.py:387
  66.1 23.3 %collective-permute-start.26 = (bf16[128,2048]{1,0:T(8,128)(2,1)S(1)}, bf16[128,2048]{1,0:T(8,128)(2,1)S(1)}, u32[]{:S(2)}, u32[]{:S(2)}) collective-permute-start(bf16[128,2048]{1,0:T(8,128)(2,1)S(1)} %pack.5), channel_id=1, source_target_pairs={{0,1},{1,0},{2,3},{3,2},{4,5},{5,4},{6,7},{7,6},{8,9},{9,8},{10,11... | collective-permute-start | bytes 1572872 | tf_op jit(solution)/shard_map/ppermute | solution.py:520
  71.7 12.0 %collective-permute-start.9 = (bf16[64,2048]{1,0:T(8,128)(2,1)S(1)}, bf16[64,2048]{1,0:T(8,128)(2,1)S(1)}, u32[]{:S(2)}, u32[]{:S(2)}) collective-permute-start(bf16[64,2048]{1,0:T(8,128)(2,1)S(1)} %pack.3), channel_id=1, source_target_pairs={{0,1},{1,0},{2,3},{3,2},{4,5},{5,4},{6,7},{7,6},{8,9},{9,8},{10,11... | collective-permute-start | bytes 786440 | tf_op jit(solution)/shard_map/ppermute | solution.py:520
  71.8 16.6 %collective-permute-start.4 = (f32[4,128]{1,0:T(4,128)S(1)}, f32[4,128]{1,0:T(4,128)S(1)}, u32[]{:S(2)}, u32[]{:S(2)}) collective-permute-start(f32[4,128]{1,0:T(4,128)S(1)} %get-tuple-element.101.meta_ref), channel_id=1, source_target_pairs={{0,1},{1,0},{2,3},{3,2},{4,5},{5,4},{6,7},{7,6},{8,9},{9,8},{10,11... | collective-permute-start | bytes 6152 | tf_op jit(solution)/shard_map/ppermute | solution.py:430
  78.9 21.1 %collective-permute-start.15 = (bf16[32,2048]{1,0:T(8,128)(2,1)S(1)}, bf16[32,2048]{1,0:T(8,128)(2,1)S(1)}, u32[]{:S(2)}, u32[]{:S(2)}) collective-permute-start(bf16[32,2048]{1,0:T(8,128)(2,1)S(1)} %get-tuple-element.78), channel_id=1, source_target_pairs={{0,16},{2,18},{4,20},{6,22},{8,24},{10,26},{12,28},{14,30},{16,0},... | collective-permute-start | bytes 393224 | tf_op jit(solution)/shard_map/ppermute | solution.py:387
  80.2 24.8 %collective-permute-start.16 = (bf16[32,2048]{1,0:T(8,128)(2,1)S(1)}, bf16[32,2048]{1,0:T(8,128)(2,1)S(1)}, u32[]{:S(2)}, u32[]{:S(2)}) collective-permute-start(bf16[32,2048]{1,0:T(8,128)(2,1)S(1)} %get-tuple-element.79), channel_id=1, source_target_pairs={{0,18},{2,16},{4,22},{6,20},{8,26},{10,24},{12,30},{14,28},{16,2},... | collective-permute-start | bytes 393224 | tf_op jit(solution)/shard_map/ppermute | solution.py:387
  83.7 29.1 %collective-permute-start.17 = (bf16[32,2048]{1,0:T(8,128)(2,1)S(1)}, bf16[32,2048]{1,0:T(8,128)(2,1)S(1)}, u32[]{:S(2)}, u32[]{:S(2)}) collective-permute-start(bf16[32,2048]{1,0:T(8,128)(2,1)S(1)} %get-tuple-element.80), channel_id=1, source_target_pairs={{0,20},{2,22},{4,16},{6,18},{8,28},{10,30},{12,24},{14,26},{16,4},... | collective-permute-start | bytes 393224 | tf_op jit(solution)/shard_map/ppermute | solution.py:387
  88.4 29.6 %collective-permute-start.18 = (bf16[32,2048]{1,0:T(8,128)(2,1)S(1)}, bf16[32,2048]{1,0:T(8,128)(2,1)S(1)}, u32[]{:S(2)}, u32[]{:S(2)}) collective-permute-start(bf16[32,2048]{1,0:T(8,128)(2,1)S(1)} %get-tuple-element.81), channel_id=1, source_target_pairs={{0,22},{2,20},{4,18},{6,16},{8,30},{10,28},{12,26},{14,24},{16,6},... | collective-permute-start | bytes 393224 | tf_op jit(solution)/shard_map/ppermute | solution.py:387
  89.4 28.6 %collective-permute-start.34 = (bf16[32,2048]{1,0:T(8,128)(2,1)S(1)}, bf16[32,2048]{1,0:T(8,128)(2,1)S(1)}, u32[]{:S(2)}, u32[]{:S(2)}) collective-permute-start(bf16[32,2048]{1,0:T(8,128)(2,1)S(1)} %get-tuple-element.72), channel_id=1, source_target_pairs={{0,24},{2,26},{4,28},{6,30},{8,16},{10,18},{12,20},{14,22},{16,8},... | collective-permute-start | bytes 393224 | tf_op jit(solution)/shard_map/ppermute | solution.py:387
  100.0 20.3 %collective-permute-start.35 = (bf16[32,2048]{1,0:T(8,128)(2,1)S(1)}, bf16[32,2048]{1,0:T(8,128)(2,1)S(1)}, u32[]{:S(2)}, u32[]{:S(2)}) collective-permute-start(bf16[32,2048]{1,0:T(8,128)(2,1)S(1)} %get-tuple-element.98), channel_id=1, source_target_pairs={{0,26},{2,24},{4,30},{6,28},{8,18},{10,16},{12,22},{14,20},{16,10}... | collective-permute-start | bytes 393224 | tf_op jit(solution)/shard_map/ppermute | solution.py:387
  105.1 16.8 %collective-permute-start.36 = (bf16[32,2048]{1,0:T(8,128)(2,1)S(1)}, bf16[32,2048]{1,0:T(8,128)(2,1)S(1)}, u32[]{:S(2)}, u32[]{:S(2)}) collective-permute-start(bf16[32,2048]{1,0:T(8,128)(2,1)S(1)} %get-tuple-element.99), channel_id=1, source_target_pairs={{0,28},{2,30},{4,24},{6,26},{8,20},{10,22},{12,16},{14,18},{16,12}... | collective-permute-start | bytes 393224 | tf_op jit(solution)/shard_map/ppermute | solution.py:387
  112.9 14.7 %collective-permute-start.37 = (bf16[32,2048]{1,0:T(8,128)(2,1)S(1)}, bf16[32,2048]{1,0:T(8,128)(2,1)S(1)}, u32[]{:S(2)}, u32[]{:S(2)}) collective-permute-start(bf16[32,2048]{1,0:T(8,128)(2,1)S(1)} %get-tuple-element.100), channel_id=1, source_target_pairs={{0,30},{2,28},{4,26},{6,24},{8,22},{10,20},{12,18},{14,16},{16,14}... | collective-permute-start | bytes 393224 | tf_op jit(solution)/shard_map/ppermute | solution.py:387
  118.0 13.6 %collective-permute-start.27 = (bf16[32,2048]{1,0:T(8,128)(2,1)S(1)}, bf16[32,2048]{1,0:T(8,128)(2,1)S(1)}, u32[]{:S(2)}, u32[]{:S(2)}) collective-permute-start(bf16[32,2048]{1,0:T(8,128)(2,1)S(1)} %get-tuple-element.91), channel_id=1, source_target_pairs={{0,2},{2,0},{4,6},{6,4},{8,10},{10,8},{12,14},{14,12},{16,18},{18,... | collective-permute-start | bytes 393224 | tf_op jit(solution)/shard_map/ppermute | solution.py:387
  118.0 15.3 %collective-permute-start.28 = (bf16[32,2048]{1,0:T(8,128)(2,1)S(1)}, bf16[32,2048]{1,0:T(8,128)(2,1)S(1)}, u32[]{:S(2)}, u32[]{:S(2)}) collective-permute-start(bf16[32,2048]{1,0:T(8,128)(2,1)S(1)} %get-tuple-element.92), channel_id=1, source_target_pairs={{0,4},{2,6},{4,0},{6,2},{8,12},{10,14},{12,8},{14,10},{16,20},{18,... | collective-permute-start | bytes 393224 | tf_op jit(solution)/shard_map/ppermute | solution.py:387
  120.3 17.6 %collective-permute-start.29 = (bf16[32,2048]{1,0:T(8,128)(2,1)S(1)}, bf16[32,2048]{1,0:T(8,128)(2,1)S(1)}, u32[]{:S(2)}, u32[]{:S(2)}) collective-permute-start(bf16[32,2048]{1,0:T(8,128)(2,1)S(1)} %get-tuple-element.93), channel_id=1, source_target_pairs={{0,6},{2,4},{4,2},{6,0},{8,14},{10,12},{12,10},{14,8},{16,22},{18,... | collective-permute-start | bytes 393224 | tf_op jit(solution)/shard_map/ppermute | solution.py:387
  121.8 16.1 %collective-permute-start.30 = (bf16[32,2048]{1,0:T(8,128)(2,1)S(1)}, bf16[32,2048]{1,0:T(8,128)(2,1)S(1)}, u32[]{:S(2)}, u32[]{:S(2)}) collective-permute-start(bf16[32,2048]{1,0:T(8,128)(2,1)S(1)} %get-tuple-element.94), channel_id=1, source_target_pairs={{0,8},{2,10},{4,12},{6,14},{8,0},{10,2},{12,4},{14,6},{16,24},{18,... | collective-permute-start | bytes 393224 | tf_op jit(solution)/shard_map/ppermute | solution.py:387
  127.5 10.4 %collective-permute-start.31 = (bf16[32,2048]{1,0:T(8,128)(2,1)S(1)}, bf16[32,2048]{1,0:T(8,128)(2,1)S(1)}, u32[]{:S(2)}, u32[]{:S(2)}) collective-permute-start(bf16[32,2048]{1,0:T(8,128)(2,1)S(1)} %get-tuple-element.95), channel_id=1, source_target_pairs={{0,10},{2,8},{4,14},{6,12},{8,2},{10,0},{12,6},{14,4},{16,26},{18,... | collective-permute-start | bytes 393224 | tf_op jit(solution)/shard_map/ppermute | solution.py:387
  131.6 8.5 %collective-permute-start.32 = (bf16[32,2048]{1,0:T(8,128)(2,1)S(1)}, bf16[32,2048]{1,0:T(8,128)(2,1)S(1)}, u32[]{:S(2)}, u32[]{:S(2)}) collective-permute-start(bf16[32,2048]{1,0:T(8,128)(2,1)S(1)} %get-tuple-element.96), channel_id=1, source_target_pairs={{0,12},{2,14},{4,8},{6,10},{8,4},{10,6},{12,0},{14,2},{16,28},{18,... | collective-permute-start | bytes 393224 | tf_op jit(solution)/shard_map/ppermute | solution.py:387
  133.4 8.6 %collective-permute-start.33 = (bf16[32,2048]{1,0:T(8,128)(2,1)S(1)}, bf16[32,2048]{1,0:T(8,128)(2,1)S(1)}, u32[]{:S(2)}, u32[]{:S(2)}) collective-permute-start(bf16[32,2048]{1,0:T(8,128)(2,1)S(1)} %get-tuple-element.97), channel_id=1, source_target_pairs={{0,14},{2,12},{4,10},{6,8},{8,6},{10,4},{12,2},{14,0},{16,30},{18,... | collective-permute-start | bytes 393224 | tf_op jit(solution)/shard_map/ppermute | solution.py:387
  143.4 2.0 %collective-permute-start.38 = (bf16[128,2048]{1,0:T(8,128)(2,1)S(1)}, bf16[128,2048]{1,0:T(8,128)(2,1)S(1)}, u32[]{:S(2)}, u32[]{:S(2)}) collective-permute-start(bf16[128,2048]{1,0:T(8,128)(2,1)S(1)} %shard_map.121), channel_id=1, source_target_pairs={{0,1},{1,0},{2,3},{3,2},{4,5},{5,4},{6,7},{7,6},{8,9},{9,8},{10,11... | collective-permute-start | bytes 1572872 | tf_op jit(solution)/shard_map/ppermute | solution.py:564
